TPU v7x, 256 devices: a whole 4x4x8 slice. The times are simulated.
256 devices in a mesh: sp: 32 (over z, x), tp: 8 (over y, core).
Axes of the slice: x: 4, y: 4, z: 8, core: 2. Of those that a mesh axis runs over, the one named last changes fastest.
Arguments:
- mixer_input: bfloat16 [8192, 1024], P('sp', 'tp'), may hold values from -8 to 8
- decay_shift: float32 [8192, 64], P('sp', 'tp'), may hold values from -2.3 to 0
- pole_real: float32 [64, 64], P('tp'), may hold values from -1 to 0
- pole_imaginary: float32 [64, 64], P('tp'), may hold values from 1 to 201.06176
- log_step: float32 [64], P('tp'), may hold values from -4.15 to -3
- input_map: float32 [2, 64, 64, 16], P(None, 'tp'), may hold values from -1 to 1
- readout_matrix: float32 [2, 64, 16, 64], P(None, 'tp'), may hold values from -0.5 to 0.5
- skip: float32 [1024], P('tp'), may hold values from -6 to 6
- out_proj: bfloat16 [1024, 2048], P('tp'), may hold values from -0.1875 to 0.1875
- stream: bfloat16 [8192, 2048], P(('sp', 'tp')), may hold values from -6 to 6
- norm_gain: float32 [2048], replicated, may hold values from 0.1 to 1.9
- routes: int32 [8192, 2], P(('sp', 'tp')), may hold values from 0 to 31, all different within a row; in each aligned block of 32 rows (0 to 31, 32 to 63, ...) at most 4 rows name the same one
- route_logits: float32 [8192, 2], P(('sp', 'tp')), may hold values from -7.5 to 7.5
- w_gate: bfloat16 [32, 2048, 7168], P('sp', None, 'tp'), may hold values from -0.125 to 0.125
- w_up: bfloat16 [32, 2048, 7168], P('sp', None, 'tp'), may hold values from -0.125 to 0.125
- w_down: bfloat16 [32, 7168, 2048], P('sp', 'tp'), may hold values from -0.21875 to 0.21875
Outputs:
- layer_out: bfloat16 [8192, 2048], P(('sp', 'tp'))
Inputs may be any that keep to these rules, and one draw needn't show every extreme that they name: `routes`: in the rows of one device no expert is named more than 4 times, a bound that some block reaches; the 2 experts of a token differ.
All inputs are finite; a program needn't handle non-finite values.
Results may differ from a plain program's by a relative error of at most 0.015.
Values may be sent and summed in bfloat16 or wider, within the bound.
No kernel may reach another device: no remote copies, remote signals or barrier semaphores. Data moves between devices by JAX's collectives and lax.ppermute only.
A program may use at most 64 MiB of HBM per device.

v0:
```python
import functools

import jax
import jax.numpy as jnp
from jax import lax
from jax.experimental import pallas as pl
from jax.experimental.pallas import tpu as pltpu
from jax.sharding import PartitionSpec as P


EPS = 1e-06


LANES = 8
EXACT = lax.Precision.HIGHEST


def one_hot(shape, test):
    rows = lax.broadcasted_iota(jnp.int32, shape, 0)
    columns = lax.broadcasted_iota(jnp.int32, shape, 1)
    return jnp.where(test(rows, columns), 1.0, 0.0).astype(jnp.float32)


def exact_dot(left, right, transposed=False):
    contract = ((1,), (1,)) if transposed else ((1,), (0,))
    return lax.dot_general(
        left, right, (contract, ((), ())), precision=EXACT, preferred_element_type=jnp.float32
    )


def complex_times(a_real, a_imag, b_real, b_imag):
    return a_real * b_real - a_imag * b_imag, a_real * b_imag + a_imag * b_real


def states_kernel(
    input_hbm,
    shift_hbm,
    pole_real_hbm,
    pole_imag_hbm,
    log_step_hbm,
    map_hbm,
    total_ref,
    drive_real_ref,
    drive_imag_ref,
    scale_ref,
    factor_ref,
    enter_ref,
    input_ref,
    shift_ref,
    pole_real_ref,
    pole_imag_ref,
    log_step_ref,
    map_ref,
    semaphores,
):
    sources = (pole_real_hbm, pole_imag_hbm, log_step_hbm, shift_hbm, input_hbm, map_hbm)
    targets = (pole_real_ref, pole_imag_ref, log_step_ref, shift_ref, input_ref, map_ref)
    copies = [
        pltpu.make_async_copy(source, target, semaphores.at[number])
        for number, (source, target) in enumerate(zip(sources, targets))
    ]
    for copy in copies:
        copy.start()
    for copy in copies:
        copy.wait()
    rows = input_ref.shape[0]
    groups, states = pole_real_ref.shape
    width = groups * states
    channels = map_ref.shape[1] // groups
    length = rows // LANES
    spread = one_hot((states, width), lambda r, c: c % states == r)
    group_of = one_hot((groups, width), lambda r, c: c // states == r)

    def in_a_row(ref):
        return jnp.sum(exact_dot(ref[...], spread) * group_of, axis=0, keepdims=True)

    pole_real, pole_imag = in_a_row(pole_real_ref), in_a_row(pole_imag_ref)
    logs = jnp.broadcast_to(log_step_ref[...], (groups, groups))
    step = jnp.exp(exact_dot(logs, group_of)[:1])
    magnitude = jnp.exp(pole_real * step)
    factor_real = magnitude * jnp.cos(pole_imag * step)
    factor_imag = magnitude * jnp.sin(pole_imag * step)
    denominator = pole_real * pole_real + pole_imag * pole_imag
    ratio_real = ((factor_real - 1.0) * pole_real + factor_imag * pole_imag) / denominator
    ratio_imag = (factor_imag * pole_real - (factor_real - 1.0) * pole_imag) / denominator
    factor_ref[0:1, :] = factor_real
    factor_ref[1:2, :] = factor_imag

    order = one_hot((rows, rows), lambda r, c: c == (r % LANES) * length + r // LANES)
    inputs = jnp.dot(
        order.astype(jnp.bfloat16), input_ref[...], preferred_element_type=jnp.float32
    )
    scale_ref[...] = exact_dot(exact_dot(order, jnp.exp(shift_ref[...]), True), group_of)
    same_group = one_hot(
        (groups * channels, width), lambda r, c: r // channels == c // states
    )
    plain_real = exact_dot(inputs, exact_dot(map_ref[0], spread) * same_group)
    plain_imag = exact_dot(inputs, exact_dot(map_ref[1], spread) * same_group)
    drive_real, drive_imag = complex_times(ratio_real, ratio_imag, plain_real, plain_imag)
    drive_real_ref[...] = drive_real
    drive_imag_ref[...] = drive_imag

    wide_real = jnp.broadcast_to(factor_real, (LANES, width))
    wide_imag = jnp.broadcast_to(factor_imag, (LANES, width))
    through_real = jnp.ones((LANES, width), jnp.float32)
    through_imag = state_real = state_imag = jnp.zeros((LANES, width), jnp.float32)
    for k in range(length):
        at = slice(k * LANES, (k + 1) * LANES)
        scale = scale_ref[at, :]
        real, imag = scale * wide_real, scale * wide_imag
        through_real, through_imag = complex_times(real, imag, through_real, through_imag)
        state_real, state_imag = complex_times(real, imag, state_real, state_imag)
        state_real = state_real + drive_real_ref[at, :]
        state_imag = state_imag + drive_imag_ref[at, :]

    place = lax.broadcasted_iota(jnp.int32, (LANES, width), 0)

    def moved(value, by, empty):
        return jnp.where(place >= by, pltpu.roll(value, by, 0), empty)

    by = 1
    while by < LANES:
        a_real, a_imag = moved(through_real, by, 1.0), moved(through_imag, by, 0.0)
        x_real, x_imag = moved(state_real, by, 0.0), moved(state_imag, by, 0.0)
        x_real, x_imag = complex_times(through_real, through_imag, x_real, x_imag)
        state_real, state_imag = state_real + x_real, state_imag + x_imag
        through_real, through_imag = complex_times(through_real, through_imag, a_real, a_imag)
        by *= 2
    enter_ref[0] = moved(through_real, 1, 1.0)
    enter_ref[1] = moved(through_imag, 1, 0.0)
    enter_ref[2] = moved(state_real, 1, 0.0)
    enter_ref[3] = moved(state_imag, 1, 0.0)
    total = jnp.concatenate(
        [v[LANES - 1 :] for v in (through_real, through_imag, state_real, state_imag)], axis=0
    )
    total_ref[...] = jnp.broadcast_to(total[None], total_ref.shape)


def response_kernel(
    here_ref,
    arrived_ref,
    drive_real_ref,
    drive_imag_ref,
    scale_ref,
    factor_ref,
    enter_ref,
    input_ref,
    readout_ref,
    skip_ref,
    out_ref,
    state_ref,
):
    rows = input_ref.shape[0]
    width = factor_ref.shape[1]
    states = readout_ref.shape[2]
    channels = readout_ref.shape[1] * states // width
    length = rows // LANES
    here = here_ref[0]
    carry_real = carry_imag = jnp.zeros((1, width), jnp.float32)
    for j in range(arrived_ref.shape[0]):
        block = arrived_ref[j]
        real, imag = complex_times(block[0:1], block[1:2], carry_real, carry_imag)
        earlier = j < here
        carry_real = jnp.where(earlier, real + block[2:3], carry_real)
        carry_imag = jnp.where(earlier, imag + block[3:4], carry_imag)
    state_real, state_imag = complex_times(enter_ref[0], enter_ref[1], carry_real, carry_imag)
    state_real, state_imag = state_real + enter_ref[2], state_imag + enter_ref[3]
    wide_real = jnp.broadcast_to(factor_ref[0:1, :], (LANES, width))
    wide_imag = jnp.broadcast_to(factor_ref[1:2, :], (LANES, width))
    for k in range(length):
        at = slice(k * LANES, (k + 1) * LANES)
        scale = scale_ref[at, :]
        real, imag = scale * wide_real, scale * wide_imag
        state_real, state_imag = complex_times(real, imag, state_real, state_imag)
        state_real = state_real + drive_real_ref[at, :]
        state_imag = state_imag + drive_imag_ref[at, :]
        state_ref[at, :width] = state_real
        state_ref[at, width:] = state_imag
    spread = one_hot((states, width), lambda r, c: c % states == r)
    same_group = one_hot(
        (readout_ref.shape[1], width), lambda r, c: r // channels == c // states
    )
    matrix = jnp.concatenate(
        [
            exact_dot(readout_ref[0], spread) * same_group,
            exact_dot(readout_ref[1], spread) * -same_group,
        ],
        axis=1,
    )
    response = exact_dot(state_ref[...], matrix, True)
    order = one_hot((rows, rows), lambda r, c: r == (c % LANES) * length + c // LANES)
    response = exact_dot(order, response) + skip_ref[...] * input_ref[...].astype(jnp.float32)
    out_ref[...] = jax.nn.gelu(response).astype(jnp.bfloat16)


def local_states(
    mixer_input, decay_shift, pole_real, pole_imaginary, log_step, input_map, devices
):
    rows = mixer_input.shape[0]
    groups, states = pole_real.shape
    width = groups * states
    f32 = jnp.float32
    shape = jax.ShapeDtypeStruct
    operands = (
        mixer_input,
        decay_shift.T,
        pole_real,
        pole_imaginary,
        log_step[None],
        jnp.swapaxes(input_map, 2, 3).reshape(2, -1, states),
    )
    return pl.pallas_call(
        states_kernel,
        out_shape=(
            shape((devices, 4, width), f32),
            shape((rows, width), f32),
            shape((rows, width), f32),
            shape((rows, width), f32),
            shape((2, width), f32),
            shape((4, LANES, width), f32),
        ),
        in_specs=[pl.BlockSpec(memory_space=pltpu.HBM)] * len(operands),
        scratch_shapes=[pltpu.VMEM(operand.shape, operand.dtype) for operand in operands]
        + [pltpu.SemaphoreType.DMA((len(operands),))],
        compiler_params=pltpu.CompilerParams(vmem_limit_bytes=60 * 1024 * 1024),
        name="states",
    )(*operands)


def activations(here, arrived, kept, mixer_input, readout_matrix, skip):
    rows, channels = mixer_input.shape
    width = arrived.shape[2]
    vmem = pl.BlockSpec(memory_space=pltpu.VMEM)
    return pl.pallas_call(
        response_kernel,
        out_shape=jax.ShapeDtypeStruct((rows, channels), jnp.bfloat16),
        in_specs=[pl.BlockSpec(memory_space=pltpu.SMEM)] + [vmem] * 9,
        scratch_shapes=[pltpu.VMEM((rows, 2 * width), jnp.float32)],
        compiler_params=pltpu.CompilerParams(vmem_limit_bytes=60 * 1024 * 1024),
        name="response",
    )(
        here.reshape(1),
        arrived,
        *kept,
        mixer_input,
        readout_matrix.reshape(2, channels, -1),
        skip[None],
    )


def experts_kernel(capacity, count, sets, resumed, finished, *refs):
    row_refs, refs = refs[:count], refs[count:]
    weights, refs = refs[: 3 * sets], refs[3 * sets :]
    before, outs = (refs[:count], refs[count:]) if resumed else ((), refs)
    held, part = row_refs[0].shape[0] // 2, row_refs[0].shape[1]

    def whole_rows(half):
        return one_hot(
            (held, 2 * held),
            lambda r, c: c == r // capacity * (2 * capacity) + r % capacity + half * capacity,
        ).astype(jnp.bfloat16)

    pick = [whole_rows(half) for half in range(2)]
    pieces = [
        jnp.concatenate(
            [jnp.dot(chosen, ref[...], preferred_element_type=jnp.float32) for ref in row_refs],
            axis=0,
        ).astype(jnp.bfloat16)
        for chosen in pick
    ]
    total = jnp.concatenate([ref[...] for ref in before], axis=0) if resumed else None
    for number in range(sets):
        gate_ref, up_ref, down_ref = weights[3 * number : 3 * number + 3]

        def product(ref):
            return sum(
                jnp.dot(
                    piece,
                    ref[half * part : (half + 1) * part, :],
                    preferred_element_type=jnp.float32,
                )
                for half, piece in enumerate(pieces)
            )

        hidden = (jax.nn.silu(product(gate_ref)) * product(up_ref)).astype(jnp.bfloat16)
        out = jnp.dot(hidden, down_ref[...], preferred_element_type=jnp.float32)
        total = out if total is None else total + out
    for number, ref in enumerate(outs):
        rows = total[number * held : (number + 1) * held]
        if finished:
            rows = rows.astype(jnp.bfloat16)
            rows = sum(
                lax.dot_general(
                    pick[half],
                    rows[:, half * part : (half + 1) * part],
                    (((0,), (0,)), ((), ())),
                    preferred_element_type=jnp.float32,
                )
                for half in range(2)
            ).astype(jnp.bfloat16)
        ref[...] = rows


def partial_out(rows, weights, capacity, resumed=(), finished=True):
    count, sets = len(rows), len(weights) // 3
    halves, part = rows[0].shape
    if finished:
        out = jax.ShapeDtypeStruct((halves, part), jnp.bfloat16)
    else:
        out = jax.ShapeDtypeStruct((halves // 2, 2 * part), jnp.float32)
    kernel = functools.partial(
        experts_kernel, capacity, count, sets, bool(resumed), finished
    )
    flops = 2 * count * (halves // 2) * sum(w.size for w in weights)
    return pl.pallas_call(
        kernel,
        out_shape=(out,) * count,
        in_specs=[pl.BlockSpec(memory_space=pltpu.VMEM)]
        * (count + len(weights) + len(resumed)),
        compiler_params=pltpu.CompilerParams(vmem_limit_bytes=20 << 20),
        cost_estimate=pl.CostEstimate(flops=flops, bytes_accessed=0, transcendentals=0),
        name="experts",
    )(*rows, *weights, *resumed)


def slot_numbers(route_rows, experts, capacity):
    flat = route_rows.reshape(route_rows.shape[:-2] + (-1,))
    matches = (flat[..., None] == jnp.arange(experts, dtype=jnp.int32)).astype(jnp.int32)
    earlier = jnp.cumsum(matches, axis=-2) - matches
    return flat * capacity + jnp.sum(earlier * matches, axis=-1)


def half_places(slots, capacity):
    first = slots // capacity * (2 * capacity) + slots % capacity
    return jnp.stack([first, first + capacity])


def chip_shift(distance, flip=0):
    size = lax.axis_size("tp")
    chips = size // 2
    return [
        (2 * chip + core, 2 * ((chip + distance) % chips) + (core ^ flip))
        for chip in range(chips)
        for core in range(2)
    ]


def gathered_projection(out_proj):
    chips = lax.axis_size("tp") // 2
    mine = [out_proj] + [
        lax.ppermute(out_proj, "tp", chip_shift(distance)) for distance in range(1, chips)
    ]
    other = [lax.ppermute(block, "tp", chip_shift(0, 1)) for block in mine]
    return (*mine, *other)


def mix_kernel(order_ref, arrived_ref, stream_ref, gain_ref, places_ref, *refs):
    *blocks, mixed_ref, outgoing_ref = refs
    tokens, model = stream_ref.shape
    projected = sum(
        jnp.dot(arrived_ref[order_ref[number]], block[...], preferred_element_type=jnp.float32)
        for number, block in enumerate(blocks)
    )
    mixed = (stream_ref[...].astype(jnp.float32) + projected).astype(jnp.bfloat16)
    mixed_ref[...] = mixed
    wide = mixed.astype(jnp.float32)
    mean = jnp.mean(wide * wide, axis=-1, keepdims=True)
    normed = (wide * lax.rsqrt(mean + EPS) * gain_ref[...]).astype(jnp.bfloat16)
    halves = jnp.concatenate([normed[:, : model // 2], normed[:, model // 2 :]], axis=0)
    width = outgoing_ref.shape[0]
    at = lax.broadcasted_iota(jnp.int32, (2 * tokens, width), 1)
    hits = sum(
        jnp.where(at == places_ref[:, k : k + 1], 1.0, 0.0) for k in range(places_ref.shape[1])
    ).astype(jnp.bfloat16)
    outgoing_ref[...] = lax.dot_general(
        hits, halves, (((0,), (0,)), ((), ())), preferred_element_type=jnp.float32
    ).astype(jnp.bfloat16)


def mixed_and_outgoing(activated, blocks, stream, norm_gain, places, width):
    size = lax.axis_size("tp")
    chips = size // 2
    here = lax.axis_index("tp")
    chip, core = here // 2, here % 2
    tokens, model = stream.shape
    back = 2 * ((chip - jnp.arange(chips, dtype=jnp.int32)) % chips)
    order = jnp.concatenate([back + core, back + 1 - core])
    arrived = lax.all_to_all(
        activated.reshape(size, tokens, -1), "tp", split_axis=0, concat_axis=0, tiled=True
    )
    vmem = pl.BlockSpec(memory_space=pltpu.VMEM)
    shape = jax.ShapeDtypeStruct
    return pl.pallas_call(
        mix_kernel,
        out_shape=(
            shape((tokens, model), jnp.bfloat16),
            shape((width, model // 2), jnp.bfloat16),
        ),
        in_specs=[pl.BlockSpec(memory_space=pltpu.SMEM)]
        + [vmem] * (4 + size),
        compiler_params=pltpu.CompilerParams(vmem_limit_bytes=12 << 20),
        name="mix",
    )(order, arrived, stream, norm_gain[None], places.reshape(2 * tokens, -1), *blocks)


def expert_over_chips(rows, w_gate, w_up, w_down, capacity):
    own = (w_gate, w_up, w_down)
    rows, *sent = lax.optimization_barrier((rows, *own))
    before = lax.ppermute(rows, "tp", chip_shift(1))
    after = lax.ppermute(rows, "tp", chip_shift(-1))
    other = [lax.ppermute(w, "tp", chip_shift(0, 1)) for w in sent]
    (kept,) = partial_out((rows,), own, capacity, finished=False)
    before, after, kept, late_rows = lax.optimization_barrier((before, after, kept, rows))
    across = lax.ppermute(late_rows, "tp", chip_shift(2))
    near = partial_out((before, after), own, capacity, finished=False)
    for_before, for_after = partial_out((before, after), other, capacity, near)
    (total,) = partial_out((rows,), other, capacity, (kept,))
    (for_across,) = partial_out((across,), (*own, *other), capacity)
    total = total.astype(jnp.float32)
    total = total + lax.ppermute(for_before, "tp", chip_shift(-1)).astype(jnp.float32)
    total = total + lax.ppermute(for_after, "tp", chip_shift(1)).astype(jnp.float32)
    total = lax.optimization_barrier(total)
    total = total + lax.ppermute(for_across, "tp", chip_shift(2)).astype(jnp.float32)
    return total.astype(jnp.bfloat16)


def weighted_pick(places, weights, returned_result):
    width = returned_result.shape[0]
    tokens, top = weights.shape
    hits = places.reshape(2, tokens, top)[..., None] == jnp.arange(width, dtype=jnp.int32)
    spread = jnp.sum(jnp.where(hits, weights[None, :, :, None], 0.0), axis=2)
    spread = spread.reshape(2 * tokens, width)
    high = spread.astype(jnp.bfloat16)
    low = (spread - high.astype(jnp.float32)).astype(jnp.bfloat16)
    picked = jnp.dot(high, returned_result, preferred_element_type=jnp.float32) + jnp.dot(
        low, returned_result, preferred_element_type=jnp.float32
    )
    return jnp.concatenate([picked[:tokens], picked[tokens:]], axis=1)


def shards(
    mixer_input,
    decay_shift,
    pole_real,
    pole_imaginary,
    log_step,
    input_map,
    readout_matrix,
    skip,
    out_proj,
    stream,
    norm_gain,
    routes,
    route_logits,
    w_gate,
    w_up,
    w_down,
):
    totals, *kept = local_states(
        mixer_input,
        decay_shift,
        pole_real,
        pole_imaginary,
        log_step,
        input_map,
        lax.axis_size("sp"),
    )
    ends = lax.all_to_all(totals, "sp", split_axis=0, concat_axis=0, tiled=True)
    blocks = gathered_projection(out_proj)
    activated = activations(
        lax.axis_index("sp"), ends, kept, mixer_input, readout_matrix, skip
    )
    own_rows, model = stream.shape
    weights = jax.nn.sigmoid(
        jnp.stack(
            [route_logits[:, 0] - route_logits[:, 1], route_logits[:, 1] - route_logits[:, 0]],
            axis=1,
        )
    )
    experts = lax.axis_size("sp") * w_gate.shape[0]
    capacity = 4 * own_rows // experts
    width = 2 * experts * capacity
    places = half_places(slot_numbers(routes, experts, capacity), capacity)
    mixed, outgoing = mixed_and_outgoing(
        activated, blocks, stream, norm_gain, places, width
    )
    mixed_wide = mixed.astype(jnp.float32)

    def over_experts(halves):
        blocks = halves.reshape(experts, 2 * capacity, model // 2)
        return lax.all_to_all(blocks, "sp", split_axis=0, concat_axis=0, tiled=True).reshape(
            width, model // 2
        )

    summed = expert_over_chips(over_experts(outgoing), w_gate[0], w_up[0], w_down[0], capacity)
    combined = mixed_wide + weighted_pick(places, weights, over_experts(summed))
    return combined.astype(jnp.bfloat16)


def solution(mesh):
    return jax.shard_map(
        shards,
        mesh=mesh,
        in_specs=(
            P("sp", "tp"),
            P("sp", "tp"),
            P("tp", None),
            P("tp", None),
            P("tp"),
            P(None, "tp", None, None),
            P(None, "tp", None, None),
            P("tp"),
            P("tp", None),
            P(("sp", "tp"), None),
            P(),
            P(("sp", "tp"), None),
            P(("sp", "tp"), None),
            P("sp", None, "tp"),
            P("sp", None, "tp"),
            P("sp", "tp", None),
        ),
        out_specs=P(("sp", "tp"), None),
        check_vma=False,
    )
```

profile of v0, /device:TPU:32, one launch (start us, length us, event | category | flops | bytes accessed | tf_op | source)
XLA Modules:
  0.0 151.9 jit_solution(14005145640202342787)
XLA Ops:
  0.0 1.6 %collective-permute-start = (bf16[128,2048]{1,0:T(8,128)(2,1)}, bf16[128,2048]{1,0:T(8,128)(2,1)S(1)}, u32[]{:S(2)}, u32[]{:S(2)}) collective-permute-start(bf16[128,2048]{1,0:T(8,128)(2,1)} %refs_0_.1), channel_id=1, source_target_pairs={{0,2},{1,3},{2,4},{3,5},{4,6},{5,7},{6,0},{7,1},{8,10},{9,11},{10,... | collective-permute-start | bytes 1572872 | tf_op jit(solution)/shard_map/ppermute | solution.py:351
  1.6 2.9 %collective-permute-start.1 = (bf16[128,2048]{1,0:T(8,128)(2,1)}, bf16[128,2048]{1,0:T(8,128)(2,1)S(1)}, u32[]{:S(2)}, u32[]{:S(2)}) collective-permute-start(bf16[128,2048]{1,0:T(8,128)(2,1)} %refs_0_.1), channel_id=1, source_target_pairs={{0,4},{1,5},{2,6},{3,7},{4,0},{5,1},{6,2},{7,3},{8,12},{9,13},{10,... | collective-permute-start | bytes 1572872 | tf_op jit(solution)/shard_map/ppermute | solution.py:351
  4.5 1.3 collective-permute-start.2
  5.8 5.0 %states.1 = (f32[32,4,512]{2,1,0:T(4,128)}, f32[256,512]{1,0:T(8,128)}, f32[256,512]{1,0:T(8,128)}, f32[256,512]{1,0:T(8,128)}, f32[2,512]{1,0:T(2,128)}, /*index=5*/f32[4,8,512]{2,1,0:T(8,128)}) custom-call(bf16[256,128]{1,0:T(8,128)(2,1)} %input_ref.1, f32[8,256]{1,0:T(8,128)} %bitcast.59, f32[8,64]{1,0:T(8,128)} %pole_real_hbm.1, f32[8,64]{1,0:T(8,128)} %pole_imag_hbm.1, ...), custom_call_target="tpu_custom_call" | custom-call | tf_op jit(solution)/shard_map/states/pallas_call | solution.py:212
  10.8 11.2 %all-to-all-start = ((f32[32,4,512]{2,1,0:T(4,128)}), f32[32,4,512]{2,1,0:T(4,128)S(1)}, u32[]{:S(2)}, u32[]{:S(2)}) async-start(f32[32,4,512]{2,1,0:T(4,128)} %get-tuple-element.25), calls=%async_computation | async-start | bytes 524288 | tf_op jit(solution)/shard_map/all_to_all | solution.py:468
  23.6 3.9 %collective-permute-done.1.refs_2_ = bf16[128,2048]{1,0:T(8,128)(2,1)S(1)} collective-permute-done((bf16[128,2048]{1,0:T(8,128)(2,1)}, bf16[128,2048]{1,0:T(8,128)(2,1)S(1)}, u32[]{:S(2)}, u32[]{:S(2)}) %collective-permute-start.1) | collective-permute-done | bytes 524320 | tf_op jit(solution)/shard_map/ppermute | solution.py:351
  28.2 6.6 %all-to-all-done.arrived_ref = f32[32,4,512]{2,1,0:T(4,128)S(1)} async-done(((f32[32,4,512]{2,1,0:T(4,128)}), f32[32,4,512]{2,1,0:T(4,128)S(1)}, u32[]{:S(2)}, u32[]{:S(2)}) %all-to-all-start) | async-done | bytes 262176 | tf_op jit(solution)/shard_map/all_to_all | solution.py:468
  35.5 4.5 %response.1 = bf16[256,128]{1,0:T(8,128)(2,1)} custom-call(s32[1]{0:T(128)} %bitcast.here_ref, f32[32,4,512]{2,1,0:T(4,128)} %copy-done.8, f32[256,512]{1,0:T(8,128)} %get-tuple-element.26.drive_real_ref, f32[256,512]{1,0:T(8,128)} %get-tuple-element.27.drive_imag_ref, f32[256,512]{1,0:T(8,128)} %get-tuple-element.28.scale_ref, ...), custom_call_target="tpu_custom_call" | custom-call | tf_op jit(solution)/shard_map/response/pallas_call | solution.py:234
  40.0 3.3 %all-to-all-start.1 = ((bf16[8,32,128]{2,1,0:T(8,128)(2,1)}), bf16[8,32,128]{2,1,0:T(8,128)(2,1)S(1)}, u32[]{:S(2)}, u32[]{:S(2)}) async-start(bf16[8,32,128]{2,1,0:T(8,128)(2,1)} %bitcast.54), calls=%async_computation.1 | async-start | bytes 131072 | tf_op jit(solution)/shard_map/all_to_all | solution.py:388
  43.4 5.5 %all-to-all-done.1.arrived_ref = bf16[8,32,128]{2,1,0:T(8,128)(2,1)S(1)} async-done(((bf16[8,32,128]{2,1,0:T(8,128)(2,1)}), bf16[8,32,128]{2,1,0:T(8,128)(2,1)S(1)}, u32[]{:S(2)}, u32[]{:S(2)}) %all-to-all-start.1) | async-done | bytes 65568 | tf_op jit(solution)/shard_map/all_to_all | solution.py:388
  48.9 1.0 copy-done.6
  50.8 2.3 %mix.1 = (bf16[32,2048]{1,0:T(8,128)(2,1)S(1)}, bf16[256,1024]{1,0:T(8,128)(2,1)S(1)}) custom-call(s32[8]{0:T(128)S(1)} %pad_add_fusion.1.order_ref, bf16[8,32,128]{2,1,0:T(8,128)(2,1)S(1)} %all-to-all-done.1.arrived_ref, bf16[32,2048]{1,0:T(8,128)(2,1)S(1)} %copy-done.6, f32[1,2048]{1,0:T(1,128)S(1)} %bitcast.53, s32[64,2]{1,0:T(8,128)S(1)} %reshape.204.places_ref, ...), custom_call_target="tpu_custom_call" | custom-call | tf_op jit(solution)/shard_map/mix/pallas_call | solution.py:393
  53.0 21.7 %all_to_all.20 = bf16[32,8,1024]{2,1,0:T(8,128)(2,1)S(1)} all-to-all(bf16[32,8,1024]{2,1,0:T(8,128)(2,1)S(1)} %bitcast.52), channel_id=1, replica_groups=mesh['sp'=32,'tp'=8] {'sp'}, dimensions={0} | all-to-all | bytes 1048576 | tf_op jit(solution)/shard_map/all_to_all | solution.py:491
  75.8 2.7 %collective-permute-start.11 = (bf16[256,1024]{1,0:T(8,128)(2,1)S(1)}, bf16[256,1024]{1,0:T(8,128)(2,1)S(1)}, u32[]{:S(2)}, u32[]{:S(2)}) collective-permute-start(bf16[256,1024]{1,0:T(8,128)(2,1)S(1)} %bitcast.48), channel_id=1, source_target_pairs={{0,6},{1,7},{2,0},{3,1},{4,2},{5,3},{6,4},{7,5},{8,14},{9,15},{10,... | collective-permute-start | bytes 1572872 | tf_op jit(solution)/shard_map/ppermute | solution.py:410
  78.5 2.0 %copy-done.1 = bf16[1,2048,896]{2,1,0:T(8,128)(2,1)S(1)} copy-done((bf16[1,2048,896]{2,1,0:T(8,128)(2,1)S(1)}, bf16[1,2048,896]{2,1,0:T(8,128)(2,1)}, u32[]{:S(2)}) %copy-start.1) | copy-done | bytes 3670040
  80.5 2.0 %copy-done.3 = bf16[1,896,2048]{2,1,0:T(8,128)(2,1)S(1)} copy-done((bf16[1,896,2048]{2,1,0:T(8,128)(2,1)S(1)}, bf16[1,896,2048]{2,1,0:T(8,128)(2,1)}, u32[]{:S(2)}) %copy-start.3) | copy-done | bytes 3670040
  82.6 2.1 %experts.5.refs_4_ = f32[128,2048]{1,0:T(8,128)S(1)} custom-call(bf16[256,1024]{1,0:T(8,128)(2,1)S(1)} %bitcast.49, bf16[2048,896]{1,0:T(8,128)(2,1)S(1)} %bitcast.36, bf16[2048,896]{1,0:T(8,128)(2,1)S(1)} %bitcast.40, bf16[896,2048]{1,0:T(8,128)(2,1)S(1)} %bitcast.44), custom_call_target="tpu_custom_call" | custom-call | flops 1409286144 | tf_op jit(solution)/shard_map/experts/pallas_call | solution.py:315
  84.6 6.2 %collective-permute-done.10.refs_0_ = bf16[256,1024]{1,0:T(8,128)(2,1)S(1)} collective-permute-done((bf16[256,1024]{1,0:T(8,128)(2,1)S(1)}, bf16[256,1024]{1,0:T(8,128)(2,1)S(1)}, u32[]{:S(2)}, u32[]{:S(2)}) %collective-permute-start.10) | collective-permute-done | bytes 524320 | tf_op jit(solution)/shard_map/ppermute | solution.py:409
  90.8 1.5 collective-permute-start.14
  92.2 3.7 %experts.7 = (f32[128,2048]{1,0:T(8,128)S(1)}, f32[128,2048]{1,0:T(8,128)S(1)}) custom-call(bf16[256,1024]{1,0:T(8,128)(2,1)S(1)} %collective-permute-done.10.refs_0_, bf16[256,1024]{1,0:T(8,128)(2,1)S(1)} %collective-permute-done.11.refs_1_, bf16[2048,896]{1,0:T(8,128)(2,1)S(1)} %bitcast.37, bf16[2048,896]{1,0:T(8,128)(2,1)S(1)} %bitcast.41, ...), custom_call_target="tpu_custom_call" | custom-call | flops 2818572288 | tf_op jit(solution)/shard_map/experts/pallas_call | solution.py:315
  96.0 4.3 %experts.8 = (bf16[256,1024]{1,0:T(8,128)(2,1)S(1)}, bf16[256,1024]{1,0:T(8,128)(2,1)S(1)}) custom-call(bf16[256,1024]{1,0:T(8,128)(2,1)S(1)} %collective-permute-done.10.refs_0_, bf16[256,1024]{1,0:T(8,128)(2,1)S(1)} %collective-permute-done.11.refs_1_, bf16[2048,896]{1,0:T(8,128)(2,1)S(1)} %collective-permute-done.7.refs_1_.refs_2_.refs_4_, ...), custom_call_target="tpu_custom_call" | custom-call | flops 2818572288 | tf_op jit(solution)/shard_map/experts/pallas_call | solution.py:315
  100.4 1.6 %collective-permute-start.12 = (bf16[256,1024]{1,0:T(8,128)(2,1)S(1)}, bf16[256,1024]{1,0:T(8,128)(2,1)S(1)}, u32[]{:S(2)}, u32[]{:S(2)}) collective-permute-start(bf16[256,1024]{1,0:T(8,128)(2,1)S(1)} %get-tuple-element.42), channel_id=1, source_target_pairs={{0,6},{1,7},{2,0},{3,1},{4,2},{5,3},{6,4},{7,5},{8,14},{9,15},{10,... | collective-permute-start | bytes 1572872 | tf_op jit(solution)/shard_map/ppermute | solution.py:420
  102.0 1.2 collective-permute-start.13
  103.1 3.9 %collective-permute-done.14.refs_0_ = bf16[256,1024]{1,0:T(8,128)(2,1)S(1)} collective-permute-done((bf16[256,1024]{1,0:T(8,128)(2,1)S(1)}, bf16[256,1024]{1,0:T(8,128)(2,1)S(1)}, u32[]{:S(2)}, u32[]{:S(2)}) %collective-permute-start.14) | collective-permute-done | bytes 524320 | tf_op jit(solution)/shard_map/ppermute | solution.py:414
  107.0 4.1 %experts.9 = bf16[256,1024]{1,0:T(8,128)(2,1)S(1)} custom-call(bf16[256,1024]{1,0:T(8,128)(2,1)S(1)} %collective-permute-done.14.refs_0_, bf16[2048,896]{1,0:T(8,128)(2,1)S(1)} %bitcast.38, bf16[2048,896]{1,0:T(8,128)(2,1)S(1)} %bitcast.42, bf16[896,2048]{1,0:T(8,128)(2,1)S(1)} %bitcast.46, ...), custom_call_target="tpu_custom_call" | custom-call | flops 2818572288 | tf_op jit(solution)/shard_map/experts/pallas_call | solution.py:315
  111.1 1.2 collective-permute-start.15
  112.3 2.4 %experts.6 = bf16[256,1024]{1,0:T(8,128)(2,1)S(1)} custom-call(bf16[256,1024]{1,0:T(8,128)(2,1)S(1)} %bitcast.51, bf16[2048,896]{1,0:T(8,128)(2,1)S(1)} %collective-permute-done.7.refs_1_.refs_2_.refs_4_, bf16[2048,896]{1,0:T(8,128)(2,1)S(1)} %collective-permute-done.8.refs_2_.refs_3_.refs_5_, ...), custom_call_target="tpu_custom_call" | custom-call | flops 1409286144 | tf_op jit(solution)/shard_map/experts/pallas_call | solution.py:315
  114.7 3.9 %collective-permute-done.12 = bf16[256,1024]{1,0:T(8,128)(2,1)S(1)} collective-permute-done((bf16[256,1024]{1,0:T(8,128)(2,1)S(1)}, bf16[256,1024]{1,0:T(8,128)(2,1)S(1)}, u32[]{:S(2)}, u32[]{:S(2)}) %collective-permute-start.12) | collective-permute-done | bytes 524320 | tf_op jit(solution)/shard_map/ppermute | solution.py:420
  118.6 9.8 %collective-permute-done.13 = bf16[256,1024]{1,0:T(8,128)(2,1)S(1)} collective-permute-done((bf16[256,1024]{1,0:T(8,128)(2,1)S(1)}, bf16[256,1024]{1,0:T(8,128)(2,1)S(1)}, u32[]{:S(2)}, u32[]{:S(2)}) %collective-permute-start.13) | collective-permute-done | bytes 524320 | tf_op jit(solution)/shard_map/ppermute | solution.py:421
  128.7 0.9 fusion
  129.6 5.2 %all-to-all-start.3 = ((bf16[32,8,1024]{2,1,0:T(8,128)(2,1)}), bf16[32,8,1024]{2,1,0:T(8,128)(2,1)S(1)}, u32[]{:S(2)}, u32[]{:S(2)}) async-start(bf16[32,8,1024]{2,1,0:T(8,128)(2,1)} %fusion), calls=%async_computation.3 | async-start | bytes 1048576 | tf_op jit(solution)/shard_map/all_to_all | solution.py:491
  135.1 15.6 %all-to-all-done.3 = bf16[32,8,1024]{2,1,0:T(8,128)(2,1)S(1)} async-done(((bf16[32,8,1024]{2,1,0:T(8,128)(2,1)}), bf16[32,8,1024]{2,1,0:T(8,128)(2,1)S(1)}, u32[]{:S(2)}, u32[]{:S(2)}) %all-to-all-start.3) | async-done | bytes 524320 | tf_op jit(solution)/shard_map/all_to_all | solution.py:491
  (61 shorter events, 6.5 us)
Async XLA Ops:
  0.0 48.9 %copy-start.5 = (bf16[128,2048]{1,0:T(8,128)(2,1)S(1)}, bf16[128,2048]{1,0:T(8,128)(2,1)}, u32[]{:S(2)}) copy-start(bf16[128,2048]{1,0:T(8,128)(2,1)} %refs_0_.1) | copy-start | bytes 1572868
  0.0 23.5 %collective-permute-start = (bf16[128,2048]{1,0:T(8,128)(2,1)}, bf16[128,2048]{1,0:T(8,128)(2,1)S(1)}, u32[]{:S(2)}, u32[]{:S(2)}) collective-permute-start(bf16[128,2048]{1,0:T(8,128)(2,1)} %refs_0_.1), channel_id=1, source_target_pairs={{0,2},{1,3},{2,4},{3,5},{4,6},{5,7},{6,0},{7,1},{8,10},{9,11},{10,... | collective-permute-start | bytes 1572872 | tf_op jit(solution)/shard_map/ppermute | solution.py:351
  1.6 26.0 %collective-permute-start.1 = (bf16[128,2048]{1,0:T(8,128)(2,1)}, bf16[128,2048]{1,0:T(8,128)(2,1)S(1)}, u32[]{:S(2)}, u32[]{:S(2)}) collective-permute-start(bf16[128,2048]{1,0:T(8,128)(2,1)} %refs_0_.1), channel_id=1, source_target_pairs={{0,4},{1,5},{2,6},{3,7},{4,0},{5,1},{6,2},{7,3},{8,12},{9,13},{10,... | collective-permute-start | bytes 1572872 | tf_op jit(solution)/shard_map/ppermute | solution.py:351
  4.5 23.1 %collective-permute-start.2 = (bf16[128,2048]{1,0:T(8,128)(2,1)}, bf16[128,2048]{1,0:T(8,128)(2,1)S(1)}, u32[]{:S(2)}, u32[]{:S(2)}) collective-permute-start(bf16[128,2048]{1,0:T(8,128)(2,1)} %refs_0_.1), channel_id=1, source_target_pairs={{0,6},{1,7},{2,0},{3,1},{4,2},{5,3},{6,4},{7,5},{8,14},{9,15},{10,... | collective-permute-start | bytes 1572872 | tf_op jit(solution)/shard_map/ppermute | solution.py:351
  5.8 37.6 %collective-permute-start.3 = (bf16[128,2048]{1,0:T(8,128)(2,1)}, bf16[128,2048]{1,0:T(8,128)(2,1)S(1)}, u32[]{:S(2)}, u32[]{:S(2)}) collective-permute-start(bf16[128,2048]{1,0:T(8,128)(2,1)} %refs_0_.1), channel_id=1, source_target_pairs={{0,1},{1,0},{2,3},{3,2},{4,5},{5,4},{6,7},{7,6},{8,9},{9,8},{10,11... | collective-permute-start | bytes 1572872 | tf_op jit(solution)/shard_map/ppermute | solution.py:353
  10.8 24.0 %all-to-all-start = ((f32[32,4,512]{2,1,0:T(4,128)}), f32[32,4,512]{2,1,0:T(4,128)S(1)}, u32[]{:S(2)}, u32[]{:S(2)}) async-start(f32[32,4,512]{2,1,0:T(4,128)} %get-tuple-element.25), calls=%async_computation | async-start | bytes 524288 | tf_op jit(solution)/shard_map/all_to_all | solution.py:468
  23.5 25.4 %collective-permute-start.4 = (bf16[128,2048]{1,0:T(8,128)(2,1)S(1)}, bf16[128,2048]{1,0:T(8,128)(2,1)S(1)}, u32[]{:S(2)}, u32[]{:S(2)}) collective-permute-start(bf16[128,2048]{1,0:T(8,128)(2,1)S(1)} %collective-permute-done.refs_1_), channel_id=1, source_target_pairs={{0,1},{1,0},{2,3},{3,2},{4,5},{5,4},{6,7},{7,6},{8,9},{9,8},{10,11... | collective-permute-start | bytes 1572872 | tf_op jit(solution)/shard_map/ppermute | solution.py:353
  27.6 21.3 %collective-permute-start.5 = (bf16[128,2048]{1,0:T(8,128)(2,1)S(1)}, bf16[128,2048]{1,0:T(8,128)(2,1)}, u32[]{:S(2)}, u32[]{:S(2)}) collective-permute-start(bf16[128,2048]{1,0:T(8,128)(2,1)S(1)} %collective-permute-done.1.refs_2_), channel_id=1, source_target_pairs={{0,1},{1,0},{2,3},{3,2},{4,5},{5,4},{6,7},{7,6},{8,9},{9,8},{10,11... | collective-permute-start | bytes 1572872 | tf_op jit(solution)/shard_map/ppermute | solution.py:353
  27.6 21.3 %collective-permute-start.6 = (bf16[128,2048]{1,0:T(8,128)(2,1)S(1)}, bf16[128,2048]{1,0:T(8,128)(2,1)}, u32[]{:S(2)}, u32[]{:S(2)}) collective-permute-start(bf16[128,2048]{1,0:T(8,128)(2,1)S(1)} %collective-permute-done.2.refs_3_), channel_id=1, source_target_pairs={{0,1},{1,0},{2,3},{3,2},{4,5},{5,4},{6,7},{7,6},{8,9},{9,8},{10,11... | collective-permute-start | bytes 1572872 | tf_op jit(solution)/shard_map/ppermute | solution.py:353
  34.8 0.7 copy-start.8
  40.0 8.9 %all-to-all-start.1 = ((bf16[8,32,128]{2,1,0:T(8,128)(2,1)}), bf16[8,32,128]{2,1,0:T(8,128)(2,1)S(1)}, u32[]{:S(2)}, u32[]{:S(2)}) async-start(bf16[8,32,128]{2,1,0:T(8,128)(2,1)} %bitcast.54), calls=%async_computation.1 | async-start | bytes 131072 | tf_op jit(solution)/shard_map/all_to_all | solution.py:388
  48.9 25.8 %copy-start = (bf16[1,2048,896]{2,1,0:T(8,128)(2,1)S(1)}, bf16[1,2048,896]{2,1,0:T(8,128)(2,1)}, u32[]{:S(2)}) copy-start(bf16[1,2048,896]{2,1,0:T(8,128)(2,1)} %param.29) | copy-start | bytes 11010052
  48.9 1.1 copy-start.6
  50.0 0.8 copy-start.7
  74.7 21.3 %collective-permute-start.7 = (bf16[2048,896]{1,0:T(8,128)(2,1)S(1)}, bf16[2048,896]{1,0:T(8,128)(2,1)S(1)}, u32[]{:S(2)}, u32[]{:S(2)}) collective-permute-start(bf16[2048,896]{1,0:T(8,128)(2,1)S(1)} %bitcast.35), channel_id=1, source_target_pairs={{0,1},{1,0},{2,3},{3,2},{4,5},{5,4},{6,7},{7,6},{8,9},{9,8},{10,11... | collective-permute-start | bytes 11010056 | tf_op jit(solution)/shard_map/ppermute | solution.py:411
  74.7 21.3 %collective-permute-start.8 = (bf16[2048,896]{1,0:T(8,128)(2,1)}, bf16[2048,896]{1,0:T(8,128)(2,1)S(1)}, u32[]{:S(2)}, u32[]{:S(2)}) collective-permute-start(bf16[2048,896]{1,0:T(8,128)(2,1)} %bitcast.39), channel_id=1, source_target_pairs={{0,1},{1,0},{2,3},{3,2},{4,5},{5,4},{6,7},{7,6},{8,9},{9,8},{10,11... | collective-permute-start | bytes 11010056 | tf_op jit(solution)/shard_map/ppermute | solution.py:411
  75.2 20.8 %collective-permute-start.9 = (bf16[896,2048]{1,0:T(8,128)(2,1)}, bf16[896,2048]{1,0:T(8,128)(2,1)S(1)}, u32[]{:S(2)}, u32[]{:S(2)}) collective-permute-start(bf16[896,2048]{1,0:T(8,128)(2,1)} %bitcast.43), channel_id=1, source_target_pairs={{0,1},{1,0},{2,3},{3,2},{4,5},{5,4},{6,7},{7,6},{8,9},{9,8},{10,11... | collective-permute-start | bytes 11010056 | tf_op jit(solution)/shard_map/ppermute | solution.py:411
  75.2 15.5 %collective-permute-start.10 = (bf16[256,1024]{1,0:T(8,128)(2,1)S(1)}, bf16[256,1024]{1,0:T(8,128)(2,1)S(1)}, u32[]{:S(2)}, u32[]{:S(2)}) collective-permute-start(bf16[256,1024]{1,0:T(8,128)(2,1)S(1)} %bitcast.47), channel_id=1, source_target_pairs={{0,2},{1,3},{2,4},{3,5},{4,6},{5,7},{6,0},{7,1},{8,10},{9,11},{10,... | collective-permute-start | bytes 1572872 | tf_op jit(solution)/shard_map/ppermute | solution.py:409
  75.8 15.0 %collective-permute-start.11 = (bf16[256,1024]{1,0:T(8,128)(2,1)S(1)}, bf16[256,1024]{1,0:T(8,128)(2,1)S(1)}, u32[]{:S(2)}, u32[]{:S(2)}) collective-permute-start(bf16[256,1024]{1,0:T(8,128)(2,1)S(1)} %bitcast.48), channel_id=1, source_target_pairs={{0,6},{1,7},{2,0},{3,1},{4,2},{5,3},{6,4},{7,5},{8,14},{9,15},{10,... | collective-permute-start | bytes 1572872 | tf_op jit(solution)/shard_map/ppermute | solution.py:410
  78.5 2.0 %copy-start.1 = (bf16[1,2048,896]{2,1,0:T(8,128)(2,1)S(1)}, bf16[1,2048,896]{2,1,0:T(8,128)(2,1)}, u32[]{:S(2)}) copy-start(bf16[1,2048,896]{2,1,0:T(8,128)(2,1)} %param.30) | copy-start | bytes 11010052
  80.5 2.0 %copy-start.3 = (bf16[1,896,2048]{2,1,0:T(8,128)(2,1)S(1)}, bf16[1,896,2048]{2,1,0:T(8,128)(2,1)}, u32[]{:S(2)}) copy-start(bf16[1,896,2048]{2,1,0:T(8,128)(2,1)} %param.31) | copy-start | bytes 11010052
  82.5 9.7 %copy-start.2 = (bf16[1,2048,896]{2,1,0:T(8,128)(2,1)S(1)}, bf16[1,2048,896]{2,1,0:T(8,128)(2,1)}, u32[]{:S(2)}) copy-start(bf16[1,2048,896]{2,1,0:T(8,128)(2,1)} %param.30) | copy-start | bytes 11010052
  90.8 16.2 %collective-permute-start.14 = (bf16[256,1024]{1,0:T(8,128)(2,1)S(1)}, bf16[256,1024]{1,0:T(8,128)(2,1)S(1)}, u32[]{:S(2)}, u32[]{:S(2)}) collective-permute-start(bf16[256,1024]{1,0:T(8,128)(2,1)S(1)} %bitcast.50), channel_id=1, source_target_pairs={{0,4},{1,5},{2,6},{3,7},{4,0},{5,1},{6,2},{7,3},{8,12},{9,13},{10,... | collective-permute-start | bytes 1572872 | tf_op jit(solution)/shard_map/ppermute | solution.py:414
  96.0 11.0 %copy-start.4 = (bf16[1,896,2048]{2,1,0:T(8,128)(2,1)S(1)}, bf16[1,896,2048]{2,1,0:T(8,128)(2,1)}, u32[]{:S(2)}) copy-start(bf16[1,896,2048]{2,1,0:T(8,128)(2,1)} %param.31) | copy-start | bytes 11010052
  100.4 18.2 %collective-permute-start.12 = (bf16[256,1024]{1,0:T(8,128)(2,1)S(1)}, bf16[256,1024]{1,0:T(8,128)(2,1)S(1)}, u32[]{:S(2)}, u32[]{:S(2)}) collective-permute-start(bf16[256,1024]{1,0:T(8,128)(2,1)S(1)} %get-tuple-element.42), channel_id=1, source_target_pairs={{0,6},{1,7},{2,0},{3,1},{4,2},{5,3},{6,4},{7,5},{8,14},{9,15},{10,... | collective-permute-start | bytes 1572872 | tf_op jit(solution)/shard_map/ppermute | solution.py:420
  102.0 26.4 %collective-permute-start.13 = (bf16[256,1024]{1,0:T(8,128)(2,1)S(1)}, bf16[256,1024]{1,0:T(8,128)(2,1)S(1)}, u32[]{:S(2)}, u32[]{:S(2)}) collective-permute-start(bf16[256,1024]{1,0:T(8,128)(2,1)S(1)} %get-tuple-element.43), channel_id=1, source_target_pairs={{0,2},{1,3},{2,4},{3,5},{4,6},{5,7},{6,0},{7,1},{8,10},{9,11},{10,... | collective-permute-start | bytes 1572872 | tf_op jit(solution)/shard_map/ppermute | solution.py:421
  111.1 17.6 %collective-permute-start.15 = (bf16[256,1024]{1,0:T(8,128)(2,1)S(1)}, bf16[256,1024]{1,0:T(8,128)(2,1)S(1)}, u32[]{:S(2)}, u32[]{:S(2)}) collective-permute-start(bf16[256,1024]{1,0:T(8,128)(2,1)S(1)} %experts.9), channel_id=1, source_target_pairs={{0,4},{1,5},{2,6},{3,7},{4,0},{5,1},{6,2},{7,3},{8,12},{9,13},{10,... | collective-permute-start | bytes 1572872 | tf_op jit(solution)/shard_map/ppermute | solution.py:423
  114.7 20.2 %copy-start.9 = (f32[32,2]{0,1:T(2,128)S(1)}, f32[32,2]{0,1:T(2,128)}, u32[]{:S(2)}) copy-start(f32[32,2]{0,1:T(2,128)} %param.28) | copy-start | bytes 772
  129.6 21.2 %all-to-all-start.3 = ((bf16[32,8,1024]{2,1,0:T(8,128)(2,1)}), bf16[32,8,1024]{2,1,0:T(8,128)(2,1)S(1)}, u32[]{:S(2)}, u32[]{:S(2)}) async-start(bf16[32,8,1024]{2,1,0:T(8,128)(2,1)} %fusion), calls=%async_computation.3 | async-start | bytes 1048576 | tf_op jit(solution)/shard_map/all_to_all | solution.py:491
where the time goes:
time: 152 us
  waiting for transfers between devices  55.3 us (36%)
  starting transfers between devices  35.4 us (23%)
  Pallas kernels  28.3 us (19%)
  blocking collectives  21.7 us (14%)
  local copies, waits for them, and re-layouts  7.97 us (5%)
  other arithmetic  2.5 us (2%)
    all_to_all x1, blocking collectives, over_experts(): lax.all_to_all(blocks, 'sp', split_axis=0, concat_axis=0, tiled=True)  21.7 us
    pallas_call x5, Pallas kernels, partial_out(): pl.pallas_call(kernel, out_shape=(out,) * count, in_specs=[pl.BlockSpec(m...  16.6 us
    all_to_all x1, waiting for transfers between devices, over_experts(): lax.all_to_all(blocks, 'sp', split_axis=0, concat_axis=0, tiled=True)  15.6 us
    all_to_all x1, starting transfers between devices, shards(): ends = lax.all_to_all(totals, 'sp', split_axis=0, concat_axis=0, tiled=True)  11.2 us
    ppermute x1, waiting for transfers between devices, expert_over_chips(): lax.ppermute(for_after, 'tp', chip_shift(1)).astype(jnp.float32)  9.77 us
    unnamed x21, local copies, waits for them, and re-layouts  7.38 us
    all_to_all x1, waiting for transfers between devices, shards(): ends = lax.all_to_all(totals, 'sp', split_axis=0, concat_axis=0, tiled=True)  6.57 us
    ppermute x1, waiting for transfers between devices, expert_over_chips(): before = lax.ppermute(rows, 'tp', chip_shift(1))  6.15 us
  transfers between devices with their start and end apart: 19, of which 8 were waited for; matrix products, arithmetic and copies ran while one was open for 1% of the time, Pallas kernels for 17%

commit v1 on v0

--- a/solution.py
+++ b/solution.py
@@ -136,20 +136,31 @@
     total_ref[...] = jnp.broadcast_to(total[None], total_ref.shape)
 
 
-def response_kernel(
-    here_ref,
-    arrived_ref,
-    drive_real_ref,
-    drive_imag_ref,
-    scale_ref,
-    factor_ref,
-    enter_ref,
-    input_ref,
-    readout_ref,
-    skip_ref,
-    out_ref,
-    state_ref,
-):
+def response_kernel(here_ref, *refs):
+    sources, (out_ref, state_ref), targets, semaphores = (
+        refs[:9],
+        refs[9:11],
+        refs[11:20],
+        refs[20],
+    )
+    copies = [
+        pltpu.make_async_copy(source, target, semaphores.at[number])
+        for number, (source, target) in enumerate(zip(sources, targets))
+    ]
+    for copy in copies:
+        copy.start()
+    (
+        arrived_ref,
+        drive_real_ref,
+        drive_imag_ref,
+        scale_ref,
+        factor_ref,
+        enter_ref,
+        input_ref,
+        readout_ref,
+        skip_ref,
+    ) = targets
+    copies[0].wait()
     rows = input_ref.shape[0]
     width = factor_ref.shape[1]
     states = readout_ref.shape[2]
@@ -163,6 +174,8 @@
         earlier = j < here
         carry_real = jnp.where(earlier, real + block[2:3], carry_real)
         carry_imag = jnp.where(earlier, imag + block[3:4], carry_imag)
+    for copy in copies[1:]:
+        copy.wait()
     state_real, state_imag = complex_times(enter_ref[0], enter_ref[1], carry_real, carry_imag)
     state_real, state_imag = state_real + enter_ref[2], state_imag + enter_ref[3]
     wide_real = jnp.broadcast_to(factor_ref[0:1, :], (LANES, width))
@@ -230,22 +243,24 @@
 def activations(here, arrived, kept, mixer_input, readout_matrix, skip):
     rows, channels = mixer_input.shape
     width = arrived.shape[2]
-    vmem = pl.BlockSpec(memory_space=pltpu.VMEM)
-    return pl.pallas_call(
-        response_kernel,
-        out_shape=jax.ShapeDtypeStruct((rows, channels), jnp.bfloat16),
-        in_specs=[pl.BlockSpec(memory_space=pltpu.SMEM)] + [vmem] * 9,
-        scratch_shapes=[pltpu.VMEM((rows, 2 * width), jnp.float32)],
-        compiler_params=pltpu.CompilerParams(vmem_limit_bytes=60 * 1024 * 1024),
-        name="response",
-    )(
-        here.reshape(1),
+    operands = (
         arrived,
         *kept,
         mixer_input,
         readout_matrix.reshape(2, channels, -1),
         skip[None],
     )
+    return pl.pallas_call(
+        response_kernel,
+        out_shape=jax.ShapeDtypeStruct((rows, channels), jnp.bfloat16),
+        in_specs=[pl.BlockSpec(memory_space=pltpu.SMEM)]
+        + [pl.BlockSpec(memory_space=pltpu.HBM)] * len(operands),
+        scratch_shapes=[pltpu.VMEM((rows, 2 * width), jnp.float32)]
+        + [pltpu.VMEM(operand.shape, operand.dtype) for operand in operands]
+        + [pltpu.SemaphoreType.DMA((len(operands),))],
+        compiler_params=pltpu.CompilerParams(vmem_limit_bytes=60 * 1024 * 1024),
+        name="response",
+    )(here.reshape(1), *operands)
 
 
 def experts_kernel(capacity, count, sets, resumed, finished, *refs):
@@ -317,7 +332,7 @@
         out_shape=(out,) * count,
         in_specs=[pl.BlockSpec(memory_space=pltpu.VMEM)]
         * (count + len(weights) + len(resumed)),
-        compiler_params=pltpu.CompilerParams(vmem_limit_bytes=20 << 20),
+        compiler_params=pltpu.CompilerParams(vmem_limit_bytes=12 << 20),
         cost_estimate=pl.CostEstimate(flops=flops, bytes_accessed=0, transcendentals=0),
         name="experts",
     )(*rows, *weights, *resumed)
@@ -403,39 +418,53 @@
     )(order, arrived, stream, norm_gain[None], places.reshape(2 * tokens, -1), *blocks)
 
 
-def expert_over_chips(rows, w_gate, w_up, w_down, capacity):
+def over_experts(halves, experts):
+    blocks = halves.reshape(experts, -1, halves.shape[1])
+    return lax.all_to_all(blocks, "sp", split_axis=0, concat_axis=0, tiled=True).reshape(
+        halves.shape
+    )
+
+
+def expert_over_chips(rows, w_gate, w_up, w_down, w_down_other, capacity):
     own = (w_gate, w_up, w_down)
-    rows, *sent = lax.optimization_barrier((rows, *own))
+    rows, *sent = lax.optimization_barrier((rows, w_gate, w_up))
     before = lax.ppermute(rows, "tp", chip_shift(1))
     after = lax.ppermute(rows, "tp", chip_shift(-1))
-    other = [lax.ppermute(w, "tp", chip_shift(0, 1)) for w in sent]
+    other = [lax.ppermute(w, "tp", chip_shift(0, 1)) for w in sent] + [w_down_other]
     (kept,) = partial_out((rows,), own, capacity, finished=False)
-    before, after, kept, late_rows = lax.optimization_barrier((before, after, kept, rows))
-    across = lax.ppermute(late_rows, "tp", chip_shift(2))
+    before, after, kept = lax.optimization_barrier((before, after, kept))
+    middle = rows.shape[0] // 2
+    across = (
+        lax.ppermute(before[:middle], "tp", chip_shift(1)),
+        lax.ppermute(after[middle:], "tp", chip_shift(-1)),
+    )
     near = partial_out((before, after), own, capacity, finished=False)
     for_before, for_after = partial_out((before, after), other, capacity, near)
+    to_before = lax.ppermute(for_before, "tp", chip_shift(-1))
+    to_after = lax.ppermute(for_after, "tp", chip_shift(1))
+    across, for_before = lax.optimization_barrier((across, for_before))
+    for_across = partial_out(across, (*own, *other), capacity)
+    to_across = [lax.ppermute(part, "tp", chip_shift(2)) for part in for_across]
+    rows, _ = lax.optimization_barrier((rows, for_across))
     (total,) = partial_out((rows,), other, capacity, (kept,))
-    (for_across,) = partial_out((across,), (*own, *other), capacity)
-    total = total.astype(jnp.float32)
-    total = total + lax.ppermute(for_before, "tp", chip_shift(-1)).astype(jnp.float32)
-    total = total + lax.ppermute(for_after, "tp", chip_shift(1)).astype(jnp.float32)
-    total = lax.optimization_barrier(total)
-    total = total + lax.ppermute(for_across, "tp", chip_shift(2)).astype(jnp.float32)
+    total = total.astype(jnp.float32) + to_before.astype(jnp.float32)
+    total = lax.optimization_barrier(total + to_after.astype(jnp.float32))
+    total = total + jnp.concatenate(to_across, axis=0).astype(jnp.float32)
     return total.astype(jnp.bfloat16)
 
 
-def weighted_pick(places, weights, returned_result):
-    width = returned_result.shape[0]
+def spread_weights(places, weights, width):
     tokens, top = weights.shape
     hits = places.reshape(2, tokens, top)[..., None] == jnp.arange(width, dtype=jnp.int32)
     spread = jnp.sum(jnp.where(hits, weights[None, :, :, None], 0.0), axis=2)
     spread = spread.reshape(2 * tokens, width)
     high = spread.astype(jnp.bfloat16)
-    low = (spread - high.astype(jnp.float32)).astype(jnp.bfloat16)
-    picked = jnp.dot(high, returned_result, preferred_element_type=jnp.float32) + jnp.dot(
-        low, returned_result, preferred_element_type=jnp.float32
-    )
-    return jnp.concatenate([picked[:tokens], picked[tokens:]], axis=1)
+    return jnp.concatenate([high, (spread - high.astype(jnp.float32)).astype(jnp.bfloat16)])
+
+
+def weighted_pick(spread, returned_result):
+    parts = jnp.dot(spread, returned_result, preferred_element_type=jnp.float32)
+    return parts[: len(parts) // 2] + parts[len(parts) // 2 :]
 
 
 def shards(
@@ -456,6 +485,7 @@
     w_up,
     w_down,
 ):
+    w_down_other = lax.ppermute(w_down[0], "tp", chip_shift(0, 1))
     totals, *kept = local_states(
         mixer_input,
         decay_shift,
@@ -467,10 +497,7 @@
     )
     ends = lax.all_to_all(totals, "sp", split_axis=0, concat_axis=0, tiled=True)
     blocks = gathered_projection(out_proj)
-    activated = activations(
-        lax.axis_index("sp"), ends, kept, mixer_input, readout_matrix, skip
-    )
-    own_rows, model = stream.shape
+    own_rows, _ = stream.shape
     weights = jax.nn.sigmoid(
         jnp.stack(
             [route_logits[:, 0] - route_logits[:, 1], route_logits[:, 1] - route_logits[:, 0]],
@@ -481,20 +508,23 @@
     capacity = 4 * own_rows // experts
     width = 2 * experts * capacity
     places = half_places(slot_numbers(routes, experts, capacity), capacity)
+    spread = spread_weights(places, weights, width)
+    ends, spread, places = lax.optimization_barrier((ends, spread, places))
+    activated = activations(
+        lax.axis_index("sp"), ends, kept, mixer_input, readout_matrix, skip
+    )
     mixed, outgoing = mixed_and_outgoing(
         activated, blocks, stream, norm_gain, places, width
     )
     mixed_wide = mixed.astype(jnp.float32)
 
-    def over_experts(halves):
-        blocks = halves.reshape(experts, 2 * capacity, model // 2)
-        return lax.all_to_all(blocks, "sp", split_axis=0, concat_axis=0, tiled=True).reshape(
-            width, model // 2
-        )
-
-    summed = expert_over_chips(over_experts(outgoing), w_gate[0], w_up[0], w_down[0], capacity)
-    combined = mixed_wide + weighted_pick(places, weights, over_experts(summed))
-    return combined.astype(jnp.bfloat16)
+    arrived = over_experts(outgoing, experts)
+    summed = expert_over_chips(
+        arrived, w_gate[0], w_up[0], w_down[0], w_down_other, capacity
+    )
+    picked = weighted_pick(spread, over_experts(summed, experts))
+    picked = jnp.concatenate([picked[:own_rows], picked[own_rows:]], axis=1)
+    return (mixed_wide + picked).astype(jnp.bfloat16)
 
 
 def solution(mesh):

time: 152 us -> 151 us (level)
  waiting for transfers between devices: 55.3 us -> 41.9 us
  Pallas kernels: 28.3 us -> 34.7 us
  starting transfers between devices: 35.4 us -> 41.1 us
    ppermute x7 -> x9, waiting for transfers between devices: 17.5 us -> 7.13 us  [the longest x1 7.11 us: expert_over_chips(): to_after = lax.ppermute(for_after, 'tp', chip_shift(1))]
    pallas_call x5, Pallas kernels: 16.6 us -> 22.9 us  [partial_out(): pl.pallas_call(kernel, out_shape=(out,) * count, in_specs=[pl.BlockSpec(m...]
    ppermute x7 -> x9, starting transfers between devices: 5.95 us -> 11.6 us  [the longest x2 3.87 us: expert_over_chips(): to_across = [lax.ppermute(part, 'tp', chip_shift(2)) for part in for_across]]
    ppermute x1, waiting for transfers between devices: 6.15 us -> 3.61 us  [expert_over_chips(): before = lax.ppermute(rows, 'tp', chip_shift(1))]
    unnamed x21 -> x23, local copies, waits for them, and re-layouts: 7.38 us -> 7.71 us
  transfers between devices with their start and end apart: 19 -> 21, of which waited for: 8 -> 6; matrix products, arithmetic and copies ran while one was open for 1% -> 2% of each run, Pallas kernels for 17% -> 22%
where the time goes in v1:
time: 151 us; the launch traced here: 150 us
  waiting for transfers between devices  41.9 us (28%)
  starting transfers between devices  41.1 us (27%)
  Pallas kernels  34.7 us (23%)
  blocking collectives  20.5 us (14%)
  local copies, waits for them, and re-layouts  8.34 us (6%)
  other arithmetic  3.13 us (2%)
    pallas_call x5, Pallas kernels, partial_out(): pl.pallas_call(kernel, out_shape=(out,) * count, in_specs=[pl.BlockSpec(m...  22.9 us
    all_to_all x1, blocking collectives, over_experts(): lax.all_to_all(blocks, 'sp', split_axis=0, concat_axis=0, tiled=True)  20.5 us
    all_to_all x1, waiting for transfers between devices, over_experts(): lax.all_to_all(blocks, 'sp', split_axis=0, concat_axis=0, tiled=True)  16.8 us
    all_to_all x1, starting transfers between devices, shards(): ends = lax.all_to_all(totals, 'sp', split_axis=0, concat_axis=0, tiled=True)  11.3 us
    unnamed x23, local copies, waits for them, and re-layouts  7.71 us
    ppermute x1, waiting for transfers between devices, expert_over_chips(): to_after = lax.ppermute(for_after, 'tp', chip_shift(1))  7.11 us
    all_to_all x1, waiting for transfers between devices, shards(): ends = lax.all_to_all(totals, 'sp', split_axis=0, concat_axis=0, tiled=True)  6.21 us
    ppermute x3, starting transfers between devices, gathered_projection(): lax.ppermute(out_proj, 'tp', chip_shift(distance))  5.9 us
  transfers between devices with their start and end apart: 21, of which 6 were waited for; matrix products, arithmetic and copies ran while one was open for 2% of the time, Pallas kernels for 22%

profile of v1, /device:TPU:32, one launch (start us, length us, event | category | flops | bytes accessed | tf_op | source)
XLA Modules:
  0.0 150.2 jit_solution(8831457348110813666)
XLA Ops:
  0.0 1.7 %collective-permute-start = (bf16[128,2048]{1,0:T(8,128)(2,1)}, bf16[128,2048]{1,0:T(8,128)(2,1)S(1)}, u32[]{:S(2)}, u32[]{:S(2)}) collective-permute-start(bf16[128,2048]{1,0:T(8,128)(2,1)} %refs_0_.1), channel_id=1, source_target_pairs={{0,2},{1,3},{2,4},{3,5},{4,6},{5,7},{6,0},{7,1},{8,10},{9,11},{10,... | collective-permute-start | bytes 1572872 | tf_op jit(solution)/shard_map/ppermute | solution.py:366
  1.7 2.9 %collective-permute-start.1 = (bf16[128,2048]{1,0:T(8,128)(2,1)}, bf16[128,2048]{1,0:T(8,128)(2,1)S(1)}, u32[]{:S(2)}, u32[]{:S(2)}) collective-permute-start(bf16[128,2048]{1,0:T(8,128)(2,1)} %refs_0_.1), channel_id=1, source_target_pairs={{0,4},{1,5},{2,6},{3,7},{4,0},{5,1},{6,2},{7,3},{8,12},{9,13},{10,... | collective-permute-start | bytes 1572872 | tf_op jit(solution)/shard_map/ppermute | solution.py:366
  4.6 1.3 collective-permute-start.2
  5.9 5.0 %states.1 = (f32[32,4,512]{2,1,0:T(4,128)}, f32[256,512]{1,0:T(8,128)}, f32[256,512]{1,0:T(8,128)}, f32[256,512]{1,0:T(8,128)}, f32[2,512]{1,0:T(2,128)}, /*index=5*/f32[4,8,512]{2,1,0:T(8,128)}) custom-call(bf16[256,128]{1,0:T(8,128)(2,1)} %refs_6_.1, f32[8,256]{1,0:T(8,128)} %bitcast.57, f32[8,64]{1,0:T(8,128)} %pole_real_hbm.1, f32[8,64]{1,0:T(8,128)} %pole_imag_hbm.1, ...), custom_call_target="tpu_custom_call" | custom-call | tf_op jit(solution)/shard_map/states/pallas_call | solution.py:225
  10.9 11.3 %all-to-all-start = ((f32[32,4,512]{2,1,0:T(4,128)}), f32[32,4,512]{2,1,0:T(4,128)}, u32[]{:S(2)}, u32[]{:S(2)}) async-start(f32[32,4,512]{2,1,0:T(4,128)} %get-tuple-element.31), calls=%async_computation | async-start | bytes 524288 | tf_op jit(solution)/shard_map/all_to_all | solution.py:498
  22.2 0.8 slice_subtract_fusion.1
  23.0 0.8 copy.29
  24.9 2.7 %collective-permute-done.1.refs_2_ = bf16[128,2048]{1,0:T(8,128)(2,1)S(1)} collective-permute-done((bf16[128,2048]{1,0:T(8,128)(2,1)}, bf16[128,2048]{1,0:T(8,128)(2,1)S(1)}, u32[]{:S(2)}, u32[]{:S(2)}) %collective-permute-start.1) | collective-permute-done | bytes 524320 | tf_op jit(solution)/shard_map/ppermute | solution.py:366
  28.8 6.2 %all-to-all-done.refs_0_ = f32[32,4,512]{2,1,0:T(4,128)} async-done(((f32[32,4,512]{2,1,0:T(4,128)}), f32[32,4,512]{2,1,0:T(4,128)}, u32[]{:S(2)}, u32[]{:S(2)}) %all-to-all-start) | async-done | bytes 262176 | tf_op jit(solution)/shard_map/all_to_all | solution.py:498
  35.0 4.5 %response.1 = bf16[256,128]{1,0:T(8,128)(2,1)} custom-call(s32[1]{0:T(128)} %bitcast.here_ref, f32[32,4,512]{2,1,0:T(4,128)} %all-to-all-done.refs_0_, f32[256,512]{1,0:T(8,128)} %get-tuple-element.33.refs_1_, f32[256,512]{1,0:T(8,128)} %get-tuple-element.34.refs_2_, f32[256,512]{1,0:T(8,128)} %get-tuple-element.35.refs_3_, ...), custom_call_target="tpu_custom_call" | custom-call | tf_op jit(solution)/shard_map/response/pallas_call | solution.py:253
  39.5 3.4 %all-to-all-start.1 = ((bf16[8,32,128]{2,1,0:T(8,128)(2,1)}), bf16[8,32,128]{2,1,0:T(8,128)(2,1)S(1)}, u32[]{:S(2)}, u32[]{:S(2)}) async-start(bf16[8,32,128]{2,1,0:T(8,128)(2,1)} %bitcast.54), calls=%async_computation.1 | async-start | bytes 131072 | tf_op jit(solution)/shard_map/all_to_all | solution.py:403
  43.1 5.3 %all-to-all-done.1.arrived_ref = bf16[8,32,128]{2,1,0:T(8,128)(2,1)S(1)} async-done(((bf16[8,32,128]{2,1,0:T(8,128)(2,1)}), bf16[8,32,128]{2,1,0:T(8,128)(2,1)S(1)}, u32[]{:S(2)}, u32[]{:S(2)}) %all-to-all-start.1) | async-done | bytes 65568 | tf_op jit(solution)/shard_map/all_to_all | solution.py:403
  48.5 2.3 %mix.1 = (bf16[32,2048]{1,0:T(8,128)(2,1)S(1)}, bf16[256,1024]{1,0:T(8,128)(2,1)S(1)}) custom-call(s32[8]{0:T(128)S(1)} %pad_add_fusion.1.order_ref, bf16[8,32,128]{2,1,0:T(8,128)(2,1)S(1)} %all-to-all-done.1.arrived_ref, bf16[32,2048]{1,0:T(8,128)(2,1)S(1)} %copy-done.8, f32[1,2048]{1,0:T(1,128)S(1)} %bitcast.53, s32[64,2]{1,0:T(8,128)S(1)} %reshape.193.places_ref, ...), custom_call_target="tpu_custom_call" | custom-call | tf_op jit(solution)/shard_map/mix/pallas_call | solution.py:408
  50.8 0.8 copy-done.7
  51.6 5.2 %all-to-all-start.2 = ((bf16[32,8,1024]{2,1,0:T(8,128)(2,1)}), bf16[32,8,1024]{2,1,0:T(8,128)(2,1)S(1)}, u32[]{:S(2)}, u32[]{:S(2)}) async-start(bf16[32,8,1024]{2,1,0:T(8,128)(2,1)} %bitcast.52), calls=%async_computation.2 | async-start | bytes 1048576 | tf_op jit(solution)/shard_map/all_to_all | solution.py:423
  57.0 16.8 %all-to-all-done.2 = bf16[32,8,1024]{2,1,0:T(8,128)(2,1)S(1)} async-done(((bf16[32,8,1024]{2,1,0:T(8,128)(2,1)}), bf16[32,8,1024]{2,1,0:T(8,128)(2,1)S(1)}, u32[]{:S(2)}, u32[]{:S(2)}) %all-to-all-start.2) | async-done | bytes 524320 | tf_op jit(solution)/shard_map/all_to_all | solution.py:423
  74.9 2.7 %collective-permute-start.8 = (bf16[256,1024]{1,0:T(8,128)(2,1)S(1)}, bf16[256,1024]{1,0:T(8,128)(2,1)S(1)}, u32[]{:S(2)}, u32[]{:S(2)}) collective-permute-start(bf16[256,1024]{1,0:T(8,128)(2,1)S(1)} %bitcast.49), channel_id=1, source_target_pairs={{0,6},{1,7},{2,0},{3,1},{4,2},{5,3},{6,4},{7,5},{8,14},{9,15},{10,... | collective-permute-start | bytes 1572872 | tf_op jit(solution)/shard_map/ppermute | solution.py:432
  77.6 2.0 %copy-done = bf16[1,2048,896]{2,1,0:T(8,128)(2,1)S(1)} copy-done((bf16[1,2048,896]{2,1,0:T(8,128)(2,1)S(1)}, bf16[1,2048,896]{2,1,0:T(8,128)(2,1)}, u32[]{:S(2)}) %copy-start) | copy-done | bytes 3670040
  79.6 2.0 %copy-done.2 = bf16[1,2048,896]{2,1,0:T(8,128)(2,1)S(1)} copy-done((bf16[1,2048,896]{2,1,0:T(8,128)(2,1)S(1)}, bf16[1,2048,896]{2,1,0:T(8,128)(2,1)}, u32[]{:S(2)}) %copy-start.2) | copy-done | bytes 3670040
  81.6 2.0 %copy-done.4 = bf16[1,896,2048]{2,1,0:T(8,128)(2,1)S(1)} copy-done((bf16[1,896,2048]{2,1,0:T(8,128)(2,1)S(1)}, bf16[1,896,2048]{2,1,0:T(8,128)(2,1)}, u32[]{:S(2)}) %copy-start.4) | copy-done | bytes 3670040
  83.7 2.1 %experts.5.refs_4_ = f32[128,2048]{1,0:T(8,128)S(1)} custom-call(bf16[256,1024]{1,0:T(8,128)(2,1)S(1)} %bitcast.50, bf16[2048,896]{1,0:T(8,128)(2,1)S(1)} %bitcast.37, bf16[2048,896]{1,0:T(8,128)(2,1)S(1)} %bitcast.41, bf16[896,2048]{1,0:T(8,128)(2,1)S(1)} %bitcast.45), custom_call_target="tpu_custom_call" | custom-call | flops 1409286144 | tf_op jit(solution)/shard_map/experts/pallas_call | solution.py:330
  85.8 3.6 %collective-permute-done.7.refs_0_ = bf16[256,1024]{1,0:T(8,128)(2,1)S(1)} collective-permute-done((bf16[256,1024]{1,0:T(8,128)(2,1)S(1)}, bf16[256,1024]{1,0:T(8,128)(2,1)S(1)}, u32[]{:S(2)}, u32[]{:S(2)}) %collective-permute-start.7) | collective-permute-done | bytes 524320 | tf_op jit(solution)/shard_map/ppermute | solution.py:431
  89.5 3.5 %collective-permute-start.10 = (bf16[128,1024]{1,0:T(8,128)(2,1)S(1)}, bf16[128,1024]{1,0:T(8,128)(2,1)S(1)}, u32[]{:S(2)}, u32[]{:S(2)}) collective-permute-start(bf16[128,1024]{1,0:T(8,128)(2,1)S(1)} %slice.29), channel_id=1, source_target_pairs={{0,6},{1,7},{2,0},{3,1},{4,2},{5,3},{6,4},{7,5},{8,14},{9,15},{10,... | collective-permute-start | bytes 786440 | tf_op jit(solution)/shard_map/ppermute | solution.py:439
  93.0 3.7 %experts.6 = (f32[128,2048]{1,0:T(8,128)S(1)}, f32[128,2048]{1,0:T(8,128)S(1)}) custom-call(bf16[256,1024]{1,0:T(8,128)(2,1)S(1)} %collective-permute-done.7.refs_0_, bf16[256,1024]{1,0:T(8,128)(2,1)S(1)} %collective-permute-done.8.refs_1_, bf16[2048,896]{1,0:T(8,128)(2,1)S(1)} %bitcast.38, bf16[2048,896]{1,0:T(8,128)(2,1)S(1)} %bitcast.42, ...), custom_call_target="tpu_custom_call" | custom-call | flops 2818572288 | tf_op jit(solution)/shard_map/experts/pallas_call | solution.py:330
  96.8 6.5 %experts.7 = (bf16[256,1024]{1,0:T(8,128)(2,1)S(1)}, bf16[256,1024]{1,0:T(8,128)(2,1)S(1)}) custom-call(bf16[256,1024]{1,0:T(8,128)(2,1)S(1)} %collective-permute-done.7.refs_0_, bf16[256,1024]{1,0:T(8,128)(2,1)S(1)} %collective-permute-done.8.refs_1_, bf16[2048,896]{1,0:T(8,128)(2,1)S(1)} %collective-permute-done.11.refs_2_.refs_5_.refs_1_, ...), custom_call_target="tpu_custom_call" | custom-call | flops 2818572288 | tf_op jit(solution)/shard_map/experts/pallas_call | solution.py:330
  103.5 3.2 %collective-permute-start.14 = (bf16[256,1024]{1,0:T(8,128)(2,1)S(1)}, bf16[256,1024]{1,0:T(8,128)(2,1)S(1)}, u32[]{:S(2)}, u32[]{:S(2)}) collective-permute-start(bf16[256,1024]{1,0:T(8,128)(2,1)S(1)} %get-tuple-element.49), channel_id=1, source_target_pairs={{0,6},{1,7},{2,0},{3,1},{4,2},{5,3},{6,4},{7,5},{8,14},{9,15},{10,... | collective-permute-start | bytes 1572872 | tf_op jit(solution)/shard_map/ppermute | solution.py:443
  106.7 6.1 %experts.8 = (bf16[128,1024]{1,0:T(8,128)(2,1)S(1)}, bf16[128,1024]{1,0:T(8,128)(2,1)S(1)}) custom-call(bf16[128,1024]{1,0:T(8,128)(2,1)S(1)} %collective-permute-done.9.refs_0_, bf16[128,1024]{1,0:T(8,128)(2,1)S(1)} %collective-permute-done.10.refs_1_, bf16[2048,896]{1,0:T(8,128)(2,1)S(1)} %bitcast.39, bf16[2048,896]{1,0:T(8,128)(2,1)S(1)} %bitcast.43, ...), custom_call_target="tpu_custom_call" | custom-call | flops 2818572288 | tf_op jit(solution)/shard_map/experts/pallas_call | solution.py:330
  113.2 3.5 %collective-permute-start.16 = (bf16[128,1024]{1,0:T(8,128)(2,1)S(1)}, bf16[128,1024]{1,0:T(8,128)(2,1)S(1)}, u32[]{:S(2)}, u32[]{:S(2)}) collective-permute-start(bf16[128,1024]{1,0:T(8,128)(2,1)S(1)} %get-tuple-element.52), channel_id=1, source_target_pairs={{0,4},{1,5},{2,6},{3,7},{4,0},{5,1},{6,2},{7,3},{8,12},{9,13},{10,... | collective-permute-start | bytes 786440 | tf_op jit(solution)/shard_map/ppermute | solution.py:447
  116.7 4.5 %experts.9 = bf16[256,1024]{1,0:T(8,128)(2,1)S(1)} custom-call(bf16[256,1024]{1,0:T(8,128)(2,1)S(1)} %bitcast.51, bf16[2048,896]{1,0:T(8,128)(2,1)S(1)} %collective-permute-done.11.refs_2_.refs_5_.refs_1_, bf16[2048,896]{1,0:T(8,128)(2,1)S(1)} %collective-permute-done.12.refs_3_.refs_6_.refs_2_, ...), custom_call_target="tpu_custom_call" | custom-call | flops 1409286144 | tf_op jit(solution)/shard_map/experts/pallas_call | solution.py:330
  121.2 7.1 %collective-permute-done.15 = bf16[256,1024]{1,0:T(8,128)(2,1)S(1)} collective-permute-done((bf16[256,1024]{1,0:T(8,128)(2,1)S(1)}, bf16[256,1024]{1,0:T(8,128)(2,1)S(1)}, u32[]{:S(2)}, u32[]{:S(2)}) %collective-permute-start.15) | collective-permute-done | bytes 524320 | tf_op jit(solution)/shard_map/ppermute | solution.py:444
  128.7 20.5 %all_to_all.20 = bf16[32,8,1024]{2,1,0:T(8,128)(2,1)S(1)} all-to-all(bf16[32,8,1024]{2,1,0:T(8,128)(2,1)S(1)} %fusion), channel_id=1, replica_groups=mesh['sp'=32,'tp'=8] {'sp'}, dimensions={0} | all-to-all | bytes 1048576 | tf_op jit(solution)/shard_map/all_to_all | solution.py:423
  149.5 0.7 fusion.3
  (70 shorter events, 5.1 us)
Async XLA Ops:
  0.0 48.4 %copy-start.6 = (bf16[128,2048]{1,0:T(8,128)(2,1)S(1)}, bf16[128,2048]{1,0:T(8,128)(2,1)}, u32[]{:S(2)}) copy-start(bf16[128,2048]{1,0:T(8,128)(2,1)} %refs_0_.1) | copy-start | bytes 1572868
  0.0 48.5 %copy-start.8 = (bf16[32,2048]{1,0:T(8,128)(2,1)S(1)}, bf16[32,2048]{1,0:T(8,128)(2,1)}, u32[]{:S(2)}) copy-start(bf16[32,2048]{1,0:T(8,128)(2,1)} %stream_ref.1) | copy-start | bytes 393220
  0.0 48.5 %copy-start.9 = (f32[2048]{0:T(1024)S(1)}, f32[2048]{0:T(1024)}, u32[]{:S(2)}) copy-start(f32[2048]{0:T(1024)} %param.26) | copy-start | bytes 24580
  0.0 24.8 %collective-permute-start = (bf16[128,2048]{1,0:T(8,128)(2,1)}, bf16[128,2048]{1,0:T(8,128)(2,1)S(1)}, u32[]{:S(2)}, u32[]{:S(2)}) collective-permute-start(bf16[128,2048]{1,0:T(8,128)(2,1)} %refs_0_.1), channel_id=1, source_target_pairs={{0,2},{1,3},{2,4},{3,5},{4,6},{5,7},{6,0},{7,1},{8,10},{9,11},{10,... | collective-permute-start | bytes 1572872 | tf_op jit(solution)/shard_map/ppermute | solution.py:366
  1.7 26.0 %collective-permute-start.1 = (bf16[128,2048]{1,0:T(8,128)(2,1)}, bf16[128,2048]{1,0:T(8,128)(2,1)S(1)}, u32[]{:S(2)}, u32[]{:S(2)}) collective-permute-start(bf16[128,2048]{1,0:T(8,128)(2,1)} %refs_0_.1), channel_id=1, source_target_pairs={{0,4},{1,5},{2,6},{3,7},{4,0},{5,1},{6,2},{7,3},{8,12},{9,13},{10,... | collective-permute-start | bytes 1572872 | tf_op jit(solution)/shard_map/ppermute | solution.py:366
  4.6 23.1 %collective-permute-start.2 = (bf16[128,2048]{1,0:T(8,128)(2,1)}, bf16[128,2048]{1,0:T(8,128)(2,1)S(1)}, u32[]{:S(2)}, u32[]{:S(2)}) collective-permute-start(bf16[128,2048]{1,0:T(8,128)(2,1)} %refs_0_.1), channel_id=1, source_target_pairs={{0,6},{1,7},{2,0},{3,1},{4,2},{5,3},{6,4},{7,5},{8,14},{9,15},{10,... | collective-permute-start | bytes 1572872 | tf_op jit(solution)/shard_map/ppermute | solution.py:366
  5.9 37.2 %collective-permute-start.3 = (bf16[128,2048]{1,0:T(8,128)(2,1)}, bf16[128,2048]{1,0:T(8,128)(2,1)S(1)}, u32[]{:S(2)}, u32[]{:S(2)}) collective-permute-start(bf16[128,2048]{1,0:T(8,128)(2,1)} %refs_0_.1), channel_id=1, source_target_pairs={{0,1},{1,0},{2,3},{3,2},{4,5},{5,4},{6,7},{7,6},{8,9},{9,8},{10,11... | collective-permute-start | bytes 1572872 | tf_op jit(solution)/shard_map/ppermute | solution.py:368
  10.9 24.1 %all-to-all-start = ((f32[32,4,512]{2,1,0:T(4,128)}), f32[32,4,512]{2,1,0:T(4,128)}, u32[]{:S(2)}, u32[]{:S(2)}) async-start(f32[32,4,512]{2,1,0:T(4,128)} %get-tuple-element.31), calls=%async_computation | async-start | bytes 524288 | tf_op jit(solution)/shard_map/all_to_all | solution.py:498
  24.8 23.6 %collective-permute-start.4 = (bf16[128,2048]{1,0:T(8,128)(2,1)S(1)}, bf16[128,2048]{1,0:T(8,128)(2,1)S(1)}, u32[]{:S(2)}, u32[]{:S(2)}) collective-permute-start(bf16[128,2048]{1,0:T(8,128)(2,1)S(1)} %collective-permute-done.refs_1_), channel_id=1, source_target_pairs={{0,1},{1,0},{2,3},{3,2},{4,5},{5,4},{6,7},{7,6},{8,9},{9,8},{10,11... | collective-permute-start | bytes 1572872 | tf_op jit(solution)/shard_map/ppermute | solution.py:368
  27.6 20.8 %collective-permute-start.5 = (bf16[128,2048]{1,0:T(8,128)(2,1)S(1)}, bf16[128,2048]{1,0:T(8,128)(2,1)}, u32[]{:S(2)}, u32[]{:S(2)}) collective-permute-start(bf16[128,2048]{1,0:T(8,128)(2,1)S(1)} %collective-permute-done.1.refs_2_), channel_id=1, source_target_pairs={{0,1},{1,0},{2,3},{3,2},{4,5},{5,4},{6,7},{7,6},{8,9},{9,8},{10,11... | collective-permute-start | bytes 1572872 | tf_op jit(solution)/shard_map/ppermute | solution.py:368
  27.7 20.8 %collective-permute-start.6 = (bf16[128,2048]{1,0:T(8,128)(2,1)S(1)}, bf16[128,2048]{1,0:T(8,128)(2,1)}, u32[]{:S(2)}, u32[]{:S(2)}) collective-permute-start(bf16[128,2048]{1,0:T(8,128)(2,1)S(1)} %collective-permute-done.2.refs_3_), channel_id=1, source_target_pairs={{0,1},{1,0},{2,3},{3,2},{4,5},{5,4},{6,7},{7,6},{8,9},{9,8},{10,11... | collective-permute-start | bytes 1572872 | tf_op jit(solution)/shard_map/ppermute | solution.py:368
  39.5 8.9 %all-to-all-start.1 = ((bf16[8,32,128]{2,1,0:T(8,128)(2,1)}), bf16[8,32,128]{2,1,0:T(8,128)(2,1)S(1)}, u32[]{:S(2)}, u32[]{:S(2)}) async-start(bf16[8,32,128]{2,1,0:T(8,128)(2,1)} %bitcast.54), calls=%async_computation.1 | async-start | bytes 131072 | tf_op jit(solution)/shard_map/all_to_all | solution.py:403
  50.7 0.8 copy-start.7
  51.6 22.3 %all-to-all-start.2 = ((bf16[32,8,1024]{2,1,0:T(8,128)(2,1)}), bf16[32,8,1024]{2,1,0:T(8,128)(2,1)S(1)}, u32[]{:S(2)}, u32[]{:S(2)}) async-start(bf16[32,8,1024]{2,1,0:T(8,128)(2,1)} %bitcast.52), calls=%async_computation.2 | async-start | bytes 1048576 | tf_op jit(solution)/shard_map/all_to_all | solution.py:423
  56.7 40.1 %collective-permute-start.13 = (bf16[896,2048]{1,0:T(8,128)(2,1)}, bf16[896,2048]{1,0:T(8,128)(2,1)}, u32[]{:S(2)}, u32[]{:S(2)}) collective-permute-start(bf16[896,2048]{1,0:T(8,128)(2,1)} %bitcast.44), channel_id=1, source_target_pairs={{0,1},{1,0},{2,3},{3,2},{4,5},{5,4},{6,7},{7,6},{8,9},{9,8},{10,11... | collective-permute-start | bytes 11010056 | tf_op jit(solution)/shard_map/ppermute | solution.py:488
  73.8 23.0 %collective-permute-start.11 = (bf16[2048,896]{1,0:T(8,128)(2,1)}, bf16[2048,896]{1,0:T(8,128)(2,1)S(1)}, u32[]{:S(2)}, u32[]{:S(2)}) collective-permute-start(bf16[2048,896]{1,0:T(8,128)(2,1)} %bitcast.36), channel_id=1, source_target_pairs={{0,1},{1,0},{2,3},{3,2},{4,5},{5,4},{6,7},{7,6},{8,9},{9,8},{10,11... | collective-permute-start | bytes 11010056 | tf_op jit(solution)/shard_map/ppermute | solution.py:433
  73.8 23.0 %collective-permute-start.12 = (bf16[2048,896]{1,0:T(8,128)(2,1)}, bf16[2048,896]{1,0:T(8,128)(2,1)S(1)}, u32[]{:S(2)}, u32[]{:S(2)}) collective-permute-start(bf16[2048,896]{1,0:T(8,128)(2,1)} %bitcast.40), channel_id=1, source_target_pairs={{0,1},{1,0},{2,3},{3,2},{4,5},{5,4},{6,7},{7,6},{8,9},{9,8},{10,11... | collective-permute-start | bytes 11010056 | tf_op jit(solution)/shard_map/ppermute | solution.py:433
  74.3 15.0 %collective-permute-start.7 = (bf16[256,1024]{1,0:T(8,128)(2,1)S(1)}, bf16[256,1024]{1,0:T(8,128)(2,1)S(1)}, u32[]{:S(2)}, u32[]{:S(2)}) collective-permute-start(bf16[256,1024]{1,0:T(8,128)(2,1)S(1)} %bitcast.48), channel_id=1, source_target_pairs={{0,2},{1,3},{2,4},{3,5},{4,6},{5,7},{6,0},{7,1},{8,10},{9,11},{10,... | collective-permute-start | bytes 1572872 | tf_op jit(solution)/shard_map/ppermute | solution.py:431
  74.9 14.5 %collective-permute-start.8 = (bf16[256,1024]{1,0:T(8,128)(2,1)S(1)}, bf16[256,1024]{1,0:T(8,128)(2,1)S(1)}, u32[]{:S(2)}, u32[]{:S(2)}) collective-permute-start(bf16[256,1024]{1,0:T(8,128)(2,1)S(1)} %bitcast.49), channel_id=1, source_target_pairs={{0,6},{1,7},{2,0},{3,1},{4,2},{5,3},{6,4},{7,5},{8,14},{9,15},{10,... | collective-permute-start | bytes 1572872 | tf_op jit(solution)/shard_map/ppermute | solution.py:432
  77.6 2.0 %copy-start = (bf16[1,2048,896]{2,1,0:T(8,128)(2,1)S(1)}, bf16[1,2048,896]{2,1,0:T(8,128)(2,1)}, u32[]{:S(2)}) copy-start(bf16[1,2048,896]{2,1,0:T(8,128)(2,1)} %param.29) | copy-start | bytes 11010052
  79.6 2.0 %copy-start.2 = (bf16[1,2048,896]{2,1,0:T(8,128)(2,1)S(1)}, bf16[1,2048,896]{2,1,0:T(8,128)(2,1)}, u32[]{:S(2)}) copy-start(bf16[1,2048,896]{2,1,0:T(8,128)(2,1)} %param.30) | copy-start | bytes 11010052
  81.6 2.0 %copy-start.4 = (bf16[1,896,2048]{2,1,0:T(8,128)(2,1)S(1)}, bf16[1,896,2048]{2,1,0:T(8,128)(2,1)}, u32[]{:S(2)}) copy-start(bf16[1,896,2048]{2,1,0:T(8,128)(2,1)} %param.31) | copy-start | bytes 11010052
  89.4 17.3 %collective-permute-start.9 = (bf16[128,1024]{1,0:T(8,128)(2,1)S(1)}, bf16[128,1024]{1,0:T(8,128)(2,1)S(1)}, u32[]{:S(2)}, u32[]{:S(2)}) collective-permute-start(bf16[128,1024]{1,0:T(8,128)(2,1)S(1)} %slice.28), channel_id=1, source_target_pairs={{0,2},{1,3},{2,4},{3,5},{4,6},{5,7},{6,0},{7,1},{8,10},{9,11},{10,... | collective-permute-start | bytes 786440 | tf_op jit(solution)/shard_map/ppermute | solution.py:438
  89.5 17.2 %collective-permute-start.10 = (bf16[128,1024]{1,0:T(8,128)(2,1)S(1)}, bf16[128,1024]{1,0:T(8,128)(2,1)S(1)}, u32[]{:S(2)}, u32[]{:S(2)}) collective-permute-start(bf16[128,1024]{1,0:T(8,128)(2,1)S(1)} %slice.29), channel_id=1, source_target_pairs={{0,6},{1,7},{2,0},{3,1},{4,2},{5,3},{6,4},{7,5},{8,14},{9,15},{10,... | collective-permute-start | bytes 786440 | tf_op jit(solution)/shard_map/ppermute | solution.py:439
  96.8 9.9 %copy-start.1 = (bf16[1,2048,896]{2,1,0:T(8,128)(2,1)S(1)}, bf16[1,2048,896]{2,1,0:T(8,128)(2,1)}, u32[]{:S(2)}) copy-start(bf16[1,2048,896]{2,1,0:T(8,128)(2,1)} %param.29) | copy-start | bytes 11010052
  96.8 9.9 %copy-start.3 = (bf16[1,2048,896]{2,1,0:T(8,128)(2,1)S(1)}, bf16[1,2048,896]{2,1,0:T(8,128)(2,1)}, u32[]{:S(2)}) copy-start(bf16[1,2048,896]{2,1,0:T(8,128)(2,1)} %param.30) | copy-start | bytes 11010052
  96.8 9.9 %copy-start.5 = (bf16[1,896,2048]{2,1,0:T(8,128)(2,1)S(1)}, bf16[1,896,2048]{2,1,0:T(8,128)(2,1)}, u32[]{:S(2)}) copy-start(bf16[1,896,2048]{2,1,0:T(8,128)(2,1)} %param.31) | copy-start | bytes 11010052
  103.4 24.9 %collective-permute-start.15 = (bf16[256,1024]{1,0:T(8,128)(2,1)S(1)}, bf16[256,1024]{1,0:T(8,128)(2,1)S(1)}, u32[]{:S(2)}, u32[]{:S(2)}) collective-permute-start(bf16[256,1024]{1,0:T(8,128)(2,1)S(1)} %get-tuple-element.56), channel_id=1, source_target_pairs={{0,2},{1,3},{2,4},{3,5},{4,6},{5,7},{6,0},{7,1},{8,10},{9,11},{10,... | collective-permute-start | bytes 1572872 | tf_op jit(solution)/shard_map/ppermute | solution.py:444
  103.5 24.9 %collective-permute-start.14 = (bf16[256,1024]{1,0:T(8,128)(2,1)S(1)}, bf16[256,1024]{1,0:T(8,128)(2,1)S(1)}, u32[]{:S(2)}, u32[]{:S(2)}) collective-permute-start(bf16[256,1024]{1,0:T(8,128)(2,1)S(1)} %get-tuple-element.49), channel_id=1, source_target_pairs={{0,6},{1,7},{2,0},{3,1},{4,2},{5,3},{6,4},{7,5},{8,14},{9,15},{10,... | collective-permute-start | bytes 1572872 | tf_op jit(solution)/shard_map/ppermute | solution.py:443
  112.8 15.7 %collective-permute-start.17 = (bf16[128,1024]{1,0:T(8,128)(2,1)S(1)}, bf16[128,1024]{1,0:T(8,128)(2,1)S(1)}, u32[]{:S(2)}, u32[]{:S(2)}) collective-permute-start(bf16[128,1024]{1,0:T(8,128)(2,1)S(1)} %get-tuple-element.53), channel_id=1, source_target_pairs={{0,4},{1,5},{2,6},{3,7},{4,0},{5,1},{6,2},{7,3},{8,12},{9,13},{10,... | collective-permute-start | bytes 786440 | tf_op jit(solution)/shard_map/ppermute | solution.py:447
  113.2 15.4 %collective-permute-start.16 = (bf16[128,1024]{1,0:T(8,128)(2,1)S(1)}, bf16[128,1024]{1,0:T(8,128)(2,1)S(1)}, u32[]{:S(2)}, u32[]{:S(2)}) collective-permute-start(bf16[128,1024]{1,0:T(8,128)(2,1)S(1)} %get-tuple-element.52), channel_id=1, source_target_pairs={{0,4},{1,5},{2,6},{3,7},{4,0},{5,1},{6,2},{7,3},{8,12},{9,13},{10,... | collective-permute-start | bytes 786440 | tf_op jit(solution)/shard_map/ppermute | solution.py:447
  121.2 28.1 %copy-start.10 = (bf16[128,256]{1,0:T(8,128)(2,1)S(1)}, bf16[128,256]{1,0:T(8,128)(2,1)}, u32[]{:S(2)}) copy-start(bf16[128,256]{1,0:T(8,128)(2,1)} %pad_maximum_fusion) | copy-start | bytes 196612

commit v2 on v1

--- a/solution.py
+++ b/solution.py
@@ -104,14 +104,21 @@
     wide_imag = jnp.broadcast_to(factor_imag, (LANES, width))
     through_real = jnp.ones((LANES, width), jnp.float32)
     through_imag = state_real = state_imag = jnp.zeros((LANES, width), jnp.float32)
-    for k in range(length):
-        at = slice(k * LANES, (k + 1) * LANES)
+
+    def advance(k, held):
+        through_real, through_imag, state_real, state_imag = held
+        at = pl.ds(pl.multiple_of(k * LANES, LANES), LANES)
         scale = scale_ref[at, :]
         real, imag = scale * wide_real, scale * wide_imag
         through_real, through_imag = complex_times(real, imag, through_real, through_imag)
         state_real, state_imag = complex_times(real, imag, state_real, state_imag)
         state_real = state_real + drive_real_ref[at, :]
         state_imag = state_imag + drive_imag_ref[at, :]
+        return through_real, through_imag, state_real, state_imag
+
+    through_real, through_imag, state_real, state_imag = lax.fori_loop(
+        0, length, advance, (through_real, through_imag, state_real, state_imag), unroll=8
+    )
 
     place = lax.broadcasted_iota(jnp.int32, (LANES, width), 0)
 
@@ -180,8 +187,10 @@
     state_real, state_imag = state_real + enter_ref[2], state_imag + enter_ref[3]
     wide_real = jnp.broadcast_to(factor_ref[0:1, :], (LANES, width))
     wide_imag = jnp.broadcast_to(factor_ref[1:2, :], (LANES, width))
-    for k in range(length):
-        at = slice(k * LANES, (k + 1) * LANES)
+
+    def advance(k, held):
+        state_real, state_imag = held
+        at = pl.ds(pl.multiple_of(k * LANES, LANES), LANES)
         scale = scale_ref[at, :]
         real, imag = scale * wide_real, scale * wide_imag
         state_real, state_imag = complex_times(real, imag, state_real, state_imag)
@@ -189,6 +198,9 @@
         state_imag = state_imag + drive_imag_ref[at, :]
         state_ref[at, :width] = state_real
         state_ref[at, width:] = state_imag
+        return state_real, state_imag
+
+    lax.fori_loop(0, length, advance, (state_real, state_imag), unroll=8)
     spread = one_hot((states, width), lambda r, c: c % states == r)
     same_group = one_hot(
         (readout_ref.shape[1], width), lambda r, c: r // channels == c // states
@@ -263,10 +275,9 @@
     )(here.reshape(1), *operands)
 
 
-def experts_kernel(capacity, count, sets, resumed, finished, *refs):
+def experts_kernel(capacity, count, sets, *refs):
     row_refs, refs = refs[:count], refs[count:]
-    weights, refs = refs[: 3 * sets], refs[3 * sets :]
-    before, outs = (refs[:count], refs[count:]) if resumed else ((), refs)
+    weights, outs = refs[: 3 * sets], refs[3 * sets :]
     held, part = row_refs[0].shape[0] // 2, row_refs[0].shape[1]
 
     def whole_rows(half):
@@ -283,7 +294,7 @@
         ).astype(jnp.bfloat16)
         for chosen in pick
     ]
-    total = jnp.concatenate([ref[...] for ref in before], axis=0) if resumed else None
+    total = None
     for number in range(sets):
         gate_ref, up_ref, down_ref = weights[3 * number : 3 * number + 3]
 
@@ -300,42 +311,57 @@
         hidden = (jax.nn.silu(product(gate_ref)) * product(up_ref)).astype(jnp.bfloat16)
         out = jnp.dot(hidden, down_ref[...], preferred_element_type=jnp.float32)
         total = out if total is None else total + out
+    total = total.astype(jnp.bfloat16)
     for number, ref in enumerate(outs):
         rows = total[number * held : (number + 1) * held]
-        if finished:
-            rows = rows.astype(jnp.bfloat16)
-            rows = sum(
-                lax.dot_general(
-                    pick[half],
-                    rows[:, half * part : (half + 1) * part],
-                    (((0,), (0,)), ((), ())),
-                    preferred_element_type=jnp.float32,
-                )
-                for half in range(2)
-            ).astype(jnp.bfloat16)
-        ref[...] = rows
-
-
-def partial_out(rows, weights, capacity, resumed=(), finished=True):
+        ref[...] = sum(
+            lax.dot_general(
+                pick[half],
+                rows[:, half * part : (half + 1) * part],
+                (((0,), (0,)), ((), ())),
+                preferred_element_type=jnp.float32,
+            )
+            for half in range(2)
+        ).astype(jnp.bfloat16)
+
+
+def partial_out(rows, weights, capacity):
     count, sets = len(rows), len(weights) // 3
-    halves, part = rows[0].shape
-    if finished:
-        out = jax.ShapeDtypeStruct((halves, part), jnp.bfloat16)
-    else:
-        out = jax.ShapeDtypeStruct((halves // 2, 2 * part), jnp.float32)
-    kernel = functools.partial(
-        experts_kernel, capacity, count, sets, bool(resumed), finished
-    )
-    flops = 2 * count * (halves // 2) * sum(w.size for w in weights)
+    out = jax.ShapeDtypeStruct(rows[0].shape, jnp.bfloat16)
+    flops = count * rows[0].shape[0] * sum(w.size for w in weights)
     return pl.pallas_call(
-        kernel,
+        functools.partial(experts_kernel, capacity, count, sets),
         out_shape=(out,) * count,
-        in_specs=[pl.BlockSpec(memory_space=pltpu.VMEM)]
-        * (count + len(weights) + len(resumed)),
+        in_specs=[pl.BlockSpec(memory_space=pltpu.VMEM)] * (count + len(weights)),
         compiler_params=pltpu.CompilerParams(vmem_limit_bytes=12 << 20),
         cost_estimate=pl.CostEstimate(flops=flops, bytes_accessed=0, transcendentals=0),
         name="experts",
-    )(*rows, *weights, *resumed)
+    )(*rows, *weights)
+
+
+def stage_kernel(*refs):
+    count = len(refs) // 2
+    copies = [
+        pltpu.make_async_copy(refs[number], refs[count + number], refs[-1].at[number])
+        for number in range(count)
+    ]
+    for copy in copies:
+        copy.start()
+    for copy in copies:
+        copy.wait()
+
+
+def staged(arrays):
+    return pl.pallas_call(
+        stage_kernel,
+        out_shape=[jax.ShapeDtypeStruct(array.shape, array.dtype) for array in arrays],
+        in_specs=[pl.BlockSpec(memory_space=pltpu.HBM)] * len(arrays),
+        out_specs=[pl.BlockSpec(memory_space=pltpu.VMEM)] * len(arrays),
+        scratch_shapes=[pltpu.SemaphoreType.DMA((len(arrays),))],
+        compiler_params=pltpu.CompilerParams(vmem_limit_bytes=32 << 20),
+        cost_estimate=pl.CostEstimate(flops=1 << 33, bytes_accessed=0, transcendentals=0),
+        name="stage",
+    )(*arrays)
 
 
 def slot_numbers(route_rows, experts, capacity):
@@ -425,28 +451,31 @@
     )
 
 
-def expert_over_chips(rows, w_gate, w_up, w_down, w_down_other, capacity):
-    own = (w_gate, w_up, w_down)
-    rows, *sent = lax.optimization_barrier((rows, w_gate, w_up))
+def expert_over_chips(rows, w_gate, w_up, w_down, w_up_other, w_down_other, capacity):
+    rows, sent, *kept = lax.optimization_barrier(
+        (rows, w_gate, w_gate, w_up, w_down, w_up_other, w_down_other)
+    )
     before = lax.ppermute(rows, "tp", chip_shift(1))
     after = lax.ppermute(rows, "tp", chip_shift(-1))
-    other = [lax.ppermute(w, "tp", chip_shift(0, 1)) for w in sent] + [w_down_other]
-    (kept,) = partial_out((rows,), own, capacity, finished=False)
-    before, after, kept = lax.optimization_barrier((before, after, kept))
+    w_gate_other = lax.ppermute(sent, "tp", chip_shift(0, 1))
+    w_gate, w_up, w_down, w_up_other, w_down_other = staged(kept)
+    weights = (w_gate, w_up, w_down, w_gate_other, w_up_other, w_down_other)
+    before, after, *weights = lax.optimization_barrier((before, after, *weights))
     middle = rows.shape[0] // 2
     across = (
         lax.ppermute(before[:middle], "tp", chip_shift(1)),
         lax.ppermute(after[middle:], "tp", chip_shift(-1)),
     )
-    near = partial_out((before, after), own, capacity, finished=False)
-    for_before, for_after = partial_out((before, after), other, capacity, near)
+    (for_before,) = partial_out((before,), weights, capacity)
     to_before = lax.ppermute(for_before, "tp", chip_shift(-1))
+    after, for_before = lax.optimization_barrier((after, for_before))
+    (for_after,) = partial_out((after,), weights, capacity)
     to_after = lax.ppermute(for_after, "tp", chip_shift(1))
-    across, for_before = lax.optimization_barrier((across, for_before))
-    for_across = partial_out(across, (*own, *other), capacity)
+    across, for_after = lax.optimization_barrier((across, for_after))
+    for_across = partial_out(across, weights, capacity)
     to_across = [lax.ppermute(part, "tp", chip_shift(2)) for part in for_across]
     rows, _ = lax.optimization_barrier((rows, for_across))
-    (total,) = partial_out((rows,), other, capacity, (kept,))
+    (total,) = partial_out((rows,), weights, capacity)
     total = total.astype(jnp.float32) + to_before.astype(jnp.float32)
     total = lax.optimization_barrier(total + to_after.astype(jnp.float32))
     total = total + jnp.concatenate(to_across, axis=0).astype(jnp.float32)
@@ -486,6 +515,7 @@
     w_down,
 ):
     w_down_other = lax.ppermute(w_down[0], "tp", chip_shift(0, 1))
+    w_up_other = lax.ppermute(w_up[0], "tp", chip_shift(0, 1))
     totals, *kept = local_states(
         mixer_input,
         decay_shift,
@@ -520,7 +550,7 @@
 
     arrived = over_experts(outgoing, experts)
     summed = expert_over_chips(
-        arrived, w_gate[0], w_up[0], w_down[0], w_down_other, capacity
+        arrived, w_gate[0], w_up[0], w_down[0], w_up_other, w_down_other, capacity
     )
     picked = weighted_pick(spread, over_experts(summed, experts))
     picked = jnp.concatenate([picked[:own_rows], picked[own_rows:]], axis=1)

time: 151 us -> 153 us (1.013)
  the two profiles are of different devices: /device:TPU:32 before, /device:TPU:24 now
where the time goes in v2:
time: 153 us; the launch traced here: 152 us
  blocking collectives  43.3 us (28%)
  starting transfers between devices  36 us (24%)
  Pallas kernels  35.2 us (23%)
  waiting for transfers between devices  33.4 us (22%)
  other arithmetic  2.52 us (2%)
    all_to_all x2, blocking collectives, over_experts(): lax.all_to_all(blocks, 'sp', split_axis=0, concat_axis=0, tiled=True)  43.3 us
    pallas_call x4, Pallas kernels, partial_out(): pl.pallas_call(functools.partial(experts_kernel, capacity, count, sets),...  16.8 us
    all_to_all x1, starting transfers between devices, shards(): ends = lax.all_to_all(totals, 'sp', split_axis=0, concat_axis=0, tiled=True)  11.5 us
    ppermute x1, waiting for transfers between devices, expert_over_chips(): lax.ppermute(after[middle:], 'tp', chip_shift(-1))  9.48 us
    all_to_all x1, starting transfers between devices, mixed_and_outgoing(): lax.all_to_all(activated.reshape(size, tokens, -1), 'tp', split_axis=0, c...  6.48 us
    pallas_call x1, Pallas kernels, staged(): pl.pallas_call(stage_kernel, out_shape=[jax.ShapeDtypeStruct(array.shape,...  6.33 us
    ppermute x2, waiting for transfers between devices, expert_over_chips(): to_across = [lax.ppermute(part, 'tp', chip_shift(2)) for part in for_across]  6.05 us
    ppermute x1, waiting for transfers between devices, expert_over_chips(): after = lax.ppermute(rows, 'tp', chip_shift(-1))  5.89 us
  transfers between devices with their start and end apart: 20, of which 8 were waited for; matrix products, arithmetic and copies ran while one was open for 2% of the time, Pallas kernels for 20%

profile of v2, /device:TPU:24, one launch (start us, length us, event | category | flops | bytes accessed | tf_op | source)
XLA Modules:
  0.0 152.4 jit_solution(11235855462459916250)
XLA Ops:
  0.6 1.8 %collective-permute-start = (bf16[128,2048]{1,0:T(8,128)(2,1)}, bf16[128,2048]{1,0:T(8,128)(2,1)S(1)}, u32[]{:S(2)}, u32[]{:S(2)}) collective-permute-start(bf16[128,2048]{1,0:T(8,128)(2,1)} %refs_0_.1), channel_id=1, source_target_pairs={{0,2},{1,3},{2,4},{3,5},{4,6},{5,7},{6,0},{7,1},{8,10},{9,11},{10,... | collective-permute-start | bytes 1572872 | tf_op jit(solution)/shard_map/ppermute | solution.py:392
  2.4 1.0 collective-permute-start.1
  3.4 5.4 %states.1 = (f32[32,4,512]{2,1,0:T(4,128)}, f32[256,512]{1,0:T(8,128)}, f32[256,512]{1,0:T(8,128)}, f32[256,512]{1,0:T(8,128)}, f32[2,512]{1,0:T(2,128)}, /*index=5*/f32[4,8,512]{2,1,0:T(8,128)}) custom-call(bf16[256,128]{1,0:T(8,128)(2,1)} %refs_6_.1, f32[8,256]{1,0:T(8,128)} %bitcast.44, f32[8,64]{1,0:T(8,128)} %pole_real_hbm.1, f32[8,64]{1,0:T(8,128)} %pole_imag_hbm.1, ...), custom_call_target="tpu_custom_call" | custom-call | tf_op jit(solution)/shard_map/states/pallas_call | solution.py:237
  8.8 11.5 %all-to-all-start = ((f32[32,4,512]{2,1,0:T(4,128)}), f32[32,4,512]{2,1,0:T(4,128)}, u32[]{:S(2)}, u32[]{:S(2)}) async-start(f32[32,4,512]{2,1,0:T(4,128)} %get-tuple-element.42), calls=%async_computation | async-start | bytes 524288 | tf_op jit(solution)/shard_map/all_to_all | solution.py:528
  20.3 0.8 copy.29
  21.9 0.8 slice_subtract_fusion.1
  22.7 2.8 %collective-permute-done.refs_1_ = bf16[128,2048]{1,0:T(8,128)(2,1)S(1)} collective-permute-done((bf16[128,2048]{1,0:T(8,128)(2,1)}, bf16[128,2048]{1,0:T(8,128)(2,1)S(1)}, u32[]{:S(2)}, u32[]{:S(2)}) %collective-permute-start) | collective-permute-done | bytes 524320 | tf_op jit(solution)/shard_map/ppermute | solution.py:392
  25.7 0.6 collective-permute-start.4
  26.2 2.8 %collective-permute-done.2.refs_3_ = bf16[128,2048]{1,0:T(8,128)(2,1)S(1)} collective-permute-done((bf16[128,2048]{1,0:T(8,128)(2,1)}, bf16[128,2048]{1,0:T(8,128)(2,1)S(1)}, u32[]{:S(2)}, u32[]{:S(2)}) %collective-permute-start.2) | collective-permute-done | bytes 524320 | tf_op jit(solution)/shard_map/ppermute | solution.py:392
  29.6 3.0 %all-to-all-done.refs_0_ = f32[32,4,512]{2,1,0:T(4,128)} async-done(((f32[32,4,512]{2,1,0:T(4,128)}), f32[32,4,512]{2,1,0:T(4,128)}, u32[]{:S(2)}, u32[]{:S(2)}) %all-to-all-start) | async-done | bytes 262176 | tf_op jit(solution)/shard_map/all_to_all | solution.py:528
  32.6 4.5 %response.1 = bf16[256,128]{1,0:T(8,128)(2,1)} custom-call(s32[1]{0:T(128)} %bitcast.here_ref, f32[32,4,512]{2,1,0:T(4,128)} %all-to-all-done.refs_0_, f32[256,512]{1,0:T(8,128)} %get-tuple-element.44.refs_1_, f32[256,512]{1,0:T(8,128)} %get-tuple-element.45.refs_2_, f32[256,512]{1,0:T(8,128)} %get-tuple-element.46.refs_3_, ...), custom_call_target="tpu_custom_call" | custom-call | tf_op jit(solution)/shard_map/response/pallas_call | solution.py:265
  37.2 6.5 %all-to-all-start.1 = ((bf16[8,32,128]{2,1,0:T(8,128)(2,1)}), bf16[8,32,128]{2,1,0:T(8,128)(2,1)S(1)}, u32[]{:S(2)}, u32[]{:S(2)}) async-start(bf16[8,32,128]{2,1,0:T(8,128)(2,1)} %bitcast.41), calls=%async_computation.1 | async-start | bytes 131072 | tf_op jit(solution)/shard_map/all_to_all | solution.py:429
  43.8 3.3 %all-to-all-done.1.arrived_ref = bf16[8,32,128]{2,1,0:T(8,128)(2,1)S(1)} async-done(((bf16[8,32,128]{2,1,0:T(8,128)(2,1)}), bf16[8,32,128]{2,1,0:T(8,128)(2,1)S(1)}, u32[]{:S(2)}, u32[]{:S(2)}) %all-to-all-start.1) | async-done | bytes 65568 | tf_op jit(solution)/shard_map/all_to_all | solution.py:429
  47.2 2.3 %mix.1 = (bf16[32,2048]{1,0:T(8,128)(2,1)S(1)}, bf16[256,1024]{1,0:T(8,128)(2,1)S(1)}) custom-call(s32[8]{0:T(128)S(1)} %pad_add_fusion.1.order_ref, bf16[8,32,128]{2,1,0:T(8,128)(2,1)S(1)} %all-to-all-done.1.arrived_ref, bf16[32,2048]{1,0:T(8,128)(2,1)S(1)} %copy-done.1, f32[1,2048]{1,0:T(1,128)S(1)} %bitcast.40, s32[64,2]{1,0:T(8,128)S(1)} %reshape.193.places_ref, ...), custom_call_target="tpu_custom_call" | custom-call | tf_op jit(solution)/shard_map/mix/pallas_call | solution.py:434
  49.5 22.7 %all_to_all.20 = bf16[32,8,1024]{2,1,0:T(8,128)(2,1)S(1)} all-to-all(bf16[32,8,1024]{2,1,0:T(8,128)(2,1)S(1)} %bitcast.39), channel_id=1, replica_groups=mesh['sp'=32,'tp'=8] {'sp'}, dimensions={0} | all-to-all | bytes 1048576 | tf_op jit(solution)/shard_map/all_to_all | solution.py:449
  72.7 2.8 %collective-permute-start.9 = (bf16[256,1024]{1,0:T(8,128)(2,1)S(1)}, bf16[256,1024]{1,0:T(8,128)(2,1)S(1)}, u32[]{:S(2)}, u32[]{:S(2)}) collective-permute-start(bf16[256,1024]{1,0:T(8,128)(2,1)S(1)} %bitcast.37), channel_id=1, source_target_pairs={{0,2},{1,3},{2,4},{3,5},{4,6},{5,7},{6,0},{7,1},{8,10},{9,11},{10,... | collective-permute-start | bytes 1572872 | tf_op jit(solution)/shard_map/ppermute | solution.py:458
  75.5 6.3 %stage.1 = (bf16[2048,896]{1,0:T(8,128)(2,1)S(1)}, bf16[2048,896]{1,0:T(8,128)(2,1)S(1)}, bf16[896,2048]{1,0:T(8,128)(2,1)S(1)}, bf16[2048,896]{1,0:T(8,128)(2,1)S(1)}, bf16[896,2048]{1,0:T(8,128)(2,1)S(1)}) custom-call(bf16[2048,896]{1,0:T(8,128)(2,1)} %bitcast.16.refs_0_, bf16[2048,896]{1,0:T(8,128)(2,1)} %bitcast.50, bf16[896,2048]{1,0:T(8,128)(2,1)} %bitcast.52, ...), custom_call_target="tpu_custom_call" | custom-call | flops 8589934592 | tf_op jit(solution)/shard_map/stage/pallas_call | solution.py:355
  81.9 5.9 %collective-permute-done.10.refs_0_ = bf16[256,1024]{1,0:T(8,128)(2,1)S(1)} collective-permute-done((bf16[256,1024]{1,0:T(8,128)(2,1)S(1)}, bf16[256,1024]{1,0:T(8,128)(2,1)S(1)}, u32[]{:S(2)}, u32[]{:S(2)}) %collective-permute-start.10) | collective-permute-done | bytes 524320 | tf_op jit(solution)/shard_map/ppermute | solution.py:459
  87.8 4.2 %experts.4 = bf16[256,1024]{1,0:T(8,128)(2,1)S(1)} custom-call(bf16[256,1024]{1,0:T(8,128)(2,1)S(1)} %collective-permute-done.9.refs_0_, bf16[2048,896]{1,0:T(8,128)(2,1)S(1)} %get-tuple-element.67.refs_1_.refs_2_, bf16[2048,896]{1,0:T(8,128)(2,1)S(1)} %get-tuple-element.68.refs_2_.refs_3_, bf16[896,2048]{1,0:T(8,128)(2,1)S(1)} %get-tuple-element.69.refs_3_.refs_4_, ...), custom_call_target="tpu_custom_call" | custom-call | flops 2818572288 | tf_op jit(solution)/shard_map/experts/pallas_call | solution.py:332
  92.0 0.6 collective-permute-start.14
  92.6 2.7 %collective-permute-start.12 = (bf16[128,1024]{1,0:T(8,128)(2,1)S(1)}, bf16[128,1024]{1,0:T(8,128)(2,1)S(1)}, u32[]{:S(2)}, u32[]{:S(2)}) collective-permute-start(bf16[128,1024]{1,0:T(8,128)(2,1)S(1)} %slice.28), channel_id=1, source_target_pairs={{0,2},{1,3},{2,4},{3,5},{4,6},{5,7},{6,0},{7,1},{8,10},{9,11},{10,... | collective-permute-start | bytes 786440 | tf_op jit(solution)/shard_map/ppermute | solution.py:466
  95.3 4.2 %experts.5 = bf16[256,1024]{1,0:T(8,128)(2,1)S(1)} custom-call(bf16[256,1024]{1,0:T(8,128)(2,1)S(1)} %collective-permute-done.10.refs_0_, bf16[2048,896]{1,0:T(8,128)(2,1)S(1)} %get-tuple-element.67.refs_1_.refs_2_, bf16[2048,896]{1,0:T(8,128)(2,1)S(1)} %get-tuple-element.68.refs_2_.refs_3_, bf16[896,2048]{1,0:T(8,128)(2,1)S(1)} %get-tuple-element.69.refs_3_.refs_4_, ...), custom_call_target="tpu_custom_call" | custom-call | flops 2818572288 | tf_op jit(solution)/shard_map/experts/pallas_call | solution.py:332
  99.5 3.3 %collective-permute-start.15 = (bf16[256,1024]{1,0:T(8,128)(2,1)S(1)}, bf16[256,1024]{1,0:T(8,128)(2,1)S(1)}, u32[]{:S(2)}, u32[]{:S(2)}) collective-permute-start(bf16[256,1024]{1,0:T(8,128)(2,1)S(1)} %experts.5), channel_id=1, source_target_pairs={{0,2},{1,3},{2,4},{3,5},{4,6},{5,7},{6,0},{7,1},{8,10},{9,11},{10,... | collective-permute-start | bytes 1572872 | tf_op jit(solution)/shard_map/ppermute | solution.py:473
  102.8 9.5 %collective-permute-done.13.refs_1_ = bf16[128,1024]{1,0:T(8,128)(2,1)S(1)} collective-permute-done((bf16[128,1024]{1,0:T(8,128)(2,1)S(1)}, bf16[128,1024]{1,0:T(8,128)(2,1)S(1)}, u32[]{:S(2)}, u32[]{:S(2)}) %collective-permute-start.13) | collective-permute-done | bytes 262176 | tf_op jit(solution)/shard_map/ppermute | solution.py:467
  112.3 4.2 %experts.6 = (bf16[128,1024]{1,0:T(8,128)(2,1)S(1)}, bf16[128,1024]{1,0:T(8,128)(2,1)S(1)}) custom-call(bf16[128,1024]{1,0:T(8,128)(2,1)S(1)} %collective-permute-done.12.refs_0_, bf16[128,1024]{1,0:T(8,128)(2,1)S(1)} %collective-permute-done.13.refs_1_, bf16[2048,896]{1,0:T(8,128)(2,1)S(1)} %get-tuple-element.67.refs_1_.refs_2_, ...), custom_call_target="tpu_custom_call" | custom-call | flops 2818572288 | tf_op jit(solution)/shard_map/experts/pallas_call | solution.py:332
  116.5 0.6 collective-permute-start.16
  117.2 3.0 %collective-permute-start.17 = (bf16[128,1024]{1,0:T(8,128)(2,1)S(1)}, bf16[128,1024]{1,0:T(8,128)(2,1)S(1)}, u32[]{:S(2)}, u32[]{:S(2)}) collective-permute-start(bf16[128,1024]{1,0:T(8,128)(2,1)S(1)} %get-tuple-element.77), channel_id=1, source_target_pairs={{0,4},{1,5},{2,6},{3,7},{4,0},{5,1},{6,2},{7,3},{8,12},{9,13},{10,... | collective-permute-start | bytes 786440 | tf_op jit(solution)/shard_map/ppermute | solution.py:476
  120.1 4.2 %experts.7 = bf16[256,1024]{1,0:T(8,128)(2,1)S(1)} custom-call(bf16[256,1024]{1,0:T(8,128)(2,1)S(1)} %bitcast.38, bf16[2048,896]{1,0:T(8,128)(2,1)S(1)} %get-tuple-element.67.refs_1_.refs_2_, bf16[2048,896]{1,0:T(8,128)(2,1)S(1)} %get-tuple-element.68.refs_2_.refs_3_, bf16[896,2048]{1,0:T(8,128)(2,1)S(1)} %get-tuple-element.69.refs_3_.refs_4_, ...), custom_call_target="tpu_custom_call" | custom-call | flops 2818572288 | tf_op jit(solution)/shard_map/experts/pallas_call | solution.py:332
  124.6 2.7 %collective-permute-done.16 = bf16[128,1024]{1,0:T(8,128)(2,1)S(1)} collective-permute-done((bf16[128,1024]{1,0:T(8,128)(2,1)S(1)}, bf16[128,1024]{1,0:T(8,128)(2,1)S(1)}, u32[]{:S(2)}, u32[]{:S(2)}) %collective-permute-start.16) | collective-permute-done | bytes 262176 | tf_op jit(solution)/shard_map/ppermute | solution.py:476
  127.3 3.4 %collective-permute-done.17 = bf16[128,1024]{1,0:T(8,128)(2,1)S(1)} collective-permute-done((bf16[128,1024]{1,0:T(8,128)(2,1)S(1)}, bf16[128,1024]{1,0:T(8,128)(2,1)S(1)}, u32[]{:S(2)}, u32[]{:S(2)}) %collective-permute-start.17) | collective-permute-done | bytes 262176 | tf_op jit(solution)/shard_map/ppermute | solution.py:476
  130.8 20.6 %all_to_all.21 = bf16[32,8,1024]{2,1,0:T(8,128)(2,1)S(1)} all-to-all(bf16[32,8,1024]{2,1,0:T(8,128)(2,1)S(1)} %fusion), channel_id=1, replica_groups=mesh['sp'=32,'tp'=8] {'sp'}, dimensions={0} | all-to-all | bytes 1048576 | tf_op jit(solution)/shard_map/all_to_all | solution.py:449
  151.7 0.7 fusion.3
  (53 shorter events, 3.5 us)
Async XLA Ops:
  0.0 47.2 %copy-start = (bf16[128,2048]{1,0:T(8,128)(2,1)S(1)}, bf16[128,2048]{1,0:T(8,128)(2,1)}, u32[]{:S(2)}) copy-start(bf16[128,2048]{1,0:T(8,128)(2,1)} %refs_0_.1) | copy-start | bytes 1572868
  0.0 47.2 %copy-start.2 = (f32[2048]{0:T(1024)S(1)}, f32[2048]{0:T(1024)}, u32[]{:S(2)}) copy-start(f32[2048]{0:T(1024)} %param.26) | copy-start | bytes 24580
  0.0 47.2 %copy-start.1 = (bf16[32,2048]{1,0:T(8,128)(2,1)S(1)}, bf16[32,2048]{1,0:T(8,128)(2,1)}, u32[]{:S(2)}) copy-start(bf16[32,2048]{1,0:T(8,128)(2,1)} %stream_ref.1) | copy-start | bytes 393220
  0.0 72.2 %collective-permute-start.7 = (bf16[2048,896]{1,0:T(8,128)(2,1)}, bf16[2048,896]{1,0:T(8,128)(2,1)}, u32[]{:S(2)}, u32[]{:S(2)}) collective-permute-start(bf16[2048,896]{1,0:T(8,128)(2,1)} %bitcast.49), channel_id=1, source_target_pairs={{0,1},{1,0},{2,3},{3,2},{4,5},{5,4},{6,7},{7,6},{8,9},{9,8},{10,11... | collective-permute-start | bytes 11010056 | tf_op jit(solution)/shard_map/ppermute | solution.py:518
  0.1 72.1 %collective-permute-start.8 = (bf16[896,2048]{1,0:T(8,128)(2,1)}, bf16[896,2048]{1,0:T(8,128)(2,1)}, u32[]{:S(2)}, u32[]{:S(2)}) collective-permute-start(bf16[896,2048]{1,0:T(8,128)(2,1)} %bitcast.51), channel_id=1, source_target_pairs={{0,1},{1,0},{2,3},{3,2},{4,5},{5,4},{6,7},{7,6},{8,9},{9,8},{10,11... | collective-permute-start | bytes 11010056 | tf_op jit(solution)/shard_map/ppermute | solution.py:517
  0.6 24.9 %collective-permute-start = (bf16[128,2048]{1,0:T(8,128)(2,1)}, bf16[128,2048]{1,0:T(8,128)(2,1)S(1)}, u32[]{:S(2)}, u32[]{:S(2)}) collective-permute-start(bf16[128,2048]{1,0:T(8,128)(2,1)} %refs_0_.1), channel_id=1, source_target_pairs={{0,2},{1,3},{2,4},{3,5},{4,6},{5,7},{6,0},{7,1},{8,10},{9,11},{10,... | collective-permute-start | bytes 1572872 | tf_op jit(solution)/shard_map/ppermute | solution.py:392
  2.4 23.2 %collective-permute-start.1 = (bf16[128,2048]{1,0:T(8,128)(2,1)}, bf16[128,2048]{1,0:T(8,128)(2,1)S(1)}, u32[]{:S(2)}, u32[]{:S(2)}) collective-permute-start(bf16[128,2048]{1,0:T(8,128)(2,1)} %refs_0_.1), channel_id=1, source_target_pairs={{0,4},{1,5},{2,6},{3,7},{4,0},{5,1},{6,2},{7,3},{8,12},{9,13},{10,... | collective-permute-start | bytes 1572872 | tf_op jit(solution)/shard_map/ppermute | solution.py:392
  3.4 25.6 %collective-permute-start.2 = (bf16[128,2048]{1,0:T(8,128)(2,1)}, bf16[128,2048]{1,0:T(8,128)(2,1)S(1)}, u32[]{:S(2)}, u32[]{:S(2)}) collective-permute-start(bf16[128,2048]{1,0:T(8,128)(2,1)} %refs_0_.1), channel_id=1, source_target_pairs={{0,6},{1,7},{2,0},{3,1},{4,2},{5,3},{6,4},{7,5},{8,14},{9,15},{10,... | collective-permute-start | bytes 1572872 | tf_op jit(solution)/shard_map/ppermute | solution.py:392
  8.8 23.8 %all-to-all-start = ((f32[32,4,512]{2,1,0:T(4,128)}), f32[32,4,512]{2,1,0:T(4,128)}, u32[]{:S(2)}, u32[]{:S(2)}) async-start(f32[32,4,512]{2,1,0:T(4,128)} %get-tuple-element.42), calls=%async_computation | async-start | bytes 524288 | tf_op jit(solution)/shard_map/all_to_all | solution.py:528
  25.5 3.7 %collective-permute-start.3 = (bf16[128,2048]{1,0:T(8,128)(2,1)}, bf16[128,2048]{1,0:T(8,128)(2,1)S(1)}, u32[]{:S(2)}, u32[]{:S(2)}) collective-permute-start(bf16[128,2048]{1,0:T(8,128)(2,1)} %refs_0_.1), channel_id=1, source_target_pairs={{0,1},{1,0},{2,3},{3,2},{4,5},{5,4},{6,7},{7,6},{8,9},{9,8},{10,11... | collective-permute-start | bytes 1572872 | tf_op jit(solution)/shard_map/ppermute | solution.py:394
  25.7 21.5 %collective-permute-start.4 = (bf16[128,2048]{1,0:T(8,128)(2,1)S(1)}, bf16[128,2048]{1,0:T(8,128)(2,1)S(1)}, u32[]{:S(2)}, u32[]{:S(2)}) collective-permute-start(bf16[128,2048]{1,0:T(8,128)(2,1)S(1)} %collective-permute-done.refs_1_), channel_id=1, source_target_pairs={{0,1},{1,0},{2,3},{3,2},{4,5},{5,4},{6,7},{7,6},{8,9},{9,8},{10,11... | collective-permute-start | bytes 1572872 | tf_op jit(solution)/shard_map/ppermute | solution.py:394
  29.0 18.1 %collective-permute-start.5 = (bf16[128,2048]{1,0:T(8,128)(2,1)S(1)}, bf16[128,2048]{1,0:T(8,128)(2,1)}, u32[]{:S(2)}, u32[]{:S(2)}) collective-permute-start(bf16[128,2048]{1,0:T(8,128)(2,1)S(1)} %collective-permute-done.1.refs_2_), channel_id=1, source_target_pairs={{0,1},{1,0},{2,3},{3,2},{4,5},{5,4},{6,7},{7,6},{8,9},{9,8},{10,11... | collective-permute-start | bytes 1572872 | tf_op jit(solution)/shard_map/ppermute | solution.py:394
  29.2 18.0 %collective-permute-start.6 = (bf16[128,2048]{1,0:T(8,128)(2,1)S(1)}, bf16[128,2048]{1,0:T(8,128)(2,1)}, u32[]{:S(2)}, u32[]{:S(2)}) collective-permute-start(bf16[128,2048]{1,0:T(8,128)(2,1)S(1)} %collective-permute-done.2.refs_3_), channel_id=1, source_target_pairs={{0,1},{1,0},{2,3},{3,2},{4,5},{5,4},{6,7},{7,6},{8,9},{9,8},{10,11... | collective-permute-start | bytes 1572872 | tf_op jit(solution)/shard_map/ppermute | solution.py:394
  37.2 10.0 %all-to-all-start.1 = ((bf16[8,32,128]{2,1,0:T(8,128)(2,1)}), bf16[8,32,128]{2,1,0:T(8,128)(2,1)S(1)}, u32[]{:S(2)}, u32[]{:S(2)}) async-start(bf16[8,32,128]{2,1,0:T(8,128)(2,1)} %bitcast.41), calls=%async_computation.1 | async-start | bytes 131072 | tf_op jit(solution)/shard_map/all_to_all | solution.py:429
  72.2 15.6 %collective-permute-start.11 = (bf16[2048,896]{1,0:T(8,128)(2,1)}, bf16[2048,896]{1,0:T(8,128)(2,1)S(1)}, u32[]{:S(2)}, u32[]{:S(2)}) collective-permute-start(bf16[2048,896]{1,0:T(8,128)(2,1)} %bitcast.16.refs_0_), channel_id=1, source_target_pairs={{0,1},{1,0},{2,3},{3,2},{4,5},{5,4},{6,7},{7,6},{8,9},{9,8},{10,11... | collective-permute-start | bytes 11010056 | tf_op jit(solution)/shard_map/ppermute | solution.py:460
  72.2 15.5 %collective-permute-start.10 = (bf16[256,1024]{1,0:T(8,128)(2,1)S(1)}, bf16[256,1024]{1,0:T(8,128)(2,1)S(1)}, u32[]{:S(2)}, u32[]{:S(2)}) collective-permute-start(bf16[256,1024]{1,0:T(8,128)(2,1)S(1)} %bitcast.36), channel_id=1, source_target_pairs={{0,6},{1,7},{2,0},{3,1},{4,2},{5,3},{6,4},{7,5},{8,14},{9,15},{10,... | collective-permute-start | bytes 1572872 | tf_op jit(solution)/shard_map/ppermute | solution.py:459
  72.7 15.1 %collective-permute-start.9 = (bf16[256,1024]{1,0:T(8,128)(2,1)S(1)}, bf16[256,1024]{1,0:T(8,128)(2,1)S(1)}, u32[]{:S(2)}, u32[]{:S(2)}) collective-permute-start(bf16[256,1024]{1,0:T(8,128)(2,1)S(1)} %bitcast.37), channel_id=1, source_target_pairs={{0,2},{1,3},{2,4},{3,5},{4,6},{5,7},{6,0},{7,1},{8,10},{9,11},{10,... | collective-permute-start | bytes 1572872 | tf_op jit(solution)/shard_map/ppermute | solution.py:458
  92.0 32.3 %collective-permute-start.14 = (bf16[256,1024]{1,0:T(8,128)(2,1)S(1)}, bf16[256,1024]{1,0:T(8,128)(2,1)S(1)}, u32[]{:S(2)}, u32[]{:S(2)}) collective-permute-start(bf16[256,1024]{1,0:T(8,128)(2,1)S(1)} %experts.4), channel_id=1, source_target_pairs={{0,6},{1,7},{2,0},{3,1},{4,2},{5,3},{6,4},{7,5},{8,14},{9,15},{10,... | collective-permute-start | bytes 1572872 | tf_op jit(solution)/shard_map/ppermute | solution.py:470
  92.6 10.2 %collective-permute-start.12 = (bf16[128,1024]{1,0:T(8,128)(2,1)S(1)}, bf16[128,1024]{1,0:T(8,128)(2,1)S(1)}, u32[]{:S(2)}, u32[]{:S(2)}) collective-permute-start(bf16[128,1024]{1,0:T(8,128)(2,1)S(1)} %slice.28), channel_id=1, source_target_pairs={{0,2},{1,3},{2,4},{3,5},{4,6},{5,7},{6,0},{7,1},{8,10},{9,11},{10,... | collective-permute-start | bytes 786440 | tf_op jit(solution)/shard_map/ppermute | solution.py:466
  95.3 17.0 %collective-permute-start.13 = (bf16[128,1024]{1,0:T(8,128)(2,1)S(1)}, bf16[128,1024]{1,0:T(8,128)(2,1)S(1)}, u32[]{:S(2)}, u32[]{:S(2)}) collective-permute-start(bf16[128,1024]{1,0:T(8,128)(2,1)S(1)} %slice.29), channel_id=1, source_target_pairs={{0,6},{1,7},{2,0},{3,1},{4,2},{5,3},{6,4},{7,5},{8,14},{9,15},{10,... | collective-permute-start | bytes 786440 | tf_op jit(solution)/shard_map/ppermute | solution.py:467
  99.5 24.8 %collective-permute-start.15 = (bf16[256,1024]{1,0:T(8,128)(2,1)S(1)}, bf16[256,1024]{1,0:T(8,128)(2,1)S(1)}, u32[]{:S(2)}, u32[]{:S(2)}) collective-permute-start(bf16[256,1024]{1,0:T(8,128)(2,1)S(1)} %experts.5), channel_id=1, source_target_pairs={{0,2},{1,3},{2,4},{3,5},{4,6},{5,7},{6,0},{7,1},{8,10},{9,11},{10,... | collective-permute-start | bytes 1572872 | tf_op jit(solution)/shard_map/ppermute | solution.py:473
  116.5 10.8 %collective-permute-start.16 = (bf16[128,1024]{1,0:T(8,128)(2,1)S(1)}, bf16[128,1024]{1,0:T(8,128)(2,1)S(1)}, u32[]{:S(2)}, u32[]{:S(2)}) collective-permute-start(bf16[128,1024]{1,0:T(8,128)(2,1)S(1)} %get-tuple-element.76), channel_id=1, source_target_pairs={{0,4},{1,5},{2,6},{3,7},{4,0},{5,1},{6,2},{7,3},{8,12},{9,13},{10,... | collective-permute-start | bytes 786440 | tf_op jit(solution)/shard_map/ppermute | solution.py:476
  117.2 13.5 %collective-permute-start.17 = (bf16[128,1024]{1,0:T(8,128)(2,1)S(1)}, bf16[128,1024]{1,0:T(8,128)(2,1)S(1)}, u32[]{:S(2)}, u32[]{:S(2)}) collective-permute-start(bf16[128,1024]{1,0:T(8,128)(2,1)S(1)} %get-tuple-element.77), channel_id=1, source_target_pairs={{0,4},{1,5},{2,6},{3,7},{4,0},{5,1},{6,2},{7,3},{8,12},{9,13},{10,... | collective-permute-start | bytes 786440 | tf_op jit(solution)/shard_map/ppermute | solution.py:476

commit v3 on v2

--- a/solution.py
+++ b/solution.py
@@ -26,6 +26,20 @@
     return lax.dot_general(
         left, right, (contract, ((), ())), precision=EXACT, preferred_element_type=jnp.float32
     )
+
+
+def whole_dot(left, right, transposed=False):
+    contract = (((1,), (1 if transposed else 0,)), ((), ()))
+    plain = left if left.dtype == jnp.bfloat16 else right
+    rest = right if left.dtype == jnp.bfloat16 else left
+    total = None
+    for _ in range(3):
+        part = rest.astype(jnp.bfloat16)
+        rest = rest - part.astype(jnp.float32)
+        pair = (plain, part) if plain is left else (part, plain)
+        term = lax.dot_general(*pair, contract, preferred_element_type=jnp.float32)
+        total = term if total is None else total + term
+    return total
 
 
 def complex_times(a_real, a_imag, b_real, b_imag):
@@ -68,15 +82,15 @@
     width = groups * states
     channels = map_ref.shape[1] // groups
     length = rows // LANES
-    spread = one_hot((states, width), lambda r, c: c % states == r)
+    spread = one_hot((states, width), lambda r, c: c % states == r).astype(jnp.bfloat16)
     group_of = one_hot((groups, width), lambda r, c: c // states == r)
 
     def in_a_row(ref):
-        return jnp.sum(exact_dot(ref[...], spread) * group_of, axis=0, keepdims=True)
+        return jnp.sum(whole_dot(ref[...], spread) * group_of, axis=0, keepdims=True)
 
     pole_real, pole_imag = in_a_row(pole_real_ref), in_a_row(pole_imag_ref)
     logs = jnp.broadcast_to(log_step_ref[...], (groups, groups))
-    step = jnp.exp(exact_dot(logs, group_of)[:1])
+    step = jnp.exp(whole_dot(logs, group_of.astype(jnp.bfloat16))[:1])
     magnitude = jnp.exp(pole_real * step)
     factor_real = magnitude * jnp.cos(pole_imag * step)
     factor_imag = magnitude * jnp.sin(pole_imag * step)
@@ -87,15 +101,17 @@
     factor_ref[1:2, :] = factor_imag
 
     order = one_hot((rows, rows), lambda r, c: c == (r % LANES) * length + r // LANES)
-    inputs = jnp.dot(
-        order.astype(jnp.bfloat16), input_ref[...], preferred_element_type=jnp.float32
-    )
-    scale_ref[...] = exact_dot(exact_dot(order, jnp.exp(shift_ref[...]), True), group_of)
+    order = order.astype(jnp.bfloat16)
+    inputs = jnp.dot(order, input_ref[...], preferred_element_type=jnp.float32)
+    inputs = inputs.astype(jnp.bfloat16)
+    scale_ref[...] = whole_dot(
+        whole_dot(order, jnp.exp(shift_ref[...]), True), group_of.astype(jnp.bfloat16)
+    )
     same_group = one_hot(
         (groups * channels, width), lambda r, c: r // channels == c // states
     )
-    plain_real = exact_dot(inputs, exact_dot(map_ref[0], spread) * same_group)
-    plain_imag = exact_dot(inputs, exact_dot(map_ref[1], spread) * same_group)
+    plain_real = whole_dot(inputs, whole_dot(map_ref[0], spread) * same_group)
+    plain_imag = whole_dot(inputs, whole_dot(map_ref[1], spread) * same_group)
     drive_real, drive_imag = complex_times(ratio_real, ratio_imag, plain_real, plain_imag)
     drive_real_ref[...] = drive_real
     drive_imag_ref[...] = drive_imag
@@ -117,7 +133,7 @@
         return through_real, through_imag, state_real, state_imag
 
     through_real, through_imag, state_real, state_imag = lax.fori_loop(
-        0, length, advance, (through_real, through_imag, state_real, state_imag), unroll=8
+        0, length, advance, (through_real, through_imag, state_real, state_imag), unroll=4
     )
 
     place = lax.broadcasted_iota(jnp.int32, (LANES, width), 0)
@@ -143,78 +159,78 @@
     total_ref[...] = jnp.broadcast_to(total[None], total_ref.shape)
 
 
-def response_kernel(here_ref, *refs):
-    sources, (out_ref, state_ref), targets, semaphores = (
-        refs[:9],
-        refs[9:11],
-        refs[11:20],
-        refs[20],
-    )
-    copies = [
-        pltpu.make_async_copy(source, target, semaphores.at[number])
-        for number, (source, target) in enumerate(zip(sources, targets))
-    ]
-    for copy in copies:
-        copy.start()
-    (
-        arrived_ref,
-        drive_real_ref,
-        drive_imag_ref,
-        scale_ref,
-        factor_ref,
-        enter_ref,
-        input_ref,
-        readout_ref,
-        skip_ref,
-    ) = targets
-    copies[0].wait()
+def alone_kernel(
+    drive_real_ref,
+    drive_imag_ref,
+    scale_ref,
+    factor_ref,
+    enter_ref,
+    input_ref,
+    readout_ref,
+    skip_ref,
+    alone_ref,
+    through_ref,
+    matrix_ref,
+    state_ref,
+    product_ref,
+):
     rows = input_ref.shape[0]
     width = factor_ref.shape[1]
     states = readout_ref.shape[2]
     channels = readout_ref.shape[1] * states // width
     length = rows // LANES
-    here = here_ref[0]
-    carry_real = carry_imag = jnp.zeros((1, width), jnp.float32)
-    for j in range(arrived_ref.shape[0]):
-        block = arrived_ref[j]
-        real, imag = complex_times(block[0:1], block[1:2], carry_real, carry_imag)
-        earlier = j < here
-        carry_real = jnp.where(earlier, real + block[2:3], carry_real)
-        carry_imag = jnp.where(earlier, imag + block[3:4], carry_imag)
-    for copy in copies[1:]:
-        copy.wait()
-    state_real, state_imag = complex_times(enter_ref[0], enter_ref[1], carry_real, carry_imag)
-    state_real, state_imag = state_real + enter_ref[2], state_imag + enter_ref[3]
     wide_real = jnp.broadcast_to(factor_ref[0:1, :], (LANES, width))
     wide_imag = jnp.broadcast_to(factor_ref[1:2, :], (LANES, width))
 
     def advance(k, held):
-        state_real, state_imag = held
+        through_real, through_imag, state_real, state_imag = held
         at = pl.ds(pl.multiple_of(k * LANES, LANES), LANES)
         scale = scale_ref[at, :]
         real, imag = scale * wide_real, scale * wide_imag
+        through_real, through_imag = complex_times(real, imag, through_real, through_imag)
         state_real, state_imag = complex_times(real, imag, state_real, state_imag)
         state_real = state_real + drive_real_ref[at, :]
         state_imag = state_imag + drive_imag_ref[at, :]
+        product_ref[at, :width] = through_real
+        product_ref[at, width:] = through_imag
         state_ref[at, :width] = state_real
         state_ref[at, width:] = state_imag
-        return state_real, state_imag
-
-    lax.fori_loop(0, length, advance, (state_real, state_imag), unroll=8)
-    spread = one_hot((states, width), lambda r, c: c % states == r)
+        return through_real, through_imag, state_real, state_imag
+
+    lax.fori_loop(0, length, advance, tuple(enter_ref[i] for i in range(4)), unroll=4)
+    spread = one_hot((states, width), lambda r, c: c % states == r).astype(jnp.bfloat16)
     same_group = one_hot(
         (readout_ref.shape[1], width), lambda r, c: r // channels == c // states
     )
-    matrix = jnp.concatenate(
-        [
-            exact_dot(readout_ref[0], spread) * same_group,
-            exact_dot(readout_ref[1], spread) * -same_group,
-        ],
-        axis=1,
-    )
-    response = exact_dot(state_ref[...], matrix, True)
+    matrix_ref[:, :width] = whole_dot(readout_ref[0], spread) * same_group
+    matrix_ref[:, width:] = whole_dot(readout_ref[1], spread) * -same_group
+    response = exact_dot(state_ref[...], matrix_ref[...], True)
     order = one_hot((rows, rows), lambda r, c: r == (c % LANES) * length + c // LANES)
-    response = exact_dot(order, response) + skip_ref[...] * input_ref[...].astype(jnp.float32)
+    alone_ref[...] = whole_dot(order.astype(jnp.bfloat16), response) + skip_ref[...] * input_ref[...].astype(
+        jnp.float32
+    )
+    through_ref[...] = whole_dot(order.astype(jnp.bfloat16), product_ref[...])
+
+
+def response_kernel(here_ref, arrived_ref, alone_ref, through_ref, matrix_ref, out_ref):
+    width = arrived_ref.shape[2]
+    here = here_ref[0]
+
+    def pass_on(j, carry):
+        block = arrived_ref[j]
+        real, imag = complex_times(block[0:1], block[1:2], *carry)
+        earlier = j < here
+        return (
+            jnp.where(earlier, real + block[2:3], carry[0]),
+            jnp.where(earlier, imag + block[3:4], carry[1]),
+        )
+
+    zero = jnp.zeros((1, width), jnp.float32)
+    carry = lax.fori_loop(0, arrived_ref.shape[0], pass_on, (zero, zero), unroll=8)
+    extra = jnp.concatenate(
+        complex_times(through_ref[:, :width], through_ref[:, width:], *carry), axis=1
+    )
+    response = alone_ref[...] + exact_dot(extra, matrix_ref[...], True)
     out_ref[...] = jax.nn.gelu(response).astype(jnp.bfloat16)
 
 
@@ -252,27 +268,33 @@
     )(*operands)
 
 
-def activations(here, arrived, kept, mixer_input, readout_matrix, skip):
+def response_alone(kept, mixer_input, readout_matrix, skip):
     rows, channels = mixer_input.shape
-    width = arrived.shape[2]
-    operands = (
-        arrived,
-        *kept,
-        mixer_input,
-        readout_matrix.reshape(2, channels, -1),
-        skip[None],
-    )
+    width = kept[0].shape[1]
+    shape = jax.ShapeDtypeStruct
+    wide = pltpu.VMEM((rows, 2 * width), jnp.float32)
+    return pl.pallas_call(
+        alone_kernel,
+        out_shape=(
+            shape((rows, channels), jnp.float32),
+            shape((rows, 2 * width), jnp.float32),
+            shape((channels, 2 * width), jnp.float32),
+        ),
+        scratch_shapes=[wide, wide],
+        compiler_params=pltpu.CompilerParams(vmem_limit_bytes=16 << 20),
+        name="alone",
+    )(*kept, mixer_input, readout_matrix.reshape(2, channels, -1), skip[None])
+
+
+def activations(here, arrived, alone):
+    vmem = pl.BlockSpec(memory_space=pltpu.VMEM)
     return pl.pallas_call(
         response_kernel,
-        out_shape=jax.ShapeDtypeStruct((rows, channels), jnp.bfloat16),
-        in_specs=[pl.BlockSpec(memory_space=pltpu.SMEM)]
-        + [pl.BlockSpec(memory_space=pltpu.HBM)] * len(operands),
-        scratch_shapes=[pltpu.VMEM((rows, 2 * width), jnp.float32)]
-        + [pltpu.VMEM(operand.shape, operand.dtype) for operand in operands]
-        + [pltpu.SemaphoreType.DMA((len(operands),))],
-        compiler_params=pltpu.CompilerParams(vmem_limit_bytes=60 * 1024 * 1024),
+        out_shape=jax.ShapeDtypeStruct(alone[0].shape, jnp.bfloat16),
+        in_specs=[pl.BlockSpec(memory_space=pltpu.SMEM)] + [vmem] * 4,
+        compiler_params=pltpu.CompilerParams(vmem_limit_bytes=16 << 20),
         name="response",
-    )(here.reshape(1), *operands)
+    )(here.reshape(1), arrived, *alone)
 
 
 def experts_kernel(capacity, count, sets, *refs):
@@ -539,10 +561,9 @@
     width = 2 * experts * capacity
     places = half_places(slot_numbers(routes, experts, capacity), capacity)
     spread = spread_weights(places, weights, width)
-    ends, spread, places = lax.optimization_barrier((ends, spread, places))
-    activated = activations(
-        lax.axis_index("sp"), ends, kept, mixer_input, readout_matrix, skip
-    )
+    alone = response_alone(kept, mixer_input, readout_matrix, skip)
+    ends, spread, places, *alone = lax.optimization_barrier((ends, spread, places, *alone))
+    activated = activations(lax.axis_index("sp"), ends, alone)
     mixed, outgoing = mixed_and_outgoing(
         activated, blocks, stream, norm_gain, places, width
     )

time: 153 us -> 165 us (1.078)
  local copies, waits for them, and re-layouts: 1.4 us -> 11.2 us
  waiting for transfers between devices: 33.4 us -> 28.2 us
  blocking collectives: 43.3 us -> 47.7 us
  other arithmetic: 2.52 us -> 5.75 us
    unnamed x7 -> x33, local copies, waits for them, and re-layouts: 0.77 us -> 10.5 us
    all_to_all x2, blocking collectives: 43.3 us -> 47.7 us  [over_experts(): lax.all_to_all(blocks, 'sp', split_axis=0, concat_axis=0, tiled=True)]
    all_to_all x1, waiting for transfers between devices: 3.03 us -> 0.01 us  [shards(): ends = lax.all_to_all(totals, 'sp', split_axis=0, concat_axis=0, tiled=True)]
    pallas_call x1 -> x2, Pallas kernels: 4.53 us -> 5.11 us  [the longest x1 3.24 us: response_alone(): pl.pallas_call(alone_kernel, out_shape=(shape((rows, channels), jnp.float...]
  transfers between devices with their start and end apart: 20 -> 20, of which waited for: 8 -> 6; matrix products, arithmetic and copies ran while one was open for 2% -> 4% of each run, Pallas kernels for 20% -> 19%
where the time goes in v3:
time: 165 us; the launch traced here: 164 us
  blocking collectives  47.7 us (29%)
  starting transfers between devices  36.1 us (22%)
  Pallas kernels  35 us (21%)
  waiting for transfers between devices  28.2 us (17%)
  local copies, waits for them, and re-layouts  11.2 us (7%)
  other arithmetic  5.75 us (3%)
    all_to_all x2, blocking collectives, over_experts(): lax.all_to_all(blocks, 'sp', split_axis=0, concat_axis=0, tiled=True)  47.7 us
    pallas_call x4, Pallas kernels, partial_out(): pl.pallas_call(functools.partial(experts_kernel, capacity, count, sets),...  16.8 us
    all_to_all x1, starting transfers between devices, shards(): ends = lax.all_to_all(totals, 'sp', split_axis=0, concat_axis=0, tiled=True)  11.3 us
    unnamed x33, local copies, waits for them, and re-layouts  10.5 us
    ppermute x1, waiting for transfers between devices, expert_over_chips(): lax.ppermute(after[middle:], 'tp', chip_shift(-1))  9.48 us
    all_to_all x1, starting transfers between devices, mixed_and_outgoing(): lax.all_to_all(activated.reshape(size, tokens, -1), 'tp', split_axis=0, c...  6.84 us
    pallas_call x1, Pallas kernels, staged(): pl.pallas_call(stage_kernel, out_shape=[jax.ShapeDtypeStruct(array.shape,...  6.33 us
    ppermute x2, waiting for transfers between devices, expert_over_chips(): to_across = [lax.ppermute(part, 'tp', chip_shift(2)) for part in for_across]  6.04 us
  transfers between devices with their start and end apart: 20, of which 6 were waited for; matrix products, arithmetic and copies ran while one was open for 4% of the time, Pallas kernels for 19%

profile of v3, /device:TPU:24, one launch (start us, length us, event | category | flops | bytes accessed | tf_op | source)
XLA Modules:
  0.0 164.5 jit_solution(4834105018035648229)
XLA Ops:
  0.6 1.8 %collective-permute-start = (bf16[128,2048]{1,0:T(8,128)(2,1)}, bf16[128,2048]{1,0:T(8,128)(2,1)S(1)}, u32[]{:S(2)}, u32[]{:S(2)}) collective-permute-start(bf16[128,2048]{1,0:T(8,128)(2,1)} %refs_0_.1), channel_id=1, source_target_pairs={{0,2},{1,3},{2,4},{3,5},{4,6},{5,7},{6,0},{7,1},{8,10},{9,11},{10,... | collective-permute-start | bytes 1572872 | tf_op jit(solution)/shard_map/ppermute | solution.py:414
  2.4 1.0 collective-permute-start.1
  3.4 4.2 %states.1 = (f32[32,4,512]{2,1,0:T(4,128)}, f32[256,512]{1,0:T(8,128)}, f32[256,512]{1,0:T(8,128)}, f32[256,512]{1,0:T(8,128)}, f32[2,512]{1,0:T(2,128)}, /*index=5*/f32[4,8,512]{2,1,0:T(8,128)}) custom-call(bf16[256,128]{1,0:T(8,128)(2,1)} %input_ref.1, f32[8,256]{1,0:T(8,128)} %bitcast.44, f32[8,64]{1,0:T(8,128)} %pole_real_hbm.1, f32[8,64]{1,0:T(8,128)} %pole_imag_hbm.1, ...), custom_call_target="tpu_custom_call" | custom-call | tf_op jit(solution)/shard_map/states/pallas_call | solution.py:253
  7.6 11.3 %all-to-all-start = ((f32[32,4,512]{2,1,0:T(4,128)}), f32[32,4,512]{2,1,0:T(4,128)S(1)}, u32[]{:S(2)}, u32[]{:S(2)}) async-start(f32[32,4,512]{2,1,0:T(4,128)} %get-tuple-element.48), calls=%async_computation | async-start | bytes 524288 | tf_op jit(solution)/shard_map/all_to_all | solution.py:550
  21.4 4.1 %collective-permute-done.refs_1_ = bf16[128,2048]{1,0:T(8,128)(2,1)S(1)} collective-permute-done((bf16[128,2048]{1,0:T(8,128)(2,1)}, bf16[128,2048]{1,0:T(8,128)(2,1)S(1)}, u32[]{:S(2)}, u32[]{:S(2)}) %collective-permute-start) | collective-permute-done | bytes 524320 | tf_op jit(solution)/shard_map/ppermute | solution.py:414
  26.3 1.0 copy-done.3
  27.3 1.0 copy-done.4
  28.4 1.0 copy-done.5
  30.2 0.9 copy-done.10
  33.3 3.2 %alone.1 = (f32[256,128]{1,0:T(8,128)S(1)}, f32[256,1024]{1,0:T(8,128)S(1)}, f32[128,1024]{1,0:T(8,128)S(1)}) custom-call(f32[256,512]{1,0:T(8,128)S(1)} %copy-done.3, f32[256,512]{1,0:T(8,128)S(1)} %copy-done.4, f32[256,512]{1,0:T(8,128)S(1)} %copy-done.5, f32[2,512]{1,0:T(2,128)S(1)} %copy-done.13, f32[4,8,512]{2,1,0:T(8,128)S(1)} %copy-done.11, ...), custom_call_target="tpu_custom_call" | custom-call | tf_op jit(solution)/shard_map/alone/pallas_call | solution.py:276
  38.9 0.8 fusion.4
  40.4 1.0 copy-done.2
  41.4 0.9 copy-done.9
  42.3 1.9 %response.1 = bf16[256,128]{1,0:T(8,128)(2,1)} custom-call(s32[1]{0:T(128)} %bitcast.here_ref, f32[32,4,512]{2,1,0:T(4,128)S(1)} %all-to-all-done.arrived_ref, f32[256,128]{1,0:T(8,128)S(1)} %copy-done.9, f32[256,1024]{1,0:T(8,128)S(1)} %get-tuple-element.59.through_ref, f32[128,1024]{1,0:T(8,128)S(1)} %copy-done.2), custom_call_target="tpu_custom_call" | custom-call | tf_op jit(solution)/shard_map/response/pallas_call | solution.py:291
  44.2 6.8 %all-to-all-start.1 = ((bf16[8,32,128]{2,1,0:T(8,128)(2,1)}), bf16[8,32,128]{2,1,0:T(8,128)(2,1)S(1)}, u32[]{:S(2)}, u32[]{:S(2)}) async-start(bf16[8,32,128]{2,1,0:T(8,128)(2,1)} %bitcast.12), calls=%async_computation.1 | async-start | bytes 131072 | tf_op jit(solution)/shard_map/all_to_all | solution.py:451
  51.9 2.7 %all-to-all-done.1.arrived_ref = bf16[8,32,128]{2,1,0:T(8,128)(2,1)S(1)} async-done(((bf16[8,32,128]{2,1,0:T(8,128)(2,1)}), bf16[8,32,128]{2,1,0:T(8,128)(2,1)S(1)}, u32[]{:S(2)}, u32[]{:S(2)}) %all-to-all-start.1) | async-done | bytes 65568 | tf_op jit(solution)/shard_map/all_to_all | solution.py:451
  54.6 2.6 %mix.1 = (bf16[32,2048]{1,0:T(8,128)(2,1)S(1)}, bf16[256,1024]{1,0:T(8,128)(2,1)S(1)}) custom-call(s32[8]{0:T(128)S(1)} %pad_add_fusion.1.order_ref, bf16[8,32,128]{2,1,0:T(8,128)(2,1)S(1)} %all-to-all-done.1.arrived_ref, bf16[32,2048]{1,0:T(8,128)(2,1)S(1)} %copy-done.7, f32[1,2048]{1,0:T(1,128)S(1)} %bitcast.41, s32[64,2]{1,0:T(8,128)S(1)} %reshape.193.places_ref, ...), custom_call_target="tpu_custom_call" | custom-call | tf_op jit(solution)/shard_map/mix/pallas_call | solution.py:456
  57.2 27.1 %all_to_all.20 = bf16[32,8,1024]{2,1,0:T(8,128)(2,1)S(1)} all-to-all(bf16[32,8,1024]{2,1,0:T(8,128)(2,1)S(1)} %bitcast.39), channel_id=1, replica_groups=mesh['sp'=32,'tp'=8] {'sp'}, dimensions={0} | all-to-all | bytes 1048576 | tf_op jit(solution)/shard_map/all_to_all | solution.py:471
  84.8 2.8 %collective-permute-start.9 = (bf16[256,1024]{1,0:T(8,128)(2,1)S(1)}, bf16[256,1024]{1,0:T(8,128)(2,1)S(1)}, u32[]{:S(2)}, u32[]{:S(2)}) collective-permute-start(bf16[256,1024]{1,0:T(8,128)(2,1)S(1)} %bitcast.37), channel_id=1, source_target_pairs={{0,2},{1,3},{2,4},{3,5},{4,6},{5,7},{6,0},{7,1},{8,10},{9,11},{10,... | collective-permute-start | bytes 1572872 | tf_op jit(solution)/shard_map/ppermute | solution.py:480
  87.6 6.3 %stage.1 = (bf16[2048,896]{1,0:T(8,128)(2,1)S(1)}, bf16[2048,896]{1,0:T(8,128)(2,1)S(1)}, bf16[896,2048]{1,0:T(8,128)(2,1)S(1)}, bf16[2048,896]{1,0:T(8,128)(2,1)S(1)}, bf16[896,2048]{1,0:T(8,128)(2,1)S(1)}) custom-call(bf16[2048,896]{1,0:T(8,128)(2,1)} %bitcast.16.refs_0_, bf16[2048,896]{1,0:T(8,128)(2,1)} %bitcast.49, bf16[896,2048]{1,0:T(8,128)(2,1)} %bitcast.51, ...), custom_call_target="tpu_custom_call" | custom-call | flops 8589934592 | tf_op jit(solution)/shard_map/stage/pallas_call | solution.py:377
  94.0 5.9 %collective-permute-done.10.refs_0_ = bf16[256,1024]{1,0:T(8,128)(2,1)S(1)} collective-permute-done((bf16[256,1024]{1,0:T(8,128)(2,1)S(1)}, bf16[256,1024]{1,0:T(8,128)(2,1)S(1)}, u32[]{:S(2)}, u32[]{:S(2)}) %collective-permute-start.10) | collective-permute-done | bytes 524320 | tf_op jit(solution)/shard_map/ppermute | solution.py:481
  99.9 4.2 %experts.4 = bf16[256,1024]{1,0:T(8,128)(2,1)S(1)} custom-call(bf16[256,1024]{1,0:T(8,128)(2,1)S(1)} %collective-permute-done.9.refs_0_, bf16[2048,896]{1,0:T(8,128)(2,1)S(1)} %get-tuple-element.79.refs_1_.refs_2_, bf16[2048,896]{1,0:T(8,128)(2,1)S(1)} %get-tuple-element.80.refs_2_.refs_3_, bf16[896,2048]{1,0:T(8,128)(2,1)S(1)} %get-tuple-element.81.refs_3_.refs_4_, ...), custom_call_target="tpu_custom_call" | custom-call | flops 2818572288 | tf_op jit(solution)/shard_map/experts/pallas_call | solution.py:354
  104.7 2.7 %collective-permute-start.12 = (bf16[128,1024]{1,0:T(8,128)(2,1)S(1)}, bf16[128,1024]{1,0:T(8,128)(2,1)S(1)}, u32[]{:S(2)}, u32[]{:S(2)}) collective-permute-start(bf16[128,1024]{1,0:T(8,128)(2,1)S(1)} %slice.28), channel_id=1, source_target_pairs={{0,2},{1,3},{2,4},{3,5},{4,6},{5,7},{6,0},{7,1},{8,10},{9,11},{10,... | collective-permute-start | bytes 786440 | tf_op jit(solution)/shard_map/ppermute | solution.py:488
  107.4 4.2 %experts.5 = bf16[256,1024]{1,0:T(8,128)(2,1)S(1)} custom-call(bf16[256,1024]{1,0:T(8,128)(2,1)S(1)} %collective-permute-done.10.refs_0_, bf16[2048,896]{1,0:T(8,128)(2,1)S(1)} %get-tuple-element.79.refs_1_.refs_2_, bf16[2048,896]{1,0:T(8,128)(2,1)S(1)} %get-tuple-element.80.refs_2_.refs_3_, bf16[896,2048]{1,0:T(8,128)(2,1)S(1)} %get-tuple-element.81.refs_3_.refs_4_, ...), custom_call_target="tpu_custom_call" | custom-call | flops 2818572288 | tf_op jit(solution)/shard_map/experts/pallas_call | solution.py:354
  111.6 3.3 %collective-permute-start.15 = (bf16[256,1024]{1,0:T(8,128)(2,1)S(1)}, bf16[256,1024]{1,0:T(8,128)(2,1)S(1)}, u32[]{:S(2)}, u32[]{:S(2)}) collective-permute-start(bf16[256,1024]{1,0:T(8,128)(2,1)S(1)} %experts.5), channel_id=1, source_target_pairs={{0,2},{1,3},{2,4},{3,5},{4,6},{5,7},{6,0},{7,1},{8,10},{9,11},{10,... | collective-permute-start | bytes 1572872 | tf_op jit(solution)/shard_map/ppermute | solution.py:495
  114.9 9.5 %collective-permute-done.13.refs_1_ = bf16[128,1024]{1,0:T(8,128)(2,1)S(1)} collective-permute-done((bf16[128,1024]{1,0:T(8,128)(2,1)S(1)}, bf16[128,1024]{1,0:T(8,128)(2,1)S(1)}, u32[]{:S(2)}, u32[]{:S(2)}) %collective-permute-start.13) | collective-permute-done | bytes 262176 | tf_op jit(solution)/shard_map/ppermute | solution.py:489
  124.4 4.2 %experts.6 = (bf16[128,1024]{1,0:T(8,128)(2,1)S(1)}, bf16[128,1024]{1,0:T(8,128)(2,1)S(1)}) custom-call(bf16[128,1024]{1,0:T(8,128)(2,1)S(1)} %collective-permute-done.12.refs_0_, bf16[128,1024]{1,0:T(8,128)(2,1)S(1)} %collective-permute-done.13.refs_1_, bf16[2048,896]{1,0:T(8,128)(2,1)S(1)} %get-tuple-element.79.refs_1_.refs_2_, ...), custom_call_target="tpu_custom_call" | custom-call | flops 2818572288 | tf_op jit(solution)/shard_map/experts/pallas_call | solution.py:354
  129.3 3.0 %collective-permute-start.17 = (bf16[128,1024]{1,0:T(8,128)(2,1)S(1)}, bf16[128,1024]{1,0:T(8,128)(2,1)S(1)}, u32[]{:S(2)}, u32[]{:S(2)}) collective-permute-start(bf16[128,1024]{1,0:T(8,128)(2,1)S(1)} %get-tuple-element.89), channel_id=1, source_target_pairs={{0,4},{1,5},{2,6},{3,7},{4,0},{5,1},{6,2},{7,3},{8,12},{9,13},{10,... | collective-permute-start | bytes 786440 | tf_op jit(solution)/shard_map/ppermute | solution.py:498
  132.3 4.2 %experts.7 = bf16[256,1024]{1,0:T(8,128)(2,1)S(1)} custom-call(bf16[256,1024]{1,0:T(8,128)(2,1)S(1)} %bitcast.38, bf16[2048,896]{1,0:T(8,128)(2,1)S(1)} %get-tuple-element.79.refs_1_.refs_2_, bf16[2048,896]{1,0:T(8,128)(2,1)S(1)} %get-tuple-element.80.refs_2_.refs_3_, bf16[896,2048]{1,0:T(8,128)(2,1)S(1)} %get-tuple-element.81.refs_3_.refs_4_, ...), custom_call_target="tpu_custom_call" | custom-call | flops 2818572288 | tf_op jit(solution)/shard_map/experts/pallas_call | solution.py:354
  136.7 2.7 %collective-permute-done.16 = bf16[128,1024]{1,0:T(8,128)(2,1)S(1)} collective-permute-done((bf16[128,1024]{1,0:T(8,128)(2,1)S(1)}, bf16[128,1024]{1,0:T(8,128)(2,1)S(1)}, u32[]{:S(2)}, u32[]{:S(2)}) %collective-permute-start.16) | collective-permute-done | bytes 262176 | tf_op jit(solution)/shard_map/ppermute | solution.py:498
  139.4 3.4 %collective-permute-done.17 = bf16[128,1024]{1,0:T(8,128)(2,1)S(1)} collective-permute-done((bf16[128,1024]{1,0:T(8,128)(2,1)S(1)}, bf16[128,1024]{1,0:T(8,128)(2,1)S(1)}, u32[]{:S(2)}, u32[]{:S(2)}) %collective-permute-start.17) | collective-permute-done | bytes 262176 | tf_op jit(solution)/shard_map/ppermute | solution.py:498
  142.9 20.6 %all_to_all.21 = bf16[32,8,1024]{2,1,0:T(8,128)(2,1)S(1)} all-to-all(bf16[32,8,1024]{2,1,0:T(8,128)(2,1)S(1)} %fusion), channel_id=1, replica_groups=mesh['sp'=32,'tp'=8] {'sp'}, dimensions={0} | all-to-all | bytes 1048576 | tf_op jit(solution)/shard_map/all_to_all | solution.py:471
  (80 shorter events, 13.7 us)
Async XLA Ops:
  0.0 54.6 %copy-start = (bf16[128,2048]{1,0:T(8,128)(2,1)S(1)}, bf16[128,2048]{1,0:T(8,128)(2,1)}, u32[]{:S(2)}) copy-start(bf16[128,2048]{1,0:T(8,128)(2,1)} %refs_0_.1) | copy-start | bytes 1572868
  0.0 54.6 %copy-start.12 = (f32[2048]{0:T(1024)S(1)}, f32[2048]{0:T(1024)}, u32[]{:S(2)}) copy-start(f32[2048]{0:T(1024)} %param.26) | copy-start | bytes 24580
  0.0 54.6 %copy-start.7 = (bf16[32,2048]{1,0:T(8,128)(2,1)S(1)}, bf16[32,2048]{1,0:T(8,128)(2,1)}, u32[]{:S(2)}) copy-start(bf16[32,2048]{1,0:T(8,128)(2,1)} %stream_ref.1) | copy-start | bytes 393220
  0.0 84.3 %collective-permute-start.7 = (bf16[2048,896]{1,0:T(8,128)(2,1)}, bf16[2048,896]{1,0:T(8,128)(2,1)}, u32[]{:S(2)}, u32[]{:S(2)}) collective-permute-start(bf16[2048,896]{1,0:T(8,128)(2,1)} %bitcast.48), channel_id=1, source_target_pairs={{0,1},{1,0},{2,3},{3,2},{4,5},{5,4},{6,7},{7,6},{8,9},{9,8},{10,11... | collective-permute-start | bytes 11010056 | tf_op jit(solution)/shard_map/ppermute | solution.py:540
  0.1 84.2 %collective-permute-start.8 = (bf16[896,2048]{1,0:T(8,128)(2,1)}, bf16[896,2048]{1,0:T(8,128)(2,1)}, u32[]{:S(2)}, u32[]{:S(2)}) collective-permute-start(bf16[896,2048]{1,0:T(8,128)(2,1)} %bitcast.50), channel_id=1, source_target_pairs={{0,1},{1,0},{2,3},{3,2},{4,5},{5,4},{6,7},{7,6},{8,9},{9,8},{10,11... | collective-permute-start | bytes 11010056 | tf_op jit(solution)/shard_map/ppermute | solution.py:539
  0.6 24.9 %collective-permute-start = (bf16[128,2048]{1,0:T(8,128)(2,1)}, bf16[128,2048]{1,0:T(8,128)(2,1)S(1)}, u32[]{:S(2)}, u32[]{:S(2)}) collective-permute-start(bf16[128,2048]{1,0:T(8,128)(2,1)} %refs_0_.1), channel_id=1, source_target_pairs={{0,2},{1,3},{2,4},{3,5},{4,6},{5,7},{6,0},{7,1},{8,10},{9,11},{10,... | collective-permute-start | bytes 1572872 | tf_op jit(solution)/shard_map/ppermute | solution.py:414
  2.4 34.9 %collective-permute-start.1 = (bf16[128,2048]{1,0:T(8,128)(2,1)}, bf16[128,2048]{1,0:T(8,128)(2,1)S(1)}, u32[]{:S(2)}, u32[]{:S(2)}) collective-permute-start(bf16[128,2048]{1,0:T(8,128)(2,1)} %refs_0_.1), channel_id=1, source_target_pairs={{0,4},{1,5},{2,6},{3,7},{4,0},{5,1},{6,2},{7,3},{8,12},{9,13},{10,... | collective-permute-start | bytes 1572872 | tf_op jit(solution)/shard_map/ppermute | solution.py:414
  3.4 34.4 %collective-permute-start.2 = (bf16[128,2048]{1,0:T(8,128)(2,1)}, bf16[128,2048]{1,0:T(8,128)(2,1)S(1)}, u32[]{:S(2)}, u32[]{:S(2)}) collective-permute-start(bf16[128,2048]{1,0:T(8,128)(2,1)} %refs_0_.1), channel_id=1, source_target_pairs={{0,6},{1,7},{2,0},{3,1},{4,2},{5,3},{6,4},{7,5},{8,14},{9,15},{10,... | collective-permute-start | bytes 1572872 | tf_op jit(solution)/shard_map/ppermute | solution.py:414
  7.6 32.8 %all-to-all-start = ((f32[32,4,512]{2,1,0:T(4,128)}), f32[32,4,512]{2,1,0:T(4,128)S(1)}, u32[]{:S(2)}, u32[]{:S(2)}) async-start(f32[32,4,512]{2,1,0:T(4,128)} %get-tuple-element.48), calls=%async_computation | async-start | bytes 524288 | tf_op jit(solution)/shard_map/all_to_all | solution.py:550
  25.5 12.5 %collective-permute-start.3 = (bf16[128,2048]{1,0:T(8,128)(2,1)}, bf16[128,2048]{1,0:T(8,128)(2,1)}, u32[]{:S(2)}, u32[]{:S(2)}) collective-permute-start(bf16[128,2048]{1,0:T(8,128)(2,1)} %refs_0_.1), channel_id=1, source_target_pairs={{0,1},{1,0},{2,3},{3,2},{4,5},{5,4},{6,7},{7,6},{8,9},{9,8},{10,11... | collective-permute-start | bytes 1572872 | tf_op jit(solution)/shard_map/ppermute | solution.py:416
  26.3 1.0 copy-start.3
  27.3 1.0 copy-start.4
  28.4 1.0 copy-start.5
  29.4 0.8 copy-start.6
  30.2 0.9 copy-start.10
  37.3 2.4 %copy-start.8 = (f32[256,128]{1,0:T(8,128)}, f32[256,128]{1,0:T(8,128)S(1)}, u32[]{:S(2)}) copy-start(f32[256,128]{1,0:T(8,128)S(1)} %get-tuple-element.58.alone_ref) | copy-start | bytes 393220
  37.4 17.2 %collective-permute-start.4 = (bf16[128,2048]{1,0:T(8,128)(2,1)S(1)}, bf16[128,2048]{1,0:T(8,128)(2,1)}, u32[]{:S(2)}, u32[]{:S(2)}) collective-permute-start(bf16[128,2048]{1,0:T(8,128)(2,1)S(1)} %collective-permute-done.refs_1_), channel_id=1, source_target_pairs={{0,1},{1,0},{2,3},{3,2},{4,5},{5,4},{6,7},{7,6},{8,9},{9,8},{10,11... | collective-permute-start | bytes 1572872 | tf_op jit(solution)/shard_map/ppermute | solution.py:416
  37.9 16.7 %collective-permute-start.5 = (bf16[128,2048]{1,0:T(8,128)(2,1)S(1)}, bf16[128,2048]{1,0:T(8,128)(2,1)}, u32[]{:S(2)}, u32[]{:S(2)}) collective-permute-start(bf16[128,2048]{1,0:T(8,128)(2,1)S(1)} %collective-permute-done.1.refs_2_), channel_id=1, source_target_pairs={{0,1},{1,0},{2,3},{3,2},{4,5},{5,4},{6,7},{7,6},{8,9},{9,8},{10,11... | collective-permute-start | bytes 1572872 | tf_op jit(solution)/shard_map/ppermute | solution.py:416
  38.0 16.6 %collective-permute-start.6 = (bf16[128,2048]{1,0:T(8,128)(2,1)S(1)}, bf16[128,2048]{1,0:T(8,128)(2,1)}, u32[]{:S(2)}, u32[]{:S(2)}) collective-permute-start(bf16[128,2048]{1,0:T(8,128)(2,1)S(1)} %collective-permute-done.2.refs_3_), channel_id=1, source_target_pairs={{0,1},{1,0},{2,3},{3,2},{4,5},{5,4},{6,7},{7,6},{8,9},{9,8},{10,11... | collective-permute-start | bytes 1572872 | tf_op jit(solution)/shard_map/ppermute | solution.py:416
  40.4 1.0 copy-start.2
  41.4 0.9 copy-start.9
  44.2 10.4 %all-to-all-start.1 = ((bf16[8,32,128]{2,1,0:T(8,128)(2,1)}), bf16[8,32,128]{2,1,0:T(8,128)(2,1)S(1)}, u32[]{:S(2)}, u32[]{:S(2)}) async-start(bf16[8,32,128]{2,1,0:T(8,128)(2,1)} %bitcast.12), calls=%async_computation.1 | async-start | bytes 131072 | tf_op jit(solution)/shard_map/all_to_all | solution.py:451
  84.3 15.6 %collective-permute-start.11 = (bf16[2048,896]{1,0:T(8,128)(2,1)}, bf16[2048,896]{1,0:T(8,128)(2,1)S(1)}, u32[]{:S(2)}, u32[]{:S(2)}) collective-permute-start(bf16[2048,896]{1,0:T(8,128)(2,1)} %bitcast.16.refs_0_), channel_id=1, source_target_pairs={{0,1},{1,0},{2,3},{3,2},{4,5},{5,4},{6,7},{7,6},{8,9},{9,8},{10,11... | collective-permute-start | bytes 11010056 | tf_op jit(solution)/shard_map/ppermute | solution.py:482
  84.3 15.5 %collective-permute-start.10 = (bf16[256,1024]{1,0:T(8,128)(2,1)S(1)}, bf16[256,1024]{1,0:T(8,128)(2,1)S(1)}, u32[]{:S(2)}, u32[]{:S(2)}) collective-permute-start(bf16[256,1024]{1,0:T(8,128)(2,1)S(1)} %bitcast.36), channel_id=1, source_target_pairs={{0,6},{1,7},{2,0},{3,1},{4,2},{5,3},{6,4},{7,5},{8,14},{9,15},{10,... | collective-permute-start | bytes 1572872 | tf_op jit(solution)/shard_map/ppermute | solution.py:481
  84.8 15.1 %collective-permute-start.9 = (bf16[256,1024]{1,0:T(8,128)(2,1)S(1)}, bf16[256,1024]{1,0:T(8,128)(2,1)S(1)}, u32[]{:S(2)}, u32[]{:S(2)}) collective-permute-start(bf16[256,1024]{1,0:T(8,128)(2,1)S(1)} %bitcast.37), channel_id=1, source_target_pairs={{0,2},{1,3},{2,4},{3,5},{4,6},{5,7},{6,0},{7,1},{8,10},{9,11},{10,... | collective-permute-start | bytes 1572872 | tf_op jit(solution)/shard_map/ppermute | solution.py:480
  104.1 32.4 %collective-permute-start.14 = (bf16[256,1024]{1,0:T(8,128)(2,1)S(1)}, bf16[256,1024]{1,0:T(8,128)(2,1)S(1)}, u32[]{:S(2)}, u32[]{:S(2)}) collective-permute-start(bf16[256,1024]{1,0:T(8,128)(2,1)S(1)} %experts.4), channel_id=1, source_target_pairs={{0,6},{1,7},{2,0},{3,1},{4,2},{5,3},{6,4},{7,5},{8,14},{9,15},{10,... | collective-permute-start | bytes 1572872 | tf_op jit(solution)/shard_map/ppermute | solution.py:492
  104.7 10.2 %collective-permute-start.12 = (bf16[128,1024]{1,0:T(8,128)(2,1)S(1)}, bf16[128,1024]{1,0:T(8,128)(2,1)S(1)}, u32[]{:S(2)}, u32[]{:S(2)}) collective-permute-start(bf16[128,1024]{1,0:T(8,128)(2,1)S(1)} %slice.28), channel_id=1, source_target_pairs={{0,2},{1,3},{2,4},{3,5},{4,6},{5,7},{6,0},{7,1},{8,10},{9,11},{10,... | collective-permute-start | bytes 786440 | tf_op jit(solution)/shard_map/ppermute | solution.py:488
  107.4 17.0 %collective-permute-start.13 = (bf16[128,1024]{1,0:T(8,128)(2,1)S(1)}, bf16[128,1024]{1,0:T(8,128)(2,1)S(1)}, u32[]{:S(2)}, u32[]{:S(2)}) collective-permute-start(bf16[128,1024]{1,0:T(8,128)(2,1)S(1)} %slice.29), channel_id=1, source_target_pairs={{0,6},{1,7},{2,0},{3,1},{4,2},{5,3},{6,4},{7,5},{8,14},{9,15},{10,... | collective-permute-start | bytes 786440 | tf_op jit(solution)/shard_map/ppermute | solution.py:489
  111.6 24.8 %collective-permute-start.15 = (bf16[256,1024]{1,0:T(8,128)(2,1)S(1)}, bf16[256,1024]{1,0:T(8,128)(2,1)S(1)}, u32[]{:S(2)}, u32[]{:S(2)}) collective-permute-start(bf16[256,1024]{1,0:T(8,128)(2,1)S(1)} %experts.5), channel_id=1, source_target_pairs={{0,2},{1,3},{2,4},{3,5},{4,6},{5,7},{6,0},{7,1},{8,10},{9,11},{10,... | collective-permute-start | bytes 1572872 | tf_op jit(solution)/shard_map/ppermute | solution.py:495
  128.7 10.8 %collective-permute-start.16 = (bf16[128,1024]{1,0:T(8,128)(2,1)S(1)}, bf16[128,1024]{1,0:T(8,128)(2,1)S(1)}, u32[]{:S(2)}, u32[]{:S(2)}) collective-permute-start(bf16[128,1024]{1,0:T(8,128)(2,1)S(1)} %get-tuple-element.88), channel_id=1, source_target_pairs={{0,4},{1,5},{2,6},{3,7},{4,0},{5,1},{6,2},{7,3},{8,12},{9,13},{10,... | collective-permute-start | bytes 786440 | tf_op jit(solution)/shard_map/ppermute | solution.py:498
  129.3 13.5 %collective-permute-start.17 = (bf16[128,1024]{1,0:T(8,128)(2,1)S(1)}, bf16[128,1024]{1,0:T(8,128)(2,1)S(1)}, u32[]{:S(2)}, u32[]{:S(2)}) collective-permute-start(bf16[128,1024]{1,0:T(8,128)(2,1)S(1)} %get-tuple-element.89), channel_id=1, source_target_pairs={{0,4},{1,5},{2,6},{3,7},{4,0},{5,1},{6,2},{7,3},{8,12},{9,13},{10,... | collective-permute-start | bytes 786440 | tf_op jit(solution)/shard_map/ppermute | solution.py:498
  136.5 27.1 %copy-start.15 = (bf16[128,256]{1,0:T(8,128)(2,1)S(1)}, bf16[128,256]{1,0:T(8,128)(2,1)}, u32[]{:S(2)}) copy-start(bf16[128,256]{1,0:T(8,128)(2,1)} %pad_maximum_fusion) | copy-start | bytes 196612
  (4 other events, 3.0 us)

commit v4 on v2

--- a/solution.py
+++ b/solution.py
@@ -26,6 +26,20 @@
     return lax.dot_general(
         left, right, (contract, ((), ())), precision=EXACT, preferred_element_type=jnp.float32
     )
+
+
+def whole_dot(left, right, transposed=False):
+    contract = (((1,), (1 if transposed else 0,)), ((), ()))
+    plain = left if left.dtype == jnp.bfloat16 else right
+    rest = right if left.dtype == jnp.bfloat16 else left
+    total = None
+    for _ in range(3):
+        part = rest.astype(jnp.bfloat16)
+        rest = rest - part.astype(jnp.float32)
+        pair = (plain, part) if plain is left else (part, plain)
+        term = lax.dot_general(*pair, contract, preferred_element_type=jnp.float32)
+        total = term if total is None else total + term
+    return total
 
 
 def complex_times(a_real, a_imag, b_real, b_imag):
@@ -68,15 +82,15 @@
     width = groups * states
     channels = map_ref.shape[1] // groups
     length = rows // LANES
-    spread = one_hot((states, width), lambda r, c: c % states == r)
+    spread = one_hot((states, width), lambda r, c: c % states == r).astype(jnp.bfloat16)
     group_of = one_hot((groups, width), lambda r, c: c // states == r)
 
     def in_a_row(ref):
-        return jnp.sum(exact_dot(ref[...], spread) * group_of, axis=0, keepdims=True)
+        return jnp.sum(whole_dot(ref[...], spread) * group_of, axis=0, keepdims=True)
 
     pole_real, pole_imag = in_a_row(pole_real_ref), in_a_row(pole_imag_ref)
     logs = jnp.broadcast_to(log_step_ref[...], (groups, groups))
-    step = jnp.exp(exact_dot(logs, group_of)[:1])
+    step = jnp.exp(whole_dot(logs, group_of.astype(jnp.bfloat16))[:1])
     magnitude = jnp.exp(pole_real * step)
     factor_real = magnitude * jnp.cos(pole_imag * step)
     factor_imag = magnitude * jnp.sin(pole_imag * step)
@@ -87,15 +101,17 @@
     factor_ref[1:2, :] = factor_imag
 
     order = one_hot((rows, rows), lambda r, c: c == (r % LANES) * length + r // LANES)
-    inputs = jnp.dot(
-        order.astype(jnp.bfloat16), input_ref[...], preferred_element_type=jnp.float32
-    )
-    scale_ref[...] = exact_dot(exact_dot(order, jnp.exp(shift_ref[...]), True), group_of)
+    order = order.astype(jnp.bfloat16)
+    inputs = jnp.dot(order, input_ref[...], preferred_element_type=jnp.float32)
+    inputs = inputs.astype(jnp.bfloat16)
+    scale_ref[...] = whole_dot(
+        whole_dot(order, jnp.exp(shift_ref[...]), True), group_of.astype(jnp.bfloat16)
+    )
     same_group = one_hot(
         (groups * channels, width), lambda r, c: r // channels == c // states
     )
-    plain_real = exact_dot(inputs, exact_dot(map_ref[0], spread) * same_group)
-    plain_imag = exact_dot(inputs, exact_dot(map_ref[1], spread) * same_group)
+    plain_real = whole_dot(inputs, whole_dot(map_ref[0], spread) * same_group)
+    plain_imag = whole_dot(inputs, whole_dot(map_ref[1], spread) * same_group)
     drive_real, drive_imag = complex_times(ratio_real, ratio_imag, plain_real, plain_imag)
     drive_real_ref[...] = drive_real
     drive_imag_ref[...] = drive_imag
@@ -117,7 +133,7 @@
         return through_real, through_imag, state_real, state_imag
 
     through_real, through_imag, state_real, state_imag = lax.fori_loop(
-        0, length, advance, (through_real, through_imag, state_real, state_imag), unroll=8
+        0, length, advance, (through_real, through_imag, state_real, state_imag), unroll=4
     )
 
     place = lax.broadcasted_iota(jnp.int32, (LANES, width), 0)
@@ -201,20 +217,20 @@
         return state_real, state_imag
 
     lax.fori_loop(0, length, advance, (state_real, state_imag), unroll=8)
-    spread = one_hot((states, width), lambda r, c: c % states == r)
+    spread = one_hot((states, width), lambda r, c: c % states == r).astype(jnp.bfloat16)
     same_group = one_hot(
         (readout_ref.shape[1], width), lambda r, c: r // channels == c // states
     )
     matrix = jnp.concatenate(
         [
-            exact_dot(readout_ref[0], spread) * same_group,
-            exact_dot(readout_ref[1], spread) * -same_group,
+            whole_dot(readout_ref[0], spread) * same_group,
+            whole_dot(readout_ref[1], spread) * -same_group,
         ],
         axis=1,
     )
     response = exact_dot(state_ref[...], matrix, True)
     order = one_hot((rows, rows), lambda r, c: r == (c % LANES) * length + c // LANES)
-    response = exact_dot(order, response) + skip_ref[...] * input_ref[...].astype(jnp.float32)
+    response = whole_dot(order.astype(jnp.bfloat16), response) + skip_ref[...] * input_ref[...].astype(jnp.float32)
     out_ref[...] = jax.nn.gelu(response).astype(jnp.bfloat16)
 
 

time: 153 us -> 152 us (level)
  transfers between devices with their start and end apart: 20 -> 20, of which waited for: 8 -> 8; matrix products, arithmetic and copies ran while one was open for 2% -> 2% of each run, Pallas kernels for 20% -> 19%
where the time goes in v4:
time: 152 us; the launch traced here: 151 us
  blocking collectives  44.2 us (29%)
  starting transfers between devices  36.4 us (24%)
  Pallas kernels  33.7 us (22%)
  waiting for transfers between devices  32.6 us (21%)
  other arithmetic  2.52 us (2%)
    all_to_all x2, blocking collectives, over_experts(): lax.all_to_all(blocks, 'sp', split_axis=0, concat_axis=0, tiled=True)  44.2 us
    pallas_call x4, Pallas kernels, partial_out(): pl.pallas_call(functools.partial(experts_kernel, capacity, count, sets),...  16.8 us
    all_to_all x1, starting transfers between devices, shards(): ends = lax.all_to_all(totals, 'sp', split_axis=0, concat_axis=0, tiled=True)  11.5 us
    ppermute x1, waiting for transfers between devices, expert_over_chips(): lax.ppermute(after[middle:], 'tp', chip_shift(-1))  9.08 us
    ppermute x3, waiting for transfers between devices, gathered_projection(): lax.ppermute(out_proj, 'tp', chip_shift(distance))  6.71 us
    all_to_all x1, starting transfers between devices, mixed_and_outgoing(): lax.all_to_all(activated.reshape(size, tokens, -1), 'tp', split_axis=0, c...  6.48 us
    pallas_call x1, Pallas kernels, staged(): pl.pallas_call(stage_kernel, out_shape=[jax.ShapeDtypeStruct(array.shape,...  6.33 us
    ppermute x2, waiting for transfers between devices, expert_over_chips(): to_across = [lax.ppermute(part, 'tp', chip_shift(2)) for part in for_across]  5.87 us
  transfers between devices with their start and end apart: 20, of which 8 were waited for; matrix products, arithmetic and copies ran while one was open for 2% of the time, Pallas kernels for 19%

profile of v4, /device:TPU:24, one launch (start us, length us, event | category | flops | bytes accessed | tf_op | source)
XLA Modules:
  0.0 151.4 jit_solution(16458055757977979172)
XLA Ops:
  0.6 1.8 %collective-permute-start = (bf16[128,2048]{1,0:T(8,128)(2,1)}, bf16[128,2048]{1,0:T(8,128)(2,1)S(1)}, u32[]{:S(2)}, u32[]{:S(2)}) collective-permute-start(bf16[128,2048]{1,0:T(8,128)(2,1)} %refs_0_.1), channel_id=1, source_target_pairs={{0,2},{1,3},{2,4},{3,5},{4,6},{5,7},{6,0},{7,1},{8,10},{9,11},{10,... | collective-permute-start | bytes 1572872 | tf_op jit(solution)/shard_map/ppermute | solution.py:408
  2.4 1.0 collective-permute-start.1
  3.4 4.2 %states.1 = (f32[32,4,512]{2,1,0:T(4,128)}, f32[256,512]{1,0:T(8,128)}, f32[256,512]{1,0:T(8,128)}, f32[256,512]{1,0:T(8,128)}, f32[2,512]{1,0:T(2,128)}, /*index=5*/f32[4,8,512]{2,1,0:T(8,128)}) custom-call(bf16[256,128]{1,0:T(8,128)(2,1)} %refs_6_.1, f32[8,256]{1,0:T(8,128)} %bitcast.44, f32[8,64]{1,0:T(8,128)} %pole_real_hbm.1, f32[8,64]{1,0:T(8,128)} %pole_imag_hbm.1, ...), custom_call_target="tpu_custom_call" | custom-call | tf_op jit(solution)/shard_map/states/pallas_call | solution.py:253
  7.6 11.5 %all-to-all-start = ((f32[32,4,512]{2,1,0:T(4,128)}), f32[32,4,512]{2,1,0:T(4,128)}, u32[]{:S(2)}, u32[]{:S(2)}) async-start(f32[32,4,512]{2,1,0:T(4,128)} %get-tuple-element.42), calls=%async_computation | async-start | bytes 524288 | tf_op jit(solution)/shard_map/all_to_all | solution.py:544
  19.1 0.8 copy.29
  20.8 0.8 slice_subtract_fusion.1
  21.6 3.9 %collective-permute-done.refs_1_ = bf16[128,2048]{1,0:T(8,128)(2,1)S(1)} collective-permute-done((bf16[128,2048]{1,0:T(8,128)(2,1)}, bf16[128,2048]{1,0:T(8,128)(2,1)S(1)}, u32[]{:S(2)}, u32[]{:S(2)}) %collective-permute-start) | collective-permute-done | bytes 524320 | tf_op jit(solution)/shard_map/ppermute | solution.py:408
  26.2 2.8 %collective-permute-done.2.refs_3_ = bf16[128,2048]{1,0:T(8,128)(2,1)S(1)} collective-permute-done((bf16[128,2048]{1,0:T(8,128)(2,1)}, bf16[128,2048]{1,0:T(8,128)(2,1)S(1)}, u32[]{:S(2)}, u32[]{:S(2)}) %collective-permute-start.2) | collective-permute-done | bytes 524320 | tf_op jit(solution)/shard_map/ppermute | solution.py:408
  29.6 1.9 %all-to-all-done.refs_0_ = f32[32,4,512]{2,1,0:T(4,128)} async-done(((f32[32,4,512]{2,1,0:T(4,128)}), f32[32,4,512]{2,1,0:T(4,128)}, u32[]{:S(2)}, u32[]{:S(2)}) %all-to-all-start) | async-done | bytes 262176 | tf_op jit(solution)/shard_map/all_to_all | solution.py:544
  31.5 4.1 %response.1 = bf16[256,128]{1,0:T(8,128)(2,1)} custom-call(s32[1]{0:T(128)} %bitcast.here_ref, f32[32,4,512]{2,1,0:T(4,128)} %all-to-all-done.refs_0_, f32[256,512]{1,0:T(8,128)} %get-tuple-element.44.refs_1_, f32[256,512]{1,0:T(8,128)} %get-tuple-element.45.refs_2_, f32[256,512]{1,0:T(8,128)} %get-tuple-element.46.refs_3_, ...), custom_call_target="tpu_custom_call" | custom-call | tf_op jit(solution)/shard_map/response/pallas_call | solution.py:281
  35.6 6.5 %all-to-all-start.1 = ((bf16[8,32,128]{2,1,0:T(8,128)(2,1)}), bf16[8,32,128]{2,1,0:T(8,128)(2,1)S(1)}, u32[]{:S(2)}, u32[]{:S(2)}) async-start(bf16[8,32,128]{2,1,0:T(8,128)(2,1)} %bitcast.41), calls=%async_computation.1 | async-start | bytes 131072 | tf_op jit(solution)/shard_map/all_to_all | solution.py:445
  42.3 3.3 %all-to-all-done.1.arrived_ref = bf16[8,32,128]{2,1,0:T(8,128)(2,1)S(1)} async-done(((bf16[8,32,128]{2,1,0:T(8,128)(2,1)}), bf16[8,32,128]{2,1,0:T(8,128)(2,1)S(1)}, u32[]{:S(2)}, u32[]{:S(2)}) %all-to-all-start.1) | async-done | bytes 65568 | tf_op jit(solution)/shard_map/all_to_all | solution.py:445
  45.6 2.3 %mix.1 = (bf16[32,2048]{1,0:T(8,128)(2,1)S(1)}, bf16[256,1024]{1,0:T(8,128)(2,1)S(1)}) custom-call(s32[8]{0:T(128)S(1)} %pad_add_fusion.1.order_ref, bf16[8,32,128]{2,1,0:T(8,128)(2,1)S(1)} %all-to-all-done.1.arrived_ref, bf16[32,2048]{1,0:T(8,128)(2,1)S(1)} %copy-done.1, f32[1,2048]{1,0:T(1,128)S(1)} %bitcast.40, s32[64,2]{1,0:T(8,128)S(1)} %reshape.193.places_ref, ...), custom_call_target="tpu_custom_call" | custom-call | tf_op jit(solution)/shard_map/mix/pallas_call | solution.py:450
  47.9 23.8 %all_to_all.20 = bf16[32,8,1024]{2,1,0:T(8,128)(2,1)S(1)} all-to-all(bf16[32,8,1024]{2,1,0:T(8,128)(2,1)S(1)} %bitcast.39), channel_id=1, replica_groups=mesh['sp'=32,'tp'=8] {'sp'}, dimensions={0} | all-to-all | bytes 1048576 | tf_op jit(solution)/shard_map/all_to_all | solution.py:465
  71.8 0.6 collective-permute-start.10
  72.4 2.8 %collective-permute-start.9 = (bf16[256,1024]{1,0:T(8,128)(2,1)S(1)}, bf16[256,1024]{1,0:T(8,128)(2,1)S(1)}, u32[]{:S(2)}, u32[]{:S(2)}) collective-permute-start(bf16[256,1024]{1,0:T(8,128)(2,1)S(1)} %bitcast.37), channel_id=1, source_target_pairs={{0,2},{1,3},{2,4},{3,5},{4,6},{5,7},{6,0},{7,1},{8,10},{9,11},{10,... | collective-permute-start | bytes 1572872 | tf_op jit(solution)/shard_map/ppermute | solution.py:474
  75.3 6.3 %stage.1 = (bf16[2048,896]{1,0:T(8,128)(2,1)S(1)}, bf16[2048,896]{1,0:T(8,128)(2,1)S(1)}, bf16[896,2048]{1,0:T(8,128)(2,1)S(1)}, bf16[2048,896]{1,0:T(8,128)(2,1)S(1)}, bf16[896,2048]{1,0:T(8,128)(2,1)S(1)}) custom-call(bf16[2048,896]{1,0:T(8,128)(2,1)} %bitcast.16.refs_0_, bf16[2048,896]{1,0:T(8,128)(2,1)} %bitcast.50, bf16[896,2048]{1,0:T(8,128)(2,1)} %bitcast.52, ...), custom_call_target="tpu_custom_call" | custom-call | flops 8589934592 | tf_op jit(solution)/shard_map/stage/pallas_call | solution.py:371
  81.6 5.7 %collective-permute-done.10.refs_0_ = bf16[256,1024]{1,0:T(8,128)(2,1)S(1)} collective-permute-done((bf16[256,1024]{1,0:T(8,128)(2,1)S(1)}, bf16[256,1024]{1,0:T(8,128)(2,1)S(1)}, u32[]{:S(2)}, u32[]{:S(2)}) %collective-permute-start.10) | collective-permute-done | bytes 524320 | tf_op jit(solution)/shard_map/ppermute | solution.py:475
  87.4 4.2 %experts.4 = bf16[256,1024]{1,0:T(8,128)(2,1)S(1)} custom-call(bf16[256,1024]{1,0:T(8,128)(2,1)S(1)} %collective-permute-done.9.refs_0_, bf16[2048,896]{1,0:T(8,128)(2,1)S(1)} %get-tuple-element.67.refs_1_.refs_2_, bf16[2048,896]{1,0:T(8,128)(2,1)S(1)} %get-tuple-element.68.refs_2_.refs_3_, bf16[896,2048]{1,0:T(8,128)(2,1)S(1)} %get-tuple-element.69.refs_3_.refs_4_, ...), custom_call_target="tpu_custom_call" | custom-call | flops 2818572288 | tf_op jit(solution)/shard_map/experts/pallas_call | solution.py:348
  91.6 0.6 collective-permute-start.14
  92.2 2.7 %collective-permute-start.12 = (bf16[128,1024]{1,0:T(8,128)(2,1)S(1)}, bf16[128,1024]{1,0:T(8,128)(2,1)S(1)}, u32[]{:S(2)}, u32[]{:S(2)}) collective-permute-start(bf16[128,1024]{1,0:T(8,128)(2,1)S(1)} %slice.28), channel_id=1, source_target_pairs={{0,2},{1,3},{2,4},{3,5},{4,6},{5,7},{6,0},{7,1},{8,10},{9,11},{10,... | collective-permute-start | bytes 786440 | tf_op jit(solution)/shard_map/ppermute | solution.py:482
  94.9 4.2 %experts.5 = bf16[256,1024]{1,0:T(8,128)(2,1)S(1)} custom-call(bf16[256,1024]{1,0:T(8,128)(2,1)S(1)} %collective-permute-done.10.refs_0_, bf16[2048,896]{1,0:T(8,128)(2,1)S(1)} %get-tuple-element.67.refs_1_.refs_2_, bf16[2048,896]{1,0:T(8,128)(2,1)S(1)} %get-tuple-element.68.refs_2_.refs_3_, bf16[896,2048]{1,0:T(8,128)(2,1)S(1)} %get-tuple-element.69.refs_3_.refs_4_, ...), custom_call_target="tpu_custom_call" | custom-call | flops 2818572288 | tf_op jit(solution)/shard_map/experts/pallas_call | solution.py:348
  99.1 3.5 %collective-permute-start.15 = (bf16[256,1024]{1,0:T(8,128)(2,1)S(1)}, bf16[256,1024]{1,0:T(8,128)(2,1)S(1)}, u32[]{:S(2)}, u32[]{:S(2)}) collective-permute-start(bf16[256,1024]{1,0:T(8,128)(2,1)S(1)} %experts.5), channel_id=1, source_target_pairs={{0,2},{1,3},{2,4},{3,5},{4,6},{5,7},{6,0},{7,1},{8,10},{9,11},{10,... | collective-permute-start | bytes 1572872 | tf_op jit(solution)/shard_map/ppermute | solution.py:489
  102.6 9.1 %collective-permute-done.13.refs_1_ = bf16[128,1024]{1,0:T(8,128)(2,1)S(1)} collective-permute-done((bf16[128,1024]{1,0:T(8,128)(2,1)S(1)}, bf16[128,1024]{1,0:T(8,128)(2,1)S(1)}, u32[]{:S(2)}, u32[]{:S(2)}) %collective-permute-start.13) | collective-permute-done | bytes 262176 | tf_op jit(solution)/shard_map/ppermute | solution.py:483
  111.7 4.2 %experts.6 = (bf16[128,1024]{1,0:T(8,128)(2,1)S(1)}, bf16[128,1024]{1,0:T(8,128)(2,1)S(1)}) custom-call(bf16[128,1024]{1,0:T(8,128)(2,1)S(1)} %collective-permute-done.12.refs_0_, bf16[128,1024]{1,0:T(8,128)(2,1)S(1)} %collective-permute-done.13.refs_1_, bf16[2048,896]{1,0:T(8,128)(2,1)S(1)} %get-tuple-element.67.refs_1_.refs_2_, ...), custom_call_target="tpu_custom_call" | custom-call | flops 2818572288 | tf_op jit(solution)/shard_map/experts/pallas_call | solution.py:348
  115.9 0.6 collective-permute-start.16
  116.5 3.0 %collective-permute-start.17 = (bf16[128,1024]{1,0:T(8,128)(2,1)S(1)}, bf16[128,1024]{1,0:T(8,128)(2,1)S(1)}, u32[]{:S(2)}, u32[]{:S(2)}) collective-permute-start(bf16[128,1024]{1,0:T(8,128)(2,1)S(1)} %get-tuple-element.77), channel_id=1, source_target_pairs={{0,4},{1,5},{2,6},{3,7},{4,0},{5,1},{6,2},{7,3},{8,12},{9,13},{10,... | collective-permute-start | bytes 786440 | tf_op jit(solution)/shard_map/ppermute | solution.py:492
  119.5 4.2 %experts.7 = bf16[256,1024]{1,0:T(8,128)(2,1)S(1)} custom-call(bf16[256,1024]{1,0:T(8,128)(2,1)S(1)} %bitcast.38, bf16[2048,896]{1,0:T(8,128)(2,1)S(1)} %get-tuple-element.67.refs_1_.refs_2_, bf16[2048,896]{1,0:T(8,128)(2,1)S(1)} %get-tuple-element.68.refs_2_.refs_3_, bf16[896,2048]{1,0:T(8,128)(2,1)S(1)} %get-tuple-element.69.refs_3_.refs_4_, ...), custom_call_target="tpu_custom_call" | custom-call | flops 2818572288 | tf_op jit(solution)/shard_map/experts/pallas_call | solution.py:348
  124.0 2.7 %collective-permute-done.16 = bf16[128,1024]{1,0:T(8,128)(2,1)S(1)} collective-permute-done((bf16[128,1024]{1,0:T(8,128)(2,1)S(1)}, bf16[128,1024]{1,0:T(8,128)(2,1)S(1)}, u32[]{:S(2)}, u32[]{:S(2)}) %collective-permute-start.16) | collective-permute-done | bytes 262176 | tf_op jit(solution)/shard_map/ppermute | solution.py:492
  126.7 3.2 %collective-permute-done.17 = bf16[128,1024]{1,0:T(8,128)(2,1)S(1)} collective-permute-done((bf16[128,1024]{1,0:T(8,128)(2,1)S(1)}, bf16[128,1024]{1,0:T(8,128)(2,1)S(1)}, u32[]{:S(2)}, u32[]{:S(2)}) %collective-permute-start.17) | collective-permute-done | bytes 262176 | tf_op jit(solution)/shard_map/ppermute | solution.py:492
  130.0 20.4 %all_to_all.21 = bf16[32,8,1024]{2,1,0:T(8,128)(2,1)S(1)} all-to-all(bf16[32,8,1024]{2,1,0:T(8,128)(2,1)S(1)} %fusion), channel_id=1, replica_groups=mesh['sp'=32,'tp'=8] {'sp'}, dimensions={0} | all-to-all | bytes 1048576 | tf_op jit(solution)/shard_map/all_to_all | solution.py:465
  150.7 0.7 fusion.3
  (53 shorter events, 3.7 us)
Async XLA Ops:
  0.0 45.6 %copy-start = (bf16[128,2048]{1,0:T(8,128)(2,1)S(1)}, bf16[128,2048]{1,0:T(8,128)(2,1)}, u32[]{:S(2)}) copy-start(bf16[128,2048]{1,0:T(8,128)(2,1)} %refs_0_.1) | copy-start | bytes 1572868
  0.0 45.6 %copy-start.2 = (f32[2048]{0:T(1024)S(1)}, f32[2048]{0:T(1024)}, u32[]{:S(2)}) copy-start(f32[2048]{0:T(1024)} %param.26) | copy-start | bytes 24580
  0.0 45.6 %copy-start.1 = (bf16[32,2048]{1,0:T(8,128)(2,1)S(1)}, bf16[32,2048]{1,0:T(8,128)(2,1)}, u32[]{:S(2)}) copy-start(bf16[32,2048]{1,0:T(8,128)(2,1)} %stream_ref.1) | copy-start | bytes 393220
  0.0 71.8 %collective-permute-start.7 = (bf16[2048,896]{1,0:T(8,128)(2,1)}, bf16[2048,896]{1,0:T(8,128)(2,1)}, u32[]{:S(2)}, u32[]{:S(2)}) collective-permute-start(bf16[2048,896]{1,0:T(8,128)(2,1)} %bitcast.49), channel_id=1, source_target_pairs={{0,1},{1,0},{2,3},{3,2},{4,5},{5,4},{6,7},{7,6},{8,9},{9,8},{10,11... | collective-permute-start | bytes 11010056 | tf_op jit(solution)/shard_map/ppermute | solution.py:534
  0.1 71.7 %collective-permute-start.8 = (bf16[896,2048]{1,0:T(8,128)(2,1)}, bf16[896,2048]{1,0:T(8,128)(2,1)}, u32[]{:S(2)}, u32[]{:S(2)}) collective-permute-start(bf16[896,2048]{1,0:T(8,128)(2,1)} %bitcast.51), channel_id=1, source_target_pairs={{0,1},{1,0},{2,3},{3,2},{4,5},{5,4},{6,7},{7,6},{8,9},{9,8},{10,11... | collective-permute-start | bytes 11010056 | tf_op jit(solution)/shard_map/ppermute | solution.py:533
  0.6 24.9 %collective-permute-start = (bf16[128,2048]{1,0:T(8,128)(2,1)}, bf16[128,2048]{1,0:T(8,128)(2,1)S(1)}, u32[]{:S(2)}, u32[]{:S(2)}) collective-permute-start(bf16[128,2048]{1,0:T(8,128)(2,1)} %refs_0_.1), channel_id=1, source_target_pairs={{0,2},{1,3},{2,4},{3,5},{4,6},{5,7},{6,0},{7,1},{8,10},{9,11},{10,... | collective-permute-start | bytes 1572872 | tf_op jit(solution)/shard_map/ppermute | solution.py:408
  2.4 23.2 %collective-permute-start.1 = (bf16[128,2048]{1,0:T(8,128)(2,1)}, bf16[128,2048]{1,0:T(8,128)(2,1)S(1)}, u32[]{:S(2)}, u32[]{:S(2)}) collective-permute-start(bf16[128,2048]{1,0:T(8,128)(2,1)} %refs_0_.1), channel_id=1, source_target_pairs={{0,4},{1,5},{2,6},{3,7},{4,0},{5,1},{6,2},{7,3},{8,12},{9,13},{10,... | collective-permute-start | bytes 1572872 | tf_op jit(solution)/shard_map/ppermute | solution.py:408
  3.4 25.6 %collective-permute-start.2 = (bf16[128,2048]{1,0:T(8,128)(2,1)}, bf16[128,2048]{1,0:T(8,128)(2,1)S(1)}, u32[]{:S(2)}, u32[]{:S(2)}) collective-permute-start(bf16[128,2048]{1,0:T(8,128)(2,1)} %refs_0_.1), channel_id=1, source_target_pairs={{0,6},{1,7},{2,0},{3,1},{4,2},{5,3},{6,4},{7,5},{8,14},{9,15},{10,... | collective-permute-start | bytes 1572872 | tf_op jit(solution)/shard_map/ppermute | solution.py:408
  7.6 23.8 %all-to-all-start = ((f32[32,4,512]{2,1,0:T(4,128)}), f32[32,4,512]{2,1,0:T(4,128)}, u32[]{:S(2)}, u32[]{:S(2)}) async-start(f32[32,4,512]{2,1,0:T(4,128)} %get-tuple-element.42), calls=%async_computation | async-start | bytes 524288 | tf_op jit(solution)/shard_map/all_to_all | solution.py:544
  25.5 3.7 %collective-permute-start.3 = (bf16[128,2048]{1,0:T(8,128)(2,1)}, bf16[128,2048]{1,0:T(8,128)(2,1)S(1)}, u32[]{:S(2)}, u32[]{:S(2)}) collective-permute-start(bf16[128,2048]{1,0:T(8,128)(2,1)} %refs_0_.1), channel_id=1, source_target_pairs={{0,1},{1,0},{2,3},{3,2},{4,5},{5,4},{6,7},{7,6},{8,9},{9,8},{10,11... | collective-permute-start | bytes 1572872 | tf_op jit(solution)/shard_map/ppermute | solution.py:410
  25.7 20.0 %collective-permute-start.4 = (bf16[128,2048]{1,0:T(8,128)(2,1)S(1)}, bf16[128,2048]{1,0:T(8,128)(2,1)S(1)}, u32[]{:S(2)}, u32[]{:S(2)}) collective-permute-start(bf16[128,2048]{1,0:T(8,128)(2,1)S(1)} %collective-permute-done.refs_1_), channel_id=1, source_target_pairs={{0,1},{1,0},{2,3},{3,2},{4,5},{5,4},{6,7},{7,6},{8,9},{9,8},{10,11... | collective-permute-start | bytes 1572872 | tf_op jit(solution)/shard_map/ppermute | solution.py:410
  29.0 16.6 %collective-permute-start.5 = (bf16[128,2048]{1,0:T(8,128)(2,1)S(1)}, bf16[128,2048]{1,0:T(8,128)(2,1)}, u32[]{:S(2)}, u32[]{:S(2)}) collective-permute-start(bf16[128,2048]{1,0:T(8,128)(2,1)S(1)} %collective-permute-done.1.refs_2_), channel_id=1, source_target_pairs={{0,1},{1,0},{2,3},{3,2},{4,5},{5,4},{6,7},{7,6},{8,9},{9,8},{10,11... | collective-permute-start | bytes 1572872 | tf_op jit(solution)/shard_map/ppermute | solution.py:410
  29.2 16.4 %collective-permute-start.6 = (bf16[128,2048]{1,0:T(8,128)(2,1)S(1)}, bf16[128,2048]{1,0:T(8,128)(2,1)}, u32[]{:S(2)}, u32[]{:S(2)}) collective-permute-start(bf16[128,2048]{1,0:T(8,128)(2,1)S(1)} %collective-permute-done.2.refs_3_), channel_id=1, source_target_pairs={{0,1},{1,0},{2,3},{3,2},{4,5},{5,4},{6,7},{7,6},{8,9},{9,8},{10,11... | collective-permute-start | bytes 1572872 | tf_op jit(solution)/shard_map/ppermute | solution.py:410
  35.6 10.0 %all-to-all-start.1 = ((bf16[8,32,128]{2,1,0:T(8,128)(2,1)}), bf16[8,32,128]{2,1,0:T(8,128)(2,1)S(1)}, u32[]{:S(2)}, u32[]{:S(2)}) async-start(bf16[8,32,128]{2,1,0:T(8,128)(2,1)} %bitcast.41), calls=%async_computation.1 | async-start | bytes 131072 | tf_op jit(solution)/shard_map/all_to_all | solution.py:445
  71.8 15.6 %collective-permute-start.11 = (bf16[2048,896]{1,0:T(8,128)(2,1)}, bf16[2048,896]{1,0:T(8,128)(2,1)S(1)}, u32[]{:S(2)}, u32[]{:S(2)}) collective-permute-start(bf16[2048,896]{1,0:T(8,128)(2,1)} %bitcast.16.refs_0_), channel_id=1, source_target_pairs={{0,1},{1,0},{2,3},{3,2},{4,5},{5,4},{6,7},{7,6},{8,9},{9,8},{10,11... | collective-permute-start | bytes 11010056 | tf_op jit(solution)/shard_map/ppermute | solution.py:476
  71.8 15.5 %collective-permute-start.10 = (bf16[256,1024]{1,0:T(8,128)(2,1)S(1)}, bf16[256,1024]{1,0:T(8,128)(2,1)S(1)}, u32[]{:S(2)}, u32[]{:S(2)}) collective-permute-start(bf16[256,1024]{1,0:T(8,128)(2,1)S(1)} %bitcast.36), channel_id=1, source_target_pairs={{0,6},{1,7},{2,0},{3,1},{4,2},{5,3},{6,4},{7,5},{8,14},{9,15},{10,... | collective-permute-start | bytes 1572872 | tf_op jit(solution)/shard_map/ppermute | solution.py:475
  72.4 14.9 %collective-permute-start.9 = (bf16[256,1024]{1,0:T(8,128)(2,1)S(1)}, bf16[256,1024]{1,0:T(8,128)(2,1)S(1)}, u32[]{:S(2)}, u32[]{:S(2)}) collective-permute-start(bf16[256,1024]{1,0:T(8,128)(2,1)S(1)} %bitcast.37), channel_id=1, source_target_pairs={{0,2},{1,3},{2,4},{3,5},{4,6},{5,7},{6,0},{7,1},{8,10},{9,11},{10,... | collective-permute-start | bytes 1572872 | tf_op jit(solution)/shard_map/ppermute | solution.py:474
  91.6 32.2 %collective-permute-start.14 = (bf16[256,1024]{1,0:T(8,128)(2,1)S(1)}, bf16[256,1024]{1,0:T(8,128)(2,1)S(1)}, u32[]{:S(2)}, u32[]{:S(2)}) collective-permute-start(bf16[256,1024]{1,0:T(8,128)(2,1)S(1)} %experts.4), channel_id=1, source_target_pairs={{0,6},{1,7},{2,0},{3,1},{4,2},{5,3},{6,4},{7,5},{8,14},{9,15},{10,... | collective-permute-start | bytes 1572872 | tf_op jit(solution)/shard_map/ppermute | solution.py:486
  92.2 10.4 %collective-permute-start.12 = (bf16[128,1024]{1,0:T(8,128)(2,1)S(1)}, bf16[128,1024]{1,0:T(8,128)(2,1)S(1)}, u32[]{:S(2)}, u32[]{:S(2)}) collective-permute-start(bf16[128,1024]{1,0:T(8,128)(2,1)S(1)} %slice.28), channel_id=1, source_target_pairs={{0,2},{1,3},{2,4},{3,5},{4,6},{5,7},{6,0},{7,1},{8,10},{9,11},{10,... | collective-permute-start | bytes 786440 | tf_op jit(solution)/shard_map/ppermute | solution.py:482
  94.9 16.8 %collective-permute-start.13 = (bf16[128,1024]{1,0:T(8,128)(2,1)S(1)}, bf16[128,1024]{1,0:T(8,128)(2,1)S(1)}, u32[]{:S(2)}, u32[]{:S(2)}) collective-permute-start(bf16[128,1024]{1,0:T(8,128)(2,1)S(1)} %slice.29), channel_id=1, source_target_pairs={{0,6},{1,7},{2,0},{3,1},{4,2},{5,3},{6,4},{7,5},{8,14},{9,15},{10,... | collective-permute-start | bytes 786440 | tf_op jit(solution)/shard_map/ppermute | solution.py:483
  99.1 24.7 %collective-permute-start.15 = (bf16[256,1024]{1,0:T(8,128)(2,1)S(1)}, bf16[256,1024]{1,0:T(8,128)(2,1)S(1)}, u32[]{:S(2)}, u32[]{:S(2)}) collective-permute-start(bf16[256,1024]{1,0:T(8,128)(2,1)S(1)} %experts.5), channel_id=1, source_target_pairs={{0,2},{1,3},{2,4},{3,5},{4,6},{5,7},{6,0},{7,1},{8,10},{9,11},{10,... | collective-permute-start | bytes 1572872 | tf_op jit(solution)/shard_map/ppermute | solution.py:489
  115.9 10.8 %collective-permute-start.16 = (bf16[128,1024]{1,0:T(8,128)(2,1)S(1)}, bf16[128,1024]{1,0:T(8,128)(2,1)S(1)}, u32[]{:S(2)}, u32[]{:S(2)}) collective-permute-start(bf16[128,1024]{1,0:T(8,128)(2,1)S(1)} %get-tuple-element.76), channel_id=1, source_target_pairs={{0,4},{1,5},{2,6},{3,7},{4,0},{5,1},{6,2},{7,3},{8,12},{9,13},{10,... | collective-permute-start | bytes 786440 | tf_op jit(solution)/shard_map/ppermute | solution.py:492
  116.5 13.3 %collective-permute-start.17 = (bf16[128,1024]{1,0:T(8,128)(2,1)S(1)}, bf16[128,1024]{1,0:T(8,128)(2,1)S(1)}, u32[]{:S(2)}, u32[]{:S(2)}) collective-permute-start(bf16[128,1024]{1,0:T(8,128)(2,1)S(1)} %get-tuple-element.77), channel_id=1, source_target_pairs={{0,4},{1,5},{2,6},{3,7},{4,0},{5,1},{6,2},{7,3},{8,12},{9,13},{10,... | collective-permute-start | bytes 786440 | tf_op jit(solution)/shard_map/ppermute | solution.py:492
